TPU v7x, 128 devices: a whole 4x4x4 slice. The times are simulated.
128 devices in a mesh: pp: 4 (over x), fs: 4 (over y), tp: 8 (over z, core).
Axes of the slice: x: 4, y: 4, z: 4, core: 2. Of those that a mesh axis runs over, the one named last changes fastest.
Arguments:
- micro_in: bfloat16 [2, 96, 1024], P(None, 'pp', ('tp', 'fs')), may hold values from -6 to 6
- norm_gain: float32 [4, 1024], P('pp'), may hold values from 0.5 to 1.5
- proj_gate: bfloat16 [4, 1024, 8, 4, 64], P('pp', None, 'tp', 'fs'), may hold values from -0.1875 to 0.1875
- proj_value: bfloat16 [4, 1024, 8, 4, 64], P('pp', None, 'tp', 'fs'), may hold values from -0.1875 to 0.1875
- proj_write: bfloat16 [4, 1024, 8, 128], P('pp', None, 'tp'), may hold values from -0.1875 to 0.1875
- proj_read: bfloat16 [4, 1024, 8, 128], P('pp', None, 'tp'), may hold values from -0.1875 to 0.1875
- proj_step: bfloat16 [4, 1024, 2, 8, 4], P('pp', None, None, 'tp', 'fs'), may hold values from -0.1875 to 0.1875
- step_bias: float32 [4, 2, 8, 4], P('pp', None, 'tp', 'fs'), may hold values from -4.6 to -2.3
- decay_log: float32 [4, 2, 8, 4], P('pp', None, 'tp', 'fs'), may hold values from 0 to 2.77
- skip_gain: float32 [4, 8, 4], P('pp', 'tp', 'fs'), may hold values from 0.5 to 1.5
- conv_value: float32 [4, 5, 8, 4, 64], P('pp', None, 'tp', 'fs'), may hold values from -2.5 to 2.5
- conv_write: float32 [4, 5, 8, 128], P('pp', None, 'tp'), may hold values from -2.5 to 2.5
- conv_read: float32 [4, 5, 8, 128], P('pp', None, 'tp'), may hold values from -2.5 to 2.5
- proj_out: bfloat16 [4, 8, 4, 64, 1024], P('pp', 'tp', 'fs'), may hold values from -0.125 to 0.125
Outputs:
- mixed_out: bfloat16 [2, 96, 1024], P(None, 'pp', ('tp', 'fs'))
All inputs are finite; a program needn't handle non-finite values.
Results may differ from a plain program's by a relative error of at most 0.025.
Values may be sent and summed in bfloat16 or wider, within the bound.
No kernel may reach another device: no remote copies, remote signals or barrier semaphores. Data moves between devices by JAX's collectives and lax.ppermute only.
A program may use at most 64 MiB of HBM per device.

v0:
```python
import jax
import jax.numpy as jnp
from jax import lax
from jax.experimental import pallas as pl
from jax.experimental.pallas import tpu as pltpu
from jax.sharding import Mesh
from jax.sharding import PartitionSpec as P


FS = ("ym", "yh")
TP = ("tz", "tc")
BLOCKS = ("pp", "tz", "tc")
EPS = 1e-06
T = 96
D = 1024
F32 = jnp.float32
BF16 = jnp.bfloat16
ROWS = 168


def lanes(shape):
    return lax.broadcasted_iota(jnp.int32, shape, len(shape) - 1)


def split3(v):
    hi = v.astype(BF16).astype(F32)
    mid = (v - hi).astype(BF16).astype(F32)
    low = v - hi - mid
    return hi, mid, low


def permuted(v):
    group = lanes((v.shape[0], 128)) // 32
    out = []
    for h in range(2):
        for c in range(2):
            for p in range(2):
                block = None
                for g in range(4):
                    zz, m = g // 2, g % 2
                    n = (2 * p + zz) * 2 + c
                    moved = v[:, n * 128 : (n + 1) * 128]
                    turn = (64 * zz - 32 * m - 32 * h) % 128
                    if turn:
                        moved = pltpu.roll(moved, turn, 1)
                    block = moved if block is None else jnp.where(group == g, moved, block)
                out.append(block)
    return out


def pack_kernel(
    where_ref,
    micro_hbm,
    gate_hbm,
    value_hbm,
    step_hbm,
    out_hbm,
    taps_hbm,
    bias_hbm,
    decay_hbm,
    skip_hbm,
    gain_hbm,
    near_ref,
    away_ref,
    same_ref,
    other_ref,
    gain_out,
    *scratch,
):
    sources = (
        gate_hbm,
        value_hbm,
        out_hbm,
        step_hbm,
        taps_hbm,
        bias_hbm,
        decay_hbm,
        skip_hbm,
        gain_hbm,
        micro_hbm,
    )
    buffers, sems = scratch[:-1], scratch[-1]
    copies = [pltpu.make_async_copy(s, b, sems.at[i]) for i, (s, b) in enumerate(zip(sources, buffers))]
    for copy in copies:
        copy.start()
    for copy in copies:
        copy.wait()
    gate_ref, value_ref, out_ref, step_ref, taps_ref, bias_ref, decay_ref, skip_ref, gain_ref, micro_ref = buffers
    core = where_ref[1] == 0
    half = where_ref[0] == 0
    gate = jnp.concatenate(permuted(gate_ref[...].astype(F32)), axis=1).astype(BF16)
    value = jnp.concatenate(permuted(value_ref[...].astype(F32)), axis=1).astype(BF16)
    step = jnp.concatenate(permuted(step_ref[...].astype(F32)), axis=1)
    gain_out[...] = jnp.concatenate(permuted(gain_ref[...]), axis=1)
    blank = jnp.zeros((1, 64), F32)
    wide = lambda ref, k: jnp.broadcast_to(ref[:, k : k + 1], (1, 128))
    row_a = [piece for k in range(5) for piece in (blank, taps_ref[k])]
    row_a = jnp.concatenate(row_a + [wide(bias_ref, 0), wide(bias_ref, 1), blank, blank], axis=1)
    row_b = [wide(decay_ref, 0), wide(decay_ref, 1), wide(skip_ref, 0)] + [blank] * 10
    row_b = jnp.concatenate(row_b, axis=1)
    misc = jnp.concatenate([step, *split3(row_a), *split3(row_b)], axis=0).astype(BF16)
    out = permuted(out_ref[...].astype(F32))
    halves = []
    for h in range(2):
        first, second = out[4 * h : 4 * h + 2], out[4 * h + 2 : 4 * h + 4]
        own = [jnp.where(core, a, b) for a, b in zip(first, second)]
        far = [jnp.where(core, b, a) for a, b in zip(first, second)]
        halves.append(jnp.concatenate(own + far, axis=1))
    for ref, pick in ((same_ref, half), (other_ref, jnp.logical_not(half))):
        part = jnp.where(pick, halves[0], halves[1])
        ref[0:64] = gate
        ref[64:128] = value
        ref[128:160] = jnp.concatenate([part[0:32], part[32:64]], axis=1).astype(BF16)
        ref[160:168] = misc
    first = where_ref[3] == 0
    near_ref[...] = jnp.where(first, micro_ref[0], micro_ref[1])
    away_ref[...] = jnp.where(first, micro_ref[1], micro_ref[0])


def block_kernel(where_ref, r0_ref, r1_ref, r2_ref, r3_ref, send_ref):
    y = 2 * where_ref[3] + where_ref[0]
    group = lanes((24, 128)) // 32
    blank = jnp.zeros((24, 96), F32)
    block = jnp.zeros((24, 128), F32)
    for bits, ref in enumerate((r0_ref, r1_ref, r2_ref, r3_ref)):
        wide = jnp.concatenate([ref[...].astype(F32), blank], axis=1)
        for k in range(4):
            moved = wide if k == 0 else pltpu.roll(wide, 32 * k, 1)
            block = jnp.where((group == k) & ((y ^ bits) == k), moved, block)
    block = block.astype(BF16)
    for peer in range(32):
        send_ref[peer] = block


def nt_dot(a, b):
    return lax.dot_general(a, b, (((1,), (1,)), ((), ())), preferred_element_type=F32)


def nn_dot(a, b):
    return lax.dot_general(a, b, (((1,), (0,)), ((), ())), preferred_element_type=F32)


def silu(v):
    return v * jax.nn.sigmoid(v)


def section_body(quarters, weight_refs, write_ref, read_ref, gain_ref, taps_refs, own_ref, far_ref, pad_ref):
    low = lanes((T, 128)) < 64
    total = None
    for pair in quarters:
        for q in pair:
            sq = q * q
            sq = sq[:, :128] + sq[:, 128:]
            total = sq if total is None else total + sq
    scale = lax.rsqrt(jnp.sum(total, axis=1, keepdims=True) * (1.0 / D) + EPS)
    blocks = []
    for h in range(2):
        for c in range(2):
            n = (2 * h + c) * 256
            blocks.append((quarters[h][c] * scale * gain_ref[:, n : n + 256]).astype(BF16))
    normed = jnp.concatenate(blocks, axis=1)

    step_rows = jnp.concatenate([w[160:168].astype(F32)[0:2] for w in weight_refs], axis=0)
    step_raw = nt_dot(step_rows.astype(BF16), normed)
    small = []
    for w in weight_refs:
        misc = w[160:168].astype(F32)
        small.append((misc[2:3] + misc[3:4] + misc[4:5], misc[5:6] + misc[6:7] + misc[7:8]))
    bias = jnp.concatenate([s[0][:, 640 + 128 * d : 640 + 128 * d + T] for s in small for d in range(2)], axis=0)
    decay = jnp.concatenate([s[1][:, 128 * d : 128 * d + T] for s in small for d in range(2)], axis=0)
    raw = step_raw + bias
    dt = jnp.maximum(raw, 0.0) + jnp.log1p(jnp.exp(-jnp.abs(raw)))
    log_decay = dt * (-jnp.exp(decay))
    parts = [s.astype(BF16) for s in split3(log_decay)]
    row_id = lax.broadcasted_iota(jnp.int32, (T, T), 0)
    col_id = lax.broadcasted_iota(jnp.int32, (T, T), 1)
    upto = (row_id <= col_id).astype(F32).astype(BF16)
    since = (row_id >= col_id).astype(F32).astype(BF16)
    fwd_all = (nn_dot(parts[0], upto) + nn_dot(parts[1], upto)) + nn_dot(parts[2], upto)
    bwd_all = (nn_dot(parts[0], since) + nn_dot(parts[1], since)) + nn_dot(parts[2], since)
    odd = lax.broadcasted_iota(jnp.int32, (8, T), 0) % 2 == 1
    cum = jnp.where(odd, bwd_all, fwd_all)
    cum_pad = jnp.concatenate([cum, jnp.zeros((8, 128 - T), F32)], axis=1)
    cum_cols = cum_pad.T[:T]

    gv01 = nt_dot(normed, jnp.concatenate([weight_refs[0][0:128], weight_refs[1][0:128]], axis=0))
    gv23 = nt_dot(normed, jnp.concatenate([weight_refs[2][0:128], weight_refs[3][0:128]], axis=0))
    wr_rows = [
        jnp.concatenate([r[n * 128 + y * 32 : n * 128 + y * 32 + 32] for r in (write_ref, read_ref)], axis=1)
        for h in range(2)
        for c in range(2)
        for n in (c, 2 + c, 4 + c, 6 + c)
        for y in (h, 2 + h)
    ]
    wr = nn_dot(normed, jnp.concatenate(wr_rows, axis=0))
    pad_ref[0:8] = jnp.zeros((8, 768), F32)
    pad_ref[8 + T : 16 + T] = jnp.zeros((8, 768), F32)
    pad_ref[8 : 8 + T, 0:256] = gv01.astype(BF16).astype(F32)
    pad_ref[8 : 8 + T, 256:512] = gv23.astype(BF16).astype(F32)
    pad_ref[8 : 8 + T, 512:768] = wr.astype(BF16).astype(F32)
    acts = []
    for g in range(6):
        span = slice(g * 128, (g + 1) * 128)
        acc = None
        for k in range(5):
            tap = small[g][0][:, k * 128 : (k + 1) * 128] if g < 4 else taps_refs[g - 4][k]
            term = pad_ref[6 + k : 6 + k + T, span] * tap
            acc = term if acc is None else acc + term
        acts.append(silu(acc).astype(BF16))
    scores = nt_dot(acts[5], acts[4])
    lower = row_id >= col_id
    diagonal = row_id == col_id
    gated = []
    for j in range(4):
        fc = cum_cols[:, 2 * j : 2 * j + 1]
        bc = cum_cols[:, 2 * j + 1 : 2 * j + 2]
        fr = cum[2 * j : 2 * j + 1]
        br = cum[2 * j + 1 : 2 * j + 2]
        d0 = dt[2 * j : 2 * j + 1]
        d1 = dt[2 * j + 1 : 2 * j + 2]
        mix = jnp.exp(jnp.where(lower, fc - fr, bc - br)) * jnp.where(lower, d0, d1)
        mix = mix + jnp.where(diagonal, d1, 0.0)
        combined = scores * mix
        high = combined.astype(BF16)
        rest = (combined - high.astype(F32)).astype(BF16)
        y = nn_dot(high, acts[j]) + nn_dot(rest, acts[j])
        y = y + small[j][1][:, 256:384] * acts[j].astype(F32)
        gate = pltpu.roll(pad_ref[8 : 8 + T, j * 128 : (j + 1) * 128], 64, 1)
        gated.append(y * silu(gate))
    pairs = [jnp.where(low, pltpu.roll(gated[2 * i], 64, 1), gated[2 * i + 1]).astype(BF16) for i in range(2)]
    gated_all = jnp.concatenate(pairs, axis=1)
    for side, ref in ((0, own_ref), (1, far_ref)):
        weight = jnp.concatenate(
            [
                w[128:160, 512 * r + 256 * side : 512 * r + 256 * side + 256]
                for w in weight_refs
                for r in range(2)
            ],
            axis=0,
        )
        ref[...] = nn_dot(gated_all, weight).astype(ref.dtype)


def entry_section_kernel(where_ref, recv_ref, *refs):
    *rest, quarter_out, own_ref, far_ref, pad_ref, quarter_ref = refs
    tokens = [
        jnp.concatenate([recv_ref[x * 8 + n].astype(F32) for x in range(4)], axis=0) for n in range(8)
    ]
    blocks = permuted(jnp.concatenate(tokens, axis=1))
    for q in range(4):
        quarter_ref[q] = jnp.concatenate(blocks[2 * q : 2 * q + 2], axis=1)
    quarters = [[quarter_ref[2 * h + c] for c in range(2)] for h in range(2)]
    mine = quarter_ref[2 * where_ref[0] + where_ref[1]]
    quarter_out[...] = mine.astype(BF16)
    section_body(quarters, rest[0:4], *rest[4:7], rest[7:9], own_ref, far_ref, pad_ref)


def relay_section_kernel(where_ref, a_ref, b_ref, c_ref, d_ref, *refs):
    *rest, own_ref, far_ref, pad_ref = refs
    half = where_ref[0] == 0
    core = where_ref[1] == 0
    a, b, c, d = [r[...].astype(F32) for r in (a_ref, b_ref, c_ref, d_ref)]
    own0, own1 = jnp.where(half, a, c), jnp.where(half, c, a)
    far0, far1 = jnp.where(half, b, d), jnp.where(half, d, b)
    quarters = [
        [jnp.where(core, own0, far0), jnp.where(core, far0, own0)],
        [jnp.where(core, own1, far1), jnp.where(core, far1, own1)],
    ]
    section_body(quarters, rest[0:4], *rest[4:7], rest[7:9], own_ref, far_ref, pad_ref)


def exit_pack_kernel(where_ref, mine_ref, m0_ref, m1_ref, m2_ref, m3_ref, send_ref):
    branch = (m0_ref[...].astype(F32) + m1_ref[...].astype(F32)) + (m2_ref[...].astype(F32) + m3_ref[...].astype(F32))
    branch = branch.astype(BF16).astype(F32)
    final = (mine_ref[...].astype(F32) + 0.5 * branch).astype(BF16).astype(F32)
    squares = final * final
    squares = jnp.sum(squares[:, :128] + squares[:, 128:], axis=1, keepdims=True)
    squares = jnp.broadcast_to(squares, (T, 128))
    zpos = where_ref[2]
    own = jnp.where(zpos < 2, final[:, :128], final[:, 128:])
    own = jnp.where(zpos % 2 == 0, own, pltpu.roll(own, 64, 1))
    turned = {d: own if d == 0 else pltpu.roll(own, (32 * d) % 128, 1) for d in (-1, 0, 1, 2, 3)}
    lane = lanes((6, 128))
    group = lane // 32
    spot = lane % 32 == lax.broadcasted_iota(jnp.int32, (6, 128), 0)
    for x in range(4):
        rows = [slice(x * 24 + k * 6, x * 24 + k * 6 + 6) for k in range(4)]
        total = squares[rows[0]]
        for k in range(1, 4):
            total = jnp.where(group == k, squares[rows[k]], total)
        total = jnp.sum(jnp.where(spot, total, 0.0), axis=0, keepdims=True)
        parts = split3(total)
        for m in range(2):
            block = turned[-m][rows[0]]
            for k in range(1, 4):
                block = jnp.where(group == k, turned[k - m][rows[k]], block)
            message = jnp.concatenate([block, parts[0], parts[1]], axis=0).astype(BF16)
            for peer in range(4):
                send_ref[(x * 2 + m) * 4 + peer] = message


def exit_unpack_kernel(where_ref, recv_ref, out_ref):
    lane = lanes((8, 128))
    spot = lane % 32 == lax.broadcasted_iota(jnp.int32, (8, 128), 0)
    same_group = (
        lax.broadcasted_iota(jnp.int32, (128, 128), 0) // 32 == lanes((128, 128)) // 32
    ).astype(F32).astype(BF16)
    for m in range(2):
        first = (6 + m) * 4
        sums = [recv_ref[first + i].astype(F32) for i in range(4)]
        total = (sums[0][6:7] + sums[0][7:8]) + (sums[1][6:7] + sums[1][7:8])
        total = total + ((sums[2][6:7] + sums[2][7:8]) + (sums[3][6:7] + sums[3][7:8]))
        spread = jnp.where(spot, jnp.broadcast_to(total, (8, 128)), 0.0)
        parts = [p.astype(BF16) for p in split3(spread)]
        total = (nn_dot(parts[0], same_group) + nn_dot(parts[1], same_group)) + nn_dot(parts[2], same_group)
        block = recv_ref[first + 2 * where_ref[0] + where_ref[1]].astype(F32)
        block = block * lax.rsqrt(total * (1.0 / D) + EPS)
        rows = [block if k == 0 else pltpu.roll(block, 128 - 32 * k, 1) for k in range(4)]
        out_ref[m] = jnp.concatenate([r[:6, :32] for r in rows], axis=0).astype(BF16)


SMEM_SPEC = pl.BlockSpec(memory_space=pltpu.SMEM)
VMEM_SPEC = pl.BlockSpec(memory_space=pltpu.VMEM)


def call_kernel(kernel, out_shape, count, scratch=()):
    return pl.pallas_call(
        kernel,
        out_shape=out_shape,
        in_specs=[SMEM_SPEC] + [VMEM_SPEC] * count,
        out_specs=[VMEM_SPEC] * len(out_shape),
        scratch_shapes=scratch,
        compiler_params=pltpu.CompilerParams(vmem_limit_bytes=24 * 1024 * 1024),
    )


def flip(v, axes, bits):
    size = lax.axis_size(axes)
    return lax.ppermute(v, axes, [(i, i ^ bits) for i in range(size)])


def swap_pairs(first, size):
    pairs = []
    for low in range(first % 2, size, 2):
        high = (low + 1) % size
        pairs += [(low, high), (high, low)]
    return pairs


def per_device(
    micro_in,
    norm_gain,
    proj_gate,
    proj_value,
    proj_write,
    proj_read,
    proj_step,
    step_bias,
    decay_log,
    skip_gain,
    conv_value,
    conv_write,
    conv_read,
    proj_out,
):
    sections = lax.axis_size("pp")
    half = lax.axis_index("yh")
    core = lax.axis_index("tc")
    zpos = lax.axis_index("tz")
    where = jnp.stack([half, core, zpos, lax.axis_index("ym")]).astype(jnp.int32)

    shape = jax.ShapeDtypeStruct
    raw = (
        micro_in,
        proj_gate[0, :, 0, 0, :].T,
        proj_value[0, :, 0, 0, :].T,
        proj_step[0, :, :, 0, 0].T,
        proj_out[0, 0, 0],
        conv_value.reshape(5, 1, 64),
        step_bias.reshape(1, 2),
        decay_log.reshape(1, 2),
        skip_gain.reshape(1, 1),
        norm_gain,
    )
    order = (1, 2, 4, 3, 5, 6, 7, 8, 9, 0)
    near, away, same, other, gain = pl.pallas_call(
        pack_kernel,
        out_shape=[
            shape((T // 4, 32), BF16),
            shape((T // 4, 32), BF16),
            shape((ROWS, D), BF16),
            shape((ROWS, D), BF16),
            shape((1, D), F32),
        ],
        in_specs=[SMEM_SPEC] + [pl.BlockSpec(memory_space=pltpu.HBM)] * len(raw),
        out_specs=[VMEM_SPEC] * 5,
        scratch_shapes=[pltpu.VMEM(raw[i].shape, raw[i].dtype) for i in order]
        + [pltpu.SemaphoreType.DMA((len(raw),))],
        compiler_params=pltpu.CompilerParams(vmem_limit_bytes=24 * 1024 * 1024),
    )(where, *[pltpu.with_memory_space_constraint(v, pltpu.HBM) if i in (0, 1, 2, 3, 4, 5, 9) else v for i, v in enumerate(raw)])
    r1 = flip(near, FS, 1)
    r2 = flip(away, FS, 2)
    r3 = flip(away, FS, 3)
    w1 = flip(other, FS, 1)
    w2 = flip(same, FS, 2)
    w3 = flip(other, FS, 3)
    (send,) = call_kernel(block_kernel, [shape((32, T // 4, 128), BF16)], 4)(where, near, r1, r2, r3)
    recv = lax.all_to_all(send, BLOCKS, 0, 0)

    taps_w = conv_write.reshape(5, 1, 128)
    taps_r = conv_read.reshape(5, 1, 128)
    params = (same, w1, w2, w3, proj_write[0, :, 0, :], proj_read[0, :, 0, :], gain, taps_w, taps_r)
    quarter = shape((T, 256), BF16)
    outs = [shape((T, 256), F32), quarter]
    pad = pltpu.VMEM((T + 16, 768), F32)
    mine, own, far = call_kernel(
        entry_section_kernel, [quarter, *outs], 10, [pad, pltpu.VMEM((4, T, 256), F32)]
    )(where, recv, *params)
    for s in range(sections):
        got = flip(far, "tc", 1)
        mixed = (own + got.astype(F32)).astype(BF16)
        others = [flip(mixed, "tz", d) for d in (1, 2, 3)]
        if s + 1 == sections:
            break
        r1, r2, r3 = [v.astype(F32) for v in others]
        branch = ((mixed.astype(F32) + r1) + (r2 + r3)).astype(BF16).astype(F32)
        produced = (mine.astype(F32) + 0.5 * branch).astype(BF16)
        hop = swap_pairs(s, sections)
        hop_flip = [(2 * i + h, 2 * j + 1 - h) for i, j in hop for h in range(2)]
        a = lax.ppermute(produced, "pp", hop)
        c = lax.ppermute(produced, ("pp", "yh"), hop_flip)
        b = flip(a, "tc", 1)
        d = flip(c, "tc", 1)
        mine = a
        own, far = call_kernel(relay_section_kernel, outs, 13, [pad])(where, a, b, c, d, *params)

    (send,) = call_kernel(exit_pack_kernel, [shape((32, 8, 128), BF16)], 5)(where, mine, mixed, *others)
    recv = lax.all_to_all(send, ("pp", "ym", "yh", "tc"), 0, 0)
    (result,) = call_kernel(exit_unpack_kernel, [shape((2, T // sections, 32), BF16)], 1)(where, recv)
    return result


def solution(mesh):
    split = Mesh(
        mesh.devices.reshape(mesh.shape["pp"], 2, 2, 4, 2), ("pp", "ym", "yh", "tz", "tc")
    )
    in_specs = (
        P(None, "pp", TP + FS),
        P("pp", None),
        P("pp", None, TP, FS, None),
        P("pp", None, TP, FS, None),
        P("pp", None, TP, None),
        P("pp", None, TP, None),
        P("pp", None, None, TP, FS),
        P("pp", None, TP, FS),
        P("pp", None, TP, FS),
        P("pp", TP, FS),
        P("pp", None, TP, FS, None),
        P("pp", None, TP, None),
        P("pp", None, TP, None),
        P("pp", TP, FS, None, None),
    )
    out_specs = P(None, "pp", TP + FS)
    return jax.shard_map(
        per_device, mesh=split, in_specs=in_specs, out_specs=out_specs, check_vma=False
    )
```

profile of v0, /device:TPU:1, one launch (start us, length us, event | category | flops | bytes accessed | tf_op | source)
XLA Modules:
  0.0 127.0 jit_solution(469098187136073409)
XLA Ops:
  0.7 0.7 copy-done.4
  1.4 2.0 %shard_map.136 = (bf16[24,32]{1,0:T(8,128)(2,1)S(1)}, bf16[24,32]{1,0:T(8,128)(2,1)S(1)}, bf16[168,1024]{1,0:T(8,128)(2,1)S(1)}, bf16[168,1024]{1,0:T(8,128)(2,1)S(1)}, f32[1,1024]{1,0:T(1,128)S(1)}) custom-call(s32[4]{0:T(128)S(1)} %pad_add_fusion.where_ref, bf16[2,24,32]{2,1,0:T(8,128)(2,1)} %micro_hbm.1, bf16[64,1024]{1,0:T(8,128)(2,1)} %bitcast.41, ...), custom_call_target="tpu_custom_call" | custom-call | tf_op jit(solution)/shard_map/pallas_call | solution.py:386
  3.4 3.6 %collective-permute-start.5 = (bf16[168,1024]{1,0:T(8,128)(2,1)S(1)}, bf16[168,1024]{1,0:T(8,128)(2,1)S(1)}, u32[]{:S(2)}, u32[]{:S(2)}) collective-permute-start(bf16[168,1024]{1,0:T(8,128)(2,1)S(1)} %get-tuple-element.22), channel_id=1, source_target_pairs={{0,24},{8,16},{16,8},{24,0},{1,25},{9,17},{17,9},{25,1},{2,26},{10... | collective-permute-start | bytes 1032200 | tf_op jit(solution)/shard_map/ppermute | solution.py:339
  7.1 1.3 %collective-permute-start.4 = (bf16[168,1024]{1,0:T(8,128)(2,1)S(1)}, bf16[168,1024]{1,0:T(8,128)(2,1)S(1)}, u32[]{:S(2)}, u32[]{:S(2)}) collective-permute-start(bf16[168,1024]{1,0:T(8,128)(2,1)S(1)} %get-tuple-element.21.refs_0_), channel_id=1, source_target_pairs={{0,16},{8,24},{16,0},{24,8},{1,17},{9,25},{17,1},{25,9},{2,18},{10... | collective-permute-start | bytes 1032200 | tf_op jit(solution)/shard_map/ppermute | solution.py:339
  8.6 2.4 %collective-permute-start.2 = (bf16[24,32]{1,0:T(8,128)(2,1)S(1)}, bf16[24,32]{1,0:T(8,128)(2,1)S(1)}, u32[]{:S(2)}, u32[]{:S(2)}) collective-permute-start(bf16[24,32]{1,0:T(8,128)(2,1)S(1)} %get-tuple-element.20), channel_id=1, source_target_pairs={{0,24},{8,16},{16,8},{24,0},{1,25},{9,17},{17,9},{25,1},{2,26},{10... | collective-permute-start | bytes 4616 | tf_op jit(solution)/shard_map/ppermute | solution.py:339
  10.9 12.3 %collective-permute-done.r1_ref = bf16[24,32]{1,0:T(8,128)(2,1)S(1)} collective-permute-done((bf16[24,32]{1,0:T(8,128)(2,1)S(1)}, bf16[24,32]{1,0:T(8,128)(2,1)S(1)}, u32[]{:S(2)}, u32[]{:S(2)}) %collective-permute-start) | collective-permute-done | bytes 1568 | tf_op jit(solution)/shard_map/ppermute | solution.py:339
  23.3 0.3 collective-permute-start.1
  23.6 3.6 %collective-permute-done.1.r2_ref = bf16[24,32]{1,0:T(8,128)(2,1)S(1)} collective-permute-done((bf16[24,32]{1,0:T(8,128)(2,1)S(1)}, bf16[24,32]{1,0:T(8,128)(2,1)S(1)}, u32[]{:S(2)}, u32[]{:S(2)}) %collective-permute-start.1) | collective-permute-done | bytes 1568 | tf_op jit(solution)/shard_map/ppermute | solution.py:339
  27.2 0.6 shard_map.137
  27.9 19.0 %all_to_all.10.recv_ref = bf16[32,24,128]{2,1,0:T(8,128)(2,1)S(1)} all-to-all(bf16[32,24,128]{2,1,0:T(8,128)(2,1)S(1)} %shard_map.137), channel_id=1, replica_groups=mesh['pp'=4,'ym'=2,'yh'=2,'tz'=4,'tc'=2] {'pp','tz','tc'}, dimensions={0} | all-to-all | bytes 393216 | tf_op jit(solution)/shard_map/all_to_all | solution.py:408
  46.9 0.6 copy-done.2
  47.6 2.3 %shard_map.138 = (bf16[96,256]{1,0:T(8,128)(2,1)S(1)}, f32[96,256]{1,0:T(8,128)S(1)}, bf16[96,256]{1,0:T(8,128)(2,1)S(1)}) custom-call(s32[4]{0:T(128)S(1)} %pad_add_fusion.where_ref, bf16[32,24,128]{2,1,0:T(8,128)(2,1)S(1)} %all_to_all.10.recv_ref, bf16[168,1024]{1,0:T(8,128)(2,1)S(1)} %get-tuple-element.21.refs_0_, ...), custom_call_target="tpu_custom_call" | custom-call | tf_op jit(solution)/shard_map/pallas_call | solution.py:416
  49.9 0.4 collective-permute-start.6
  50.3 0.9 collective-permute-done.6
  51.2 1.0 collective-permute-start.9
  52.2 1.1 collective-permute-start.8
  53.3 1.2 collective-permute-start.7
  54.5 0.9 collective-permute-done.9
  55.4 1.3 %collective-permute-done.8 = bf16[96,256]{1,0:T(8,128)(2,1)S(1)} collective-permute-done((bf16[96,256]{1,0:T(8,128)(2,1)S(1)}, bf16[96,256]{1,0:T(8,128)(2,1)S(1)}, u32[]{:S(2)}, u32[]{:S(2)}) %collective-permute-start.8) | collective-permute-done | bytes 49184 | tf_op jit(solution)/shard_map/ppermute | solution.py:339
  56.9 1.2 collective-permute-start.10
  58.0 2.7 %collective-permute-done.12.c_ref = bf16[96,256]{1,0:T(8,128)(2,1)S(1)} collective-permute-done((bf16[96,256]{1,0:T(8,128)(2,1)S(1)}, bf16[96,256]{1,0:T(8,128)(2,1)S(1)}, u32[]{:S(2)}, u32[]{:S(2)}) %collective-permute-start.12) | collective-permute-done | bytes 49184 | tf_op jit(solution)/shard_map/ppermute | solution.py:431
  60.7 2.8 %collective-permute-start.13 = (bf16[96,256]{1,0:T(8,128)(2,1)S(1)}, bf16[96,256]{1,0:T(8,128)(2,1)S(1)}, u32[]{:S(2)}, u32[]{:S(2)}) collective-permute-start(bf16[96,256]{1,0:T(8,128)(2,1)S(1)} %collective-permute-done.12.c_ref), channel_id=1, source_target_pairs={{0,1},{1,0},{2,3},{3,2},{4,5},{5,4},{6,7},{7,6},{8,9},{9,8},{10,11... | collective-permute-start | bytes 147464 | tf_op jit(solution)/shard_map/ppermute | solution.py:339
  63.5 0.9 collective-permute-done.13.d_ref
  64.4 0.4 collective-permute-done.11.b_ref
  64.8 2.2 %shard_map.139 = (f32[96,256]{1,0:T(8,128)S(1)}, bf16[96,256]{1,0:T(8,128)(2,1)S(1)}) custom-call(s32[4]{0:T(128)S(1)} %pad_add_fusion.where_ref, bf16[96,256]{1,0:T(8,128)(2,1)S(1)} %collective-permute-done.10.a_ref, bf16[96,256]{1,0:T(8,128)(2,1)S(1)} %collective-permute-done.11.b_ref, bf16[96,256]{1,0:T(8,128)(2,1)S(1)} %collective-permute-done.12.c_ref, ...), custom_call_target="tpu_custom_call" | custom-call | tf_op jit(solution)/shard_map/pallas_call | solution.py:435
  67.0 0.2 collective-permute-start.14
  67.2 1.1 collective-permute-done.14
  68.3 1.8 %collective-permute-start.17 = (bf16[96,256]{1,0:T(8,128)(2,1)S(1)}, bf16[96,256]{1,0:T(8,128)(2,1)S(1)}, u32[]{:S(2)}, u32[]{:S(2)}) collective-permute-start(bf16[96,256]{1,0:T(8,128)(2,1)S(1)} %add_convert_fusion.6), channel_id=1, source_target_pairs={{0,6},{2,4},{4,2},{6,0},{1,7},{3,5},{5,3},{7,1},{8,14},{10,12},{12... | collective-permute-start | bytes 147464 | tf_op jit(solution)/shard_map/ppermute | solution.py:339
  70.1 1.1 collective-permute-start.16
  71.2 0.4 collective-permute-start.15
  71.6 0.9 collective-permute-done.17
  72.5 2.0 %collective-permute-done.16 = bf16[96,256]{1,0:T(8,128)(2,1)S(1)} collective-permute-done((bf16[96,256]{1,0:T(8,128)(2,1)S(1)}, bf16[96,256]{1,0:T(8,128)(2,1)S(1)}, u32[]{:S(2)}, u32[]{:S(2)}) %collective-permute-start.16) | collective-permute-done | bytes 49184 | tf_op jit(solution)/shard_map/ppermute | solution.py:339
  74.6 1.8 %collective-permute-start.20 = (bf16[96,256]{1,0:T(8,128)(2,1)S(1)}, bf16[96,256]{1,0:T(8,128)(2,1)S(1)}, u32[]{:S(2)}, u32[]{:S(2)}) collective-permute-start(bf16[96,256]{1,0:T(8,128)(2,1)S(1)} %add_convert_fusion.4), channel_id=1, source_target_pairs={{32,72},{40,64},{64,40},{72,32},{96,8},{104,0},{0,104},{8,96},{33,... | collective-permute-start | bytes 147464 | tf_op jit(solution)/shard_map/ppermute | solution.py:431
  76.3 1.6 %collective-permute-start.18 = (bf16[96,256]{1,0:T(8,128)(2,1)S(1)}, bf16[96,256]{1,0:T(8,128)(2,1)S(1)}, u32[]{:S(2)}, u32[]{:S(2)}) collective-permute-start(bf16[96,256]{1,0:T(8,128)(2,1)S(1)} %add_convert_fusion.4), channel_id=1, source_target_pairs={{32,64},{64,32},{96,0},{0,96},{33,65},{65,33},{97,1},{1,97},{34,66... | collective-permute-start | bytes 147464 | tf_op jit(solution)/shard_map/ppermute | solution.py:430
  77.9 1.8 %collective-permute-done.20.c_ref = bf16[96,256]{1,0:T(8,128)(2,1)S(1)} collective-permute-done((bf16[96,256]{1,0:T(8,128)(2,1)S(1)}, bf16[96,256]{1,0:T(8,128)(2,1)S(1)}, u32[]{:S(2)}, u32[]{:S(2)}) %collective-permute-start.20) | collective-permute-done | bytes 49184 | tf_op jit(solution)/shard_map/ppermute | solution.py:431
  79.7 2.9 %collective-permute-start.21 = (bf16[96,256]{1,0:T(8,128)(2,1)S(1)}, bf16[96,256]{1,0:T(8,128)(2,1)S(1)}, u32[]{:S(2)}, u32[]{:S(2)}) collective-permute-start(bf16[96,256]{1,0:T(8,128)(2,1)S(1)} %collective-permute-done.20.c_ref), channel_id=1, source_target_pairs={{0,1},{1,0},{2,3},{3,2},{4,5},{5,4},{6,7},{7,6},{8,9},{9,8},{10,11... | collective-permute-start | bytes 147464 | tf_op jit(solution)/shard_map/ppermute | solution.py:339
  82.6 0.7 collective-permute-start.19
  83.3 0.2 collective-permute-done.21.d_ref
  83.5 0.7 collective-permute-done.19.b_ref
  84.2 2.2 %shard_map.140 = (f32[96,256]{1,0:T(8,128)S(1)}, bf16[96,256]{1,0:T(8,128)(2,1)S(1)}) custom-call(s32[4]{0:T(128)S(1)} %pad_add_fusion.where_ref, bf16[96,256]{1,0:T(8,128)(2,1)S(1)} %collective-permute-done.18.a_ref, bf16[96,256]{1,0:T(8,128)(2,1)S(1)} %collective-permute-done.19.b_ref, bf16[96,256]{1,0:T(8,128)(2,1)S(1)} %collective-permute-done.20.c_ref, ...), custom_call_target="tpu_custom_call" | custom-call | tf_op jit(solution)/shard_map/pallas_call | solution.py:435
  86.3 0.4 collective-permute-start.22
  86.8 0.9 collective-permute-done.22
  87.7 1.5 %collective-permute-start.25 = (bf16[96,256]{1,0:T(8,128)(2,1)S(1)}, bf16[96,256]{1,0:T(8,128)(2,1)S(1)}, u32[]{:S(2)}, u32[]{:S(2)}) collective-permute-start(bf16[96,256]{1,0:T(8,128)(2,1)S(1)} %add_convert_fusion.3), channel_id=1, source_target_pairs={{0,6},{2,4},{4,2},{6,0},{1,7},{3,5},{5,3},{7,1},{8,14},{10,12},{12... | collective-permute-start | bytes 147464 | tf_op jit(solution)/shard_map/ppermute | solution.py:339
  89.2 0.6 collective-permute-start.24
  89.8 1.2 collective-permute-start.23
  91.0 0.9 collective-permute-done.25
  91.9 1.8 %collective-permute-done.24 = bf16[96,256]{1,0:T(8,128)(2,1)S(1)} collective-permute-done((bf16[96,256]{1,0:T(8,128)(2,1)S(1)}, bf16[96,256]{1,0:T(8,128)(2,1)S(1)}, u32[]{:S(2)}, u32[]{:S(2)}) %collective-permute-start.24) | collective-permute-done | bytes 49184 | tf_op jit(solution)/shard_map/ppermute | solution.py:339
  93.7 0.3 collective-permute-start.28
  94.0 1.7 %collective-permute-start.26 = (bf16[96,256]{1,0:T(8,128)(2,1)S(1)}, bf16[96,256]{1,0:T(8,128)(2,1)S(1)}, u32[]{:S(2)}, u32[]{:S(2)}) collective-permute-start(bf16[96,256]{1,0:T(8,128)(2,1)S(1)} %add_convert_fusion.1), channel_id=1, source_target_pairs={{0,32},{32,0},{64,96},{96,64},{1,33},{33,1},{65,97},{97,65},{2,34}... | collective-permute-start | bytes 147464 | tf_op jit(solution)/shard_map/ppermute | solution.py:430
  95.7 2.1 %collective-permute-done.28.c_ref = bf16[96,256]{1,0:T(8,128)(2,1)S(1)} collective-permute-done((bf16[96,256]{1,0:T(8,128)(2,1)S(1)}, bf16[96,256]{1,0:T(8,128)(2,1)S(1)}, u32[]{:S(2)}, u32[]{:S(2)}) %collective-permute-start.28) | collective-permute-done | bytes 49184 | tf_op jit(solution)/shard_map/ppermute | solution.py:431
  97.8 2.9 %collective-permute-start.29 = (bf16[96,256]{1,0:T(8,128)(2,1)S(1)}, bf16[96,256]{1,0:T(8,128)(2,1)S(1)}, u32[]{:S(2)}, u32[]{:S(2)}) collective-permute-start(bf16[96,256]{1,0:T(8,128)(2,1)S(1)} %collective-permute-done.28.c_ref), channel_id=1, source_target_pairs={{0,1},{1,0},{2,3},{3,2},{4,5},{5,4},{6,7},{7,6},{8,9},{9,8},{10,11... | collective-permute-start | bytes 147464 | tf_op jit(solution)/shard_map/ppermute | solution.py:339
  100.7 0.9 collective-permute-done.29.d_ref
  101.6 0.4 collective-permute-done.27.b_ref
  102.0 2.2 %shard_map.141 = (f32[96,256]{1,0:T(8,128)S(1)}, bf16[96,256]{1,0:T(8,128)(2,1)S(1)}) custom-call(s32[4]{0:T(128)S(1)} %pad_add_fusion.where_ref, bf16[96,256]{1,0:T(8,128)(2,1)S(1)} %collective-permute-done.26.a_ref.mine_ref, bf16[96,256]{1,0:T(8,128)(2,1)S(1)} %collective-permute-done.27.b_ref, bf16[96,256]{1,0:T(8,128)(2,1)S(1)} %collective-permute-done.28.c_ref, ...), custom_call_target="tpu_custom_call" | custom-call | tf_op jit(solution)/shard_map/pallas_call | solution.py:435
  104.2 0.2 collective-permute-start.30
  104.4 1.1 collective-permute-done.30
  105.5 1.3 %collective-permute-start.33 = (bf16[96,256]{1,0:T(8,128)(2,1)S(1)}, bf16[96,256]{1,0:T(8,128)(2,1)S(1)}, u32[]{:S(2)}, u32[]{:S(2)}) collective-permute-start(bf16[96,256]{1,0:T(8,128)(2,1)S(1)} %add_convert_fusion.m0_ref), channel_id=1, source_target_pairs={{0,6},{2,4},{4,2},{6,0},{1,7},{3,5},{5,3},{7,1},{8,14},{10,12},{12... | collective-permute-start | bytes 147464 | tf_op jit(solution)/shard_map/ppermute | solution.py:339
  106.8 1.1 collective-permute-start.32
  107.9 0.9 collective-permute-start.31
  108.8 0.9 collective-permute-done.33.m3_ref
  109.7 1.5 %collective-permute-done.32.m2_ref = bf16[96,256]{1,0:T(8,128)(2,1)S(1)} collective-permute-done((bf16[96,256]{1,0:T(8,128)(2,1)S(1)}, bf16[96,256]{1,0:T(8,128)(2,1)S(1)}, u32[]{:S(2)}, u32[]{:S(2)}) %collective-permute-start.32) | collective-permute-done | bytes 49184 | tf_op jit(solution)/shard_map/ppermute | solution.py:339
  111.2 0.7 shard_map.142
  112.0 13.6 %all_to_all.11.recv_ref = bf16[32,8,128]{2,1,0:T(8,128)(2,1)S(1)} all-to-all(bf16[32,8,128]{2,1,0:T(8,128)(2,1)S(1)} %shard_map.142), channel_id=1, replica_groups=mesh['pp'=4,'ym'=2,'yh'=2,'tz'=4,'tc'=2] {'pp','ym','yh','tc'}, dimensions={0} | all-to-all | bytes 131072 | tf_op jit(solution)/shard_map/all_to_all | solution.py:438
  125.6 1.4 %shard_map.143 = bf16[2,24,32]{2,1,0:T(8,128)(2,1)} custom-call(s32[4]{0:T(128)S(1)} %pad_add_fusion.where_ref, bf16[32,8,128]{2,1,0:T(8,128)(2,1)S(1)} %all_to_all.11.recv_ref), custom_call_target="tpu_custom_call" | custom-call | tf_op jit(solution)/shard_map/pallas_call | solution.py:439
  (34 shorter events, 0.6 us)
Async XLA Ops:
  0.7 0.7 copy-start.4
  0.7 0.7 copy-start.5
  3.4 43.4 %collective-permute-start.5 = (bf16[168,1024]{1,0:T(8,128)(2,1)S(1)}, bf16[168,1024]{1,0:T(8,128)(2,1)S(1)}, u32[]{:S(2)}, u32[]{:S(2)}) collective-permute-start(bf16[168,1024]{1,0:T(8,128)(2,1)S(1)} %get-tuple-element.22), channel_id=1, source_target_pairs={{0,24},{8,16},{16,8},{24,0},{1,25},{9,17},{17,9},{25,1},{2,26},{10... | collective-permute-start | bytes 1032200 | tf_op jit(solution)/shard_map/ppermute | solution.py:339
  7.1 39.8 %collective-permute-start.3 = (bf16[168,1024]{1,0:T(8,128)(2,1)S(1)}, bf16[168,1024]{1,0:T(8,128)(2,1)S(1)}, u32[]{:S(2)}, u32[]{:S(2)}) collective-permute-start(bf16[168,1024]{1,0:T(8,128)(2,1)S(1)} %get-tuple-element.22), channel_id=1, source_target_pairs={{0,8},{8,0},{16,24},{24,16},{1,9},{9,1},{17,25},{25,17},{2,10},{10... | collective-permute-start | bytes 1032200 | tf_op jit(solution)/shard_map/ppermute | solution.py:339
  7.1 39.8 %collective-permute-start.4 = (bf16[168,1024]{1,0:T(8,128)(2,1)S(1)}, bf16[168,1024]{1,0:T(8,128)(2,1)S(1)}, u32[]{:S(2)}, u32[]{:S(2)}) collective-permute-start(bf16[168,1024]{1,0:T(8,128)(2,1)S(1)} %get-tuple-element.21.refs_0_), channel_id=1, source_target_pairs={{0,16},{8,24},{16,0},{24,8},{1,17},{9,25},{17,1},{25,9},{2,18},{10... | collective-permute-start | bytes 1032200 | tf_op jit(solution)/shard_map/ppermute | solution.py:339
  8.4 14.9 %collective-permute-start = (bf16[24,32]{1,0:T(8,128)(2,1)S(1)}, bf16[24,32]{1,0:T(8,128)(2,1)S(1)}, u32[]{:S(2)}, u32[]{:S(2)}) collective-permute-start(bf16[24,32]{1,0:T(8,128)(2,1)S(1)} %get-tuple-element.19.r0_ref), channel_id=1, source_target_pairs={{0,8},{8,0},{16,24},{24,16},{1,9},{9,1},{17,25},{25,17},{2,10},{10... | collective-permute-start | bytes 4616 | tf_op jit(solution)/shard_map/ppermute | solution.py:339
  8.5 38.4 %copy-start = (bf16[1,1024,1,128]{3,1,2,0:T(8,128)(2,1)S(1)}, bf16[1,1024,1,128]{3,1,2,0:T(8,128)(2,1)}, u32[]{:S(2)}) copy-start(bf16[1,1024,1,128]{3,1,2,0:T(8,128)(2,1)} %param.18) | copy-start | bytes 786436
  8.6 38.4 %copy-start.1 = (bf16[1,1024,1,128]{3,1,2,0:T(8,128)(2,1)S(1)}, bf16[1,1024,1,128]{3,1,2,0:T(8,128)(2,1)}, u32[]{:S(2)}) copy-start(bf16[1,1024,1,128]{3,1,2,0:T(8,128)(2,1)} %param.19) | copy-start | bytes 786436
  8.6 15.1 %collective-permute-start.2 = (bf16[24,32]{1,0:T(8,128)(2,1)S(1)}, bf16[24,32]{1,0:T(8,128)(2,1)S(1)}, u32[]{:S(2)}, u32[]{:S(2)}) collective-permute-start(bf16[24,32]{1,0:T(8,128)(2,1)S(1)} %get-tuple-element.20), channel_id=1, source_target_pairs={{0,24},{8,16},{16,8},{24,0},{1,25},{9,17},{17,9},{25,1},{2,26},{10... | collective-permute-start | bytes 4616 | tf_op jit(solution)/shard_map/ppermute | solution.py:339
  23.3 4.0 %collective-permute-start.1 = (bf16[24,32]{1,0:T(8,128)(2,1)S(1)}, bf16[24,32]{1,0:T(8,128)(2,1)S(1)}, u32[]{:S(2)}, u32[]{:S(2)}) collective-permute-start(bf16[24,32]{1,0:T(8,128)(2,1)S(1)} %get-tuple-element.20), channel_id=1, source_target_pairs={{0,16},{8,24},{16,0},{24,8},{1,17},{9,25},{17,1},{25,9},{2,18},{10... | collective-permute-start | bytes 4616 | tf_op jit(solution)/shard_map/ppermute | solution.py:339
  46.9 0.7 copy-start.2
  46.9 0.7 copy-start.3
  49.9 1.3 %collective-permute-start.6 = (bf16[96,256]{1,0:T(8,128)(2,1)S(1)}, bf16[96,256]{1,0:T(8,128)(2,1)S(1)}, u32[]{:S(2)}, u32[]{:S(2)}) collective-permute-start(bf16[96,256]{1,0:T(8,128)(2,1)S(1)} %get-tuple-element.26), channel_id=1, source_target_pairs={{0,1},{1,0},{2,3},{3,2},{4,5},{5,4},{6,7},{7,6},{8,9},{9,8},{10,11... | collective-permute-start | bytes 147464 | tf_op jit(solution)/shard_map/ppermute | solution.py:339
  51.2 4.2 %collective-permute-start.9 = (bf16[96,256]{1,0:T(8,128)(2,1)S(1)}, bf16[96,256]{1,0:T(8,128)(2,1)S(1)}, u32[]{:S(2)}, u32[]{:S(2)}) collective-permute-start(bf16[96,256]{1,0:T(8,128)(2,1)S(1)} %add_convert_fusion.9), channel_id=1, source_target_pairs={{0,6},{2,4},{4,2},{6,0},{1,7},{3,5},{5,3},{7,1},{8,14},{10,12},{12... | collective-permute-start | bytes 147464 | tf_op jit(solution)/shard_map/ppermute | solution.py:339
  52.2 4.5 %collective-permute-start.8 = (bf16[96,256]{1,0:T(8,128)(2,1)S(1)}, bf16[96,256]{1,0:T(8,128)(2,1)S(1)}, u32[]{:S(2)}, u32[]{:S(2)}) collective-permute-start(bf16[96,256]{1,0:T(8,128)(2,1)S(1)} %add_convert_fusion.9), channel_id=1, source_target_pairs={{0,4},{2,6},{4,0},{6,2},{1,5},{3,7},{5,1},{7,3},{8,12},{10,14},{12... | collective-permute-start | bytes 147464 | tf_op jit(solution)/shard_map/ppermute | solution.py:339
  53.3 3.4 %collective-permute-start.7 = (bf16[96,256]{1,0:T(8,128)(2,1)S(1)}, bf16[96,256]{1,0:T(8,128)(2,1)S(1)}, u32[]{:S(2)}, u32[]{:S(2)}) collective-permute-start(bf16[96,256]{1,0:T(8,128)(2,1)S(1)} %add_convert_fusion.9), channel_id=1, source_target_pairs={{0,2},{2,0},{4,6},{6,4},{1,3},{3,1},{5,7},{7,5},{8,10},{10,8},{12,... | collective-permute-start | bytes 147464 | tf_op jit(solution)/shard_map/ppermute | solution.py:339
  56.8 3.9 %collective-permute-start.12 = (bf16[96,256]{1,0:T(8,128)(2,1)S(1)}, bf16[96,256]{1,0:T(8,128)(2,1)S(1)}, u32[]{:S(2)}, u32[]{:S(2)}) collective-permute-start(bf16[96,256]{1,0:T(8,128)(2,1)S(1)} %add_convert_fusion.7), channel_id=1, source_target_pairs={{0,40},{8,32},{32,8},{40,0},{64,104},{72,96},{96,72},{104,64},{1,4... | collective-permute-start | bytes 147464 | tf_op jit(solution)/shard_map/ppermute | solution.py:431
  56.9 6.7 %collective-permute-start.10 = (bf16[96,256]{1,0:T(8,128)(2,1)S(1)}, bf16[96,256]{1,0:T(8,128)(2,1)S(1)}, u32[]{:S(2)}, u32[]{:S(2)}) collective-permute-start(bf16[96,256]{1,0:T(8,128)(2,1)S(1)} %add_convert_fusion.7), channel_id=1, source_target_pairs={{0,32},{32,0},{64,96},{96,64},{1,33},{33,1},{65,97},{97,65},{2,34}... | collective-permute-start | bytes 147464 | tf_op jit(solution)/shard_map/ppermute | solution.py:430
  60.7 3.7 %collective-permute-start.13 = (bf16[96,256]{1,0:T(8,128)(2,1)S(1)}, bf16[96,256]{1,0:T(8,128)(2,1)S(1)}, u32[]{:S(2)}, u32[]{:S(2)}) collective-permute-start(bf16[96,256]{1,0:T(8,128)(2,1)S(1)} %collective-permute-done.12.c_ref), channel_id=1, source_target_pairs={{0,1},{1,0},{2,3},{3,2},{4,5},{5,4},{6,7},{7,6},{8,9},{9,8},{10,11... | collective-permute-start | bytes 147464 | tf_op jit(solution)/shard_map/ppermute | solution.py:339
  63.5 1.2 collective-permute-start.11
  67.0 1.3 %collective-permute-start.14 = (bf16[96,256]{1,0:T(8,128)(2,1)S(1)}, bf16[96,256]{1,0:T(8,128)(2,1)S(1)}, u32[]{:S(2)}, u32[]{:S(2)}) collective-permute-start(bf16[96,256]{1,0:T(8,128)(2,1)S(1)} %get-tuple-element.28), channel_id=1, source_target_pairs={{0,1},{1,0},{2,3},{3,2},{4,5},{5,4},{6,7},{7,6},{8,9},{9,8},{10,11... | collective-permute-start | bytes 147464 | tf_op jit(solution)/shard_map/ppermute | solution.py:339
  68.3 4.2 %collective-permute-start.17 = (bf16[96,256]{1,0:T(8,128)(2,1)S(1)}, bf16[96,256]{1,0:T(8,128)(2,1)S(1)}, u32[]{:S(2)}, u32[]{:S(2)}) collective-permute-start(bf16[96,256]{1,0:T(8,128)(2,1)S(1)} %add_convert_fusion.6), channel_id=1, source_target_pairs={{0,6},{2,4},{4,2},{6,0},{1,7},{3,5},{5,3},{7,1},{8,14},{10,12},{12... | collective-permute-start | bytes 147464 | tf_op jit(solution)/shard_map/ppermute | solution.py:339
  70.1 4.4 %collective-permute-start.16 = (bf16[96,256]{1,0:T(8,128)(2,1)S(1)}, bf16[96,256]{1,0:T(8,128)(2,1)S(1)}, u32[]{:S(2)}, u32[]{:S(2)}) collective-permute-start(bf16[96,256]{1,0:T(8,128)(2,1)S(1)} %add_convert_fusion.6), channel_id=1, source_target_pairs={{0,4},{2,6},{4,0},{6,2},{1,5},{3,7},{5,1},{7,3},{8,12},{10,14},{12... | collective-permute-start | bytes 147464 | tf_op jit(solution)/shard_map/ppermute | solution.py:339
  71.2 3.3 %collective-permute-start.15 = (bf16[96,256]{1,0:T(8,128)(2,1)S(1)}, bf16[96,256]{1,0:T(8,128)(2,1)S(1)}, u32[]{:S(2)}, u32[]{:S(2)}) collective-permute-start(bf16[96,256]{1,0:T(8,128)(2,1)S(1)} %add_convert_fusion.6), channel_id=1, source_target_pairs={{0,2},{2,0},{4,6},{6,4},{1,3},{3,1},{5,7},{7,5},{8,10},{10,8},{12,... | collective-permute-start | bytes 147464 | tf_op jit(solution)/shard_map/ppermute | solution.py:339
  74.6 5.1 %collective-permute-start.20 = (bf16[96,256]{1,0:T(8,128)(2,1)S(1)}, bf16[96,256]{1,0:T(8,128)(2,1)S(1)}, u32[]{:S(2)}, u32[]{:S(2)}) collective-permute-start(bf16[96,256]{1,0:T(8,128)(2,1)S(1)} %add_convert_fusion.4), channel_id=1, source_target_pairs={{32,72},{40,64},{64,40},{72,32},{96,8},{104,0},{0,104},{8,96},{33,... | collective-permute-start | bytes 147464 | tf_op jit(solution)/shard_map/ppermute | solution.py:431
  76.3 6.3 %collective-permute-start.18 = (bf16[96,256]{1,0:T(8,128)(2,1)S(1)}, bf16[96,256]{1,0:T(8,128)(2,1)S(1)}, u32[]{:S(2)}, u32[]{:S(2)}) collective-permute-start(bf16[96,256]{1,0:T(8,128)(2,1)S(1)} %add_convert_fusion.4), channel_id=1, source_target_pairs={{32,64},{64,32},{96,0},{0,96},{33,65},{65,33},{97,1},{1,97},{34,66... | collective-permute-start | bytes 147464 | tf_op jit(solution)/shard_map/ppermute | solution.py:430
  79.7 3.8 %collective-permute-start.21 = (bf16[96,256]{1,0:T(8,128)(2,1)S(1)}, bf16[96,256]{1,0:T(8,128)(2,1)S(1)}, u32[]{:S(2)}, u32[]{:S(2)}) collective-permute-start(bf16[96,256]{1,0:T(8,128)(2,1)S(1)} %collective-permute-done.20.c_ref), channel_id=1, source_target_pairs={{0,1},{1,0},{2,3},{3,2},{4,5},{5,4},{6,7},{7,6},{8,9},{9,8},{10,11... | collective-permute-start | bytes 147464 | tf_op jit(solution)/shard_map/ppermute | solution.py:339
  82.6 1.5 %collective-permute-start.19 = (bf16[96,256]{1,0:T(8,128)(2,1)S(1)}, bf16[96,256]{1,0:T(8,128)(2,1)S(1)}, u32[]{:S(2)}, u32[]{:S(2)}) collective-permute-start(bf16[96,256]{1,0:T(8,128)(2,1)S(1)} %collective-permute-done.18.a_ref), channel_id=1, source_target_pairs={{0,1},{1,0},{2,3},{3,2},{4,5},{5,4},{6,7},{7,6},{8,9},{9,8},{10,11... | collective-permute-start | bytes 147464 | tf_op jit(solution)/shard_map/ppermute | solution.py:339
  86.3 1.3 %collective-permute-start.22 = (bf16[96,256]{1,0:T(8,128)(2,1)S(1)}, bf16[96,256]{1,0:T(8,128)(2,1)S(1)}, u32[]{:S(2)}, u32[]{:S(2)}) collective-permute-start(bf16[96,256]{1,0:T(8,128)(2,1)S(1)} %get-tuple-element.30), channel_id=1, source_target_pairs={{0,1},{1,0},{2,3},{3,2},{4,5},{5,4},{6,7},{7,6},{8,9},{9,8},{10,11... | collective-permute-start | bytes 147464 | tf_op jit(solution)/shard_map/ppermute | solution.py:339
  87.7 4.2 %collective-permute-start.25 = (bf16[96,256]{1,0:T(8,128)(2,1)S(1)}, bf16[96,256]{1,0:T(8,128)(2,1)S(1)}, u32[]{:S(2)}, u32[]{:S(2)}) collective-permute-start(bf16[96,256]{1,0:T(8,128)(2,1)S(1)} %add_convert_fusion.3), channel_id=1, source_target_pairs={{0,6},{2,4},{4,2},{6,0},{1,7},{3,5},{5,3},{7,1},{8,14},{10,12},{12... | collective-permute-start | bytes 147464 | tf_op jit(solution)/shard_map/ppermute | solution.py:339
  89.2 4.4 %collective-permute-start.24 = (bf16[96,256]{1,0:T(8,128)(2,1)S(1)}, bf16[96,256]{1,0:T(8,128)(2,1)S(1)}, u32[]{:S(2)}, u32[]{:S(2)}) collective-permute-start(bf16[96,256]{1,0:T(8,128)(2,1)S(1)} %add_convert_fusion.3), channel_id=1, source_target_pairs={{0,4},{2,6},{4,0},{6,2},{1,5},{3,7},{5,1},{7,3},{8,12},{10,14},{12... | collective-permute-start | bytes 147464 | tf_op jit(solution)/shard_map/ppermute | solution.py:339
  89.8 3.8 %collective-permute-start.23 = (bf16[96,256]{1,0:T(8,128)(2,1)S(1)}, bf16[96,256]{1,0:T(8,128)(2,1)S(1)}, u32[]{:S(2)}, u32[]{:S(2)}) collective-permute-start(bf16[96,256]{1,0:T(8,128)(2,1)S(1)} %add_convert_fusion.3), channel_id=1, source_target_pairs={{0,2},{2,0},{4,6},{6,4},{1,3},{3,1},{5,7},{7,5},{8,10},{10,8},{12,... | collective-permute-start | bytes 147464 | tf_op jit(solution)/shard_map/ppermute | solution.py:339
  93.7 4.1 %collective-permute-start.28 = (bf16[96,256]{1,0:T(8,128)(2,1)S(1)}, bf16[96,256]{1,0:T(8,128)(2,1)S(1)}, u32[]{:S(2)}, u32[]{:S(2)}) collective-permute-start(bf16[96,256]{1,0:T(8,128)(2,1)S(1)} %add_convert_fusion.1), channel_id=1, source_target_pairs={{0,40},{8,32},{32,8},{40,0},{64,104},{72,96},{96,72},{104,64},{1,4... | collective-permute-start | bytes 147464 | tf_op jit(solution)/shard_map/ppermute | solution.py:431
  94.0 6.8 %collective-permute-start.26 = (bf16[96,256]{1,0:T(8,128)(2,1)S(1)}, bf16[96,256]{1,0:T(8,128)(2,1)S(1)}, u32[]{:S(2)}, u32[]{:S(2)}) collective-permute-start(bf16[96,256]{1,0:T(8,128)(2,1)S(1)} %add_convert_fusion.1), channel_id=1, source_target_pairs={{0,32},{32,0},{64,96},{96,64},{1,33},{33,1},{65,97},{97,65},{2,34}... | collective-permute-start | bytes 147464 | tf_op jit(solution)/shard_map/ppermute | solution.py:430
  97.8 3.8 %collective-permute-start.29 = (bf16[96,256]{1,0:T(8,128)(2,1)S(1)}, bf16[96,256]{1,0:T(8,128)(2,1)S(1)}, u32[]{:S(2)}, u32[]{:S(2)}) collective-permute-start(bf16[96,256]{1,0:T(8,128)(2,1)S(1)} %collective-permute-done.28.c_ref), channel_id=1, source_target_pairs={{0,1},{1,0},{2,3},{3,2},{4,5},{5,4},{6,7},{7,6},{8,9},{9,8},{10,11... | collective-permute-start | bytes 147464 | tf_op jit(solution)/shard_map/ppermute | solution.py:339
  100.7 1.2 collective-permute-start.27
  104.2 1.3 %collective-permute-start.30 = (bf16[96,256]{1,0:T(8,128)(2,1)S(1)}, bf16[96,256]{1,0:T(8,128)(2,1)S(1)}, u32[]{:S(2)}, u32[]{:S(2)}) collective-permute-start(bf16[96,256]{1,0:T(8,128)(2,1)S(1)} %get-tuple-element.32), channel_id=1, source_target_pairs={{0,1},{1,0},{2,3},{3,2},{4,5},{5,4},{6,7},{7,6},{8,9},{9,8},{10,11... | collective-permute-start | bytes 147464 | tf_op jit(solution)/shard_map/ppermute | solution.py:339
  105.5 4.2 %collective-permute-start.33 = (bf16[96,256]{1,0:T(8,128)(2,1)S(1)}, bf16[96,256]{1,0:T(8,128)(2,1)S(1)}, u32[]{:S(2)}, u32[]{:S(2)}) collective-permute-start(bf16[96,256]{1,0:T(8,128)(2,1)S(1)} %add_convert_fusion.m0_ref), channel_id=1, source_target_pairs={{0,6},{2,4},{4,2},{6,0},{1,7},{3,5},{5,3},{7,1},{8,14},{10,12},{12... | collective-permute-start | bytes 147464 | tf_op jit(solution)/shard_map/ppermute | solution.py:339
  106.8 4.4 %collective-permute-start.32 = (bf16[96,256]{1,0:T(8,128)(2,1)S(1)}, bf16[96,256]{1,0:T(8,128)(2,1)S(1)}, u32[]{:S(2)}, u32[]{:S(2)}) collective-permute-start(bf16[96,256]{1,0:T(8,128)(2,1)S(1)} %add_convert_fusion.m0_ref), channel_id=1, source_target_pairs={{0,4},{2,6},{4,0},{6,2},{1,5},{3,7},{5,1},{7,3},{8,12},{10,14},{12... | collective-permute-start | bytes 147464 | tf_op jit(solution)/shard_map/ppermute | solution.py:339
  107.9 3.3 %collective-permute-start.31 = (bf16[96,256]{1,0:T(8,128)(2,1)S(1)}, bf16[96,256]{1,0:T(8,128)(2,1)S(1)}, u32[]{:S(2)}, u32[]{:S(2)}) collective-permute-start(bf16[96,256]{1,0:T(8,128)(2,1)S(1)} %add_convert_fusion.m0_ref), channel_id=1, source_target_pairs={{0,2},{2,0},{4,6},{6,4},{1,3},{3,1},{5,7},{7,5},{8,10},{10,8},{12,... | collective-permute-start | bytes 147464 | tf_op jit(solution)/shard_map/ppermute | solution.py:339
where the time goes:
time: 127 us
  waiting for transfers between devices  40 us (31%)
  starting transfers between devices  38.3 us (30%)
  blocking collectives  32.6 us (26%)
  Pallas kernels  13.6 us (11%)
  local copies, waits for them, and re-layouts  1.34 us (1%)
    ppermute x28, waiting for transfers between devices, flip(): return lax.ppermute(v, axes, [(i, i ^ bits) for i in range(size)])  33.4 us
    ppermute x28, starting transfers between devices, flip(): return lax.ppermute(v, axes, [(i, i ^ bits) for i in range(size)])  31.8 us
    all_to_all x1, blocking collectives, per_device(): recv = lax.all_to_all(send, BLOCKS, 0, 0)  19 us
    all_to_all x1, blocking collectives, per_device(): recv = lax.all_to_all(send, ('pp', 'ym', 'yh', 'tc'), 0, 0)  13.6 us
    ppermute x3, waiting for transfers between devices, per_device(): c = lax.ppermute(produced, ('pp', 'yh'), hop_flip)  6.59 us
    pallas_call x3, Pallas kernels, per_device(): call_kernel(relay_section_kernel, outs, 13, [pad])  6.53 us
    ppermute x3, starting transfers between devices, per_device(): a = lax.ppermute(produced, 'pp', hop)  4.43 us
  transfers between devices with their start and end apart: 34, of which 23 were waited for; matrix products, arithmetic and copies ran while one was open for 0% of the time, Pallas kernels for 1%

commit v1 on v0

--- a/solution.py
+++ b/solution.py
@@ -60,11 +60,15 @@
     decay_hbm,
     skip_hbm,
     gain_hbm,
+    taps_w_hbm,
+    taps_r_hbm,
     near_ref,
     away_ref,
     same_ref,
     other_ref,
     gain_out,
+    taps_w_out,
+    taps_r_out,
     *scratch,
 ):
     sources = (
@@ -78,14 +82,16 @@
         skip_hbm,
         gain_hbm,
         micro_hbm,
-    )
-    buffers, sems = scratch[:-1], scratch[-1]
+        taps_w_hbm,
+        taps_r_hbm,
+    )
+    buffers, sems = (*scratch[:-1], taps_w_out, taps_r_out), scratch[-1]
     copies = [pltpu.make_async_copy(s, b, sems.at[i]) for i, (s, b) in enumerate(zip(sources, buffers))]
     for copy in copies:
         copy.start()
     for copy in copies:
         copy.wait()
-    gate_ref, value_ref, out_ref, step_ref, taps_ref, bias_ref, decay_ref, skip_ref, gain_ref, micro_ref = buffers
+    gate_ref, value_ref, out_ref, step_ref, taps_ref, bias_ref, decay_ref, skip_ref, gain_ref, micro_ref = buffers[:10]
     core = where_ref[1] == 0
     half = where_ref[0] == 0
     gate = jnp.concatenate(permuted(gate_ref[...].astype(F32)), axis=1).astype(BF16)
@@ -305,15 +311,17 @@
     same_group = (
         lax.broadcasted_iota(jnp.int32, (128, 128), 0) // 32 == lanes((128, 128)) // 32
     ).astype(F32).astype(BF16)
+    parts = []
     for m in range(2):
         first = (6 + m) * 4
         sums = [recv_ref[first + i].astype(F32) for i in range(4)]
         total = (sums[0][6:7] + sums[0][7:8]) + (sums[1][6:7] + sums[1][7:8])
         total = total + ((sums[2][6:7] + sums[2][7:8]) + (sums[3][6:7] + sums[3][7:8]))
-        spread = jnp.where(spot, jnp.broadcast_to(total, (8, 128)), 0.0)
-        parts = [p.astype(BF16) for p in split3(spread)]
-        total = (nn_dot(parts[0], same_group) + nn_dot(parts[1], same_group)) + nn_dot(parts[2], same_group)
-        block = recv_ref[first + 2 * where_ref[0] + where_ref[1]].astype(F32)
+        parts += split3(jnp.where(spot, jnp.broadcast_to(total, (8, 128)), 0.0))
+    spread = nn_dot(jnp.concatenate(parts, axis=0).astype(BF16), same_group)
+    for m in range(2):
+        total = (spread[24 * m : 24 * m + 8] + spread[24 * m + 8 : 24 * m + 16]) + spread[24 * m + 16 : 24 * m + 24]
+        block = recv_ref[(6 + m) * 4 + 2 * where_ref[0] + where_ref[1]].astype(F32)
         block = block * lax.rsqrt(total * (1.0 / D) + EPS)
         rows = [block if k == 0 else pltpu.roll(block, 128 - 32 * k, 1) for k in range(4)]
         out_ref[m] = jnp.concatenate([r[:6, :32] for r in rows], axis=0).astype(BF16)
@@ -339,11 +347,17 @@
     return lax.ppermute(v, axes, [(i, i ^ bits) for i in range(size)])
 
 
-def swap_pairs(first, size):
+def hop_pairs(first, size, flip_half):
     pairs = []
-    for low in range(first % 2, size, 2):
-        high = (low + 1) % size
-        pairs += [(low, high), (high, low)]
+    for i in range(size):
+        j = i + 1 if (i - first) % 2 == 0 else i - 1
+        for h in range(2):
+            for c in range(2):
+                if 0 <= j < size:
+                    target = (j, 1 - h if flip_half else h, c)
+                else:
+                    target = (i, h, 1 - c)
+                pairs.append((4 * i + 2 * h + c, 4 * target[0] + 2 * target[1] + target[2]))
     return pairs
 
 
@@ -381,9 +395,11 @@
         decay_log.reshape(1, 2),
         skip_gain.reshape(1, 1),
         norm_gain,
+        conv_write.reshape(5, 1, 128),
+        conv_read.reshape(5, 1, 128),
     )
     order = (1, 2, 4, 3, 5, 6, 7, 8, 9, 0)
-    near, away, same, other, gain = pl.pallas_call(
+    near, away, same, other, gain, taps_w, taps_r = pl.pallas_call(
         pack_kernel,
         out_shape=[
             shape((T // 4, 32), BF16),
@@ -391,13 +407,15 @@
             shape((ROWS, D), BF16),
             shape((ROWS, D), BF16),
             shape((1, D), F32),
+            shape((5, 1, 128), F32),
+            shape((5, 1, 128), F32),
         ],
         in_specs=[SMEM_SPEC] + [pl.BlockSpec(memory_space=pltpu.HBM)] * len(raw),
-        out_specs=[VMEM_SPEC] * 5,
+        out_specs=[VMEM_SPEC] * 7,
         scratch_shapes=[pltpu.VMEM(raw[i].shape, raw[i].dtype) for i in order]
         + [pltpu.SemaphoreType.DMA((len(raw),))],
         compiler_params=pltpu.CompilerParams(vmem_limit_bytes=24 * 1024 * 1024),
-    )(where, *[pltpu.with_memory_space_constraint(v, pltpu.HBM) if i in (0, 1, 2, 3, 4, 5, 9) else v for i, v in enumerate(raw)])
+    )(where, *[pltpu.with_memory_space_constraint(v, pltpu.HBM) if i != 8 else v for i, v in enumerate(raw)])
     r1 = flip(near, FS, 1)
     r2 = flip(away, FS, 2)
     r3 = flip(away, FS, 3)
@@ -407,8 +425,6 @@
     (send,) = call_kernel(block_kernel, [shape((32, T // 4, 128), BF16)], 4)(where, near, r1, r2, r3)
     recv = lax.all_to_all(send, BLOCKS, 0, 0)
 
-    taps_w = conv_write.reshape(5, 1, 128)
-    taps_r = conv_read.reshape(5, 1, 128)
     params = (same, w1, w2, w3, proj_write[0, :, 0, :], proj_read[0, :, 0, :], gain, taps_w, taps_r)
     quarter = shape((T, 256), BF16)
     outs = [shape((T, 256), F32), quarter]
@@ -425,10 +441,7 @@
         r1, r2, r3 = [v.astype(F32) for v in others]
         branch = ((mixed.astype(F32) + r1) + (r2 + r3)).astype(BF16).astype(F32)
         produced = (mine.astype(F32) + 0.5 * branch).astype(BF16)
-        hop = swap_pairs(s, sections)
-        hop_flip = [(2 * i + h, 2 * j + 1 - h) for i, j in hop for h in range(2)]
-        a = lax.ppermute(produced, "pp", hop)
-        c = lax.ppermute(produced, ("pp", "yh"), hop_flip)
+        a, c = [lax.ppermute(produced, ("pp", "yh", "tc"), hop_pairs(s, sections, f)) for f in (False, True)]
         b = flip(a, "tc", 1)
         d = flip(c, "tc", 1)
         mine = a

time: 127 us -> 124 us (0.976)
  waiting for transfers between devices: 40 us -> 37.8 us
  local copies, waits for them, and re-layouts: 1.34 us -> 0.01 us
    ppermute x6, starting transfers between devices: 6.54 us -> 8.93 us  [per_device(): lax.ppermute(produced, ('pp', 'yh', 'tc'), hop_pairs(s, sections, f))]
    ppermute x6, waiting for transfers between devices: 6.6 us -> 4.92 us  [per_device(): lax.ppermute(produced, ('pp', 'yh', 'tc'), hop_pairs(s, sections, f))]
    unnamed x12 -> x4, local copies, waits for them, and re-layouts: 1.34 us -> 0.01 us
    ppermute x28, starting transfers between devices: 31.8 us -> 30.5 us  [flip(): return lax.ppermute(v, axes, [(i, i ^ bits) for i in range(size)])]
  transfers between devices with their start and end apart: 34 -> 34, of which waited for: 23 -> 22; matrix products, arithmetic and copies ran while one was open for 0% -> 0% of each run, Pallas kernels for 1% -> 1%
where the time goes in v1:
time: 124 us
  starting transfers between devices  39.4 us (32%)
  waiting for transfers between devices  37.8 us (30%)
  blocking collectives  31.9 us (26%)
  Pallas kernels  13.6 us (11%)
    ppermute x28, waiting for transfers between devices, flip(): return lax.ppermute(v, axes, [(i, i ^ bits) for i in range(size)])  32.9 us
    ppermute x28, starting transfers between devices, flip(): return lax.ppermute(v, axes, [(i, i ^ bits) for i in range(size)])  30.5 us
    all_to_all x1, blocking collectives, per_device(): recv = lax.all_to_all(send, BLOCKS, 0, 0)  19 us
    all_to_all x1, blocking collectives, per_device(): recv = lax.all_to_all(send, ('pp', 'ym', 'yh', 'tc'), 0, 0)  12.9 us
    ppermute x6, starting transfers between devices, per_device(): lax.ppermute(produced, ('pp', 'yh', 'tc'), hop_pairs(s, sections, f))  8.93 us
    pallas_call x3, Pallas kernels, per_device(): call_kernel(relay_section_kernel, outs, 13, [pad])  6.53 us
    ppermute x6, waiting for transfers between devices, per_device(): lax.ppermute(produced, ('pp', 'yh', 'tc'), hop_pairs(s, sections, f))  4.92 us
  transfers between devices with their start and end apart: 34, of which 22 were waited for; matrix products, arithmetic and copies ran while one was open for 0% of the time, Pallas kernels for 1%

profile of v1, /device:TPU:1, one launch (start us, length us, event | category | flops | bytes accessed | tf_op | source)
XLA Modules:
  0.0 123.8 jit_solution(15307111671832827777)
XLA Ops:
  0.7 0.1 pad_add_fusion.where_ref
  0.7 2.1 %shard_map.136 = (bf16[24,32]{1,0:T(8,128)(2,1)S(1)}, bf16[24,32]{1,0:T(8,128)(2,1)S(1)}, bf16[168,1024]{1,0:T(8,128)(2,1)S(1)}, bf16[168,1024]{1,0:T(8,128)(2,1...) custom-call(s32[4]{0:T(128)S(1)} %pad_add_fusion.where_ref, ...), custom_call_target="tpu_custom_call" | custom-call | tf_op jit(solution)/shard_map/pallas_call | solution.py:402
  2.8 3.6 %collective-permute-start.5 = (bf16[168,1024]{1,0:T(8,128)(2,1)S(1)}, bf16[168,1024]{1,0:T(8,128)(2,1)S(1)}, u32[]{:S(2)}, u32[]{:S(2)}) collective-permute-start(bf16[168,1024]{1,0:T(8,128)(2,1)S(1)} %get-tuple-element.24), channel_id=1, source_target_pairs={{0,24},{8,16},{16,8},{24,0},{1,25},{9,17},{17,9},{25,1},{2,26},{10... | collective-permute-start | bytes 1032200 | tf_op jit(solution)/shard_map/ppermute | solution.py:347
  6.4 1.3 %collective-permute-start.4 = (bf16[168,1024]{1,0:T(8,128)(2,1)S(1)}, bf16[168,1024]{1,0:T(8,128)(2,1)S(1)}, u32[]{:S(2)}, u32[]{:S(2)}) collective-permute-start(bf16[168,1024]{1,0:T(8,128)(2,1)S(1)} %get-tuple-element.23.refs_0_), channel_id=1, source_target_pairs={{0,16},{8,24},{16,0},{24,8},{1,17},{9,25},{17,1},{25,9},{2,18},{10... | collective-permute-start | bytes 1032200 | tf_op jit(solution)/shard_map/ppermute | solution.py:347
  7.7 0.2 collective-permute-start
  7.9 2.4 %collective-permute-start.2 = (bf16[24,32]{1,0:T(8,128)(2,1)S(1)}, bf16[24,32]{1,0:T(8,128)(2,1)S(1)}, u32[]{:S(2)}, u32[]{:S(2)}) collective-permute-start(bf16[24,32]{1,0:T(8,128)(2,1)S(1)} %get-tuple-element.22), channel_id=1, source_target_pairs={{0,24},{8,16},{16,8},{24,0},{1,25},{9,17},{17,9},{25,1},{2,26},{10... | collective-permute-start | bytes 4616 | tf_op jit(solution)/shard_map/ppermute | solution.py:347
  10.3 12.3 %collective-permute-done.r1_ref = bf16[24,32]{1,0:T(8,128)(2,1)S(1)} collective-permute-done((bf16[24,32]{1,0:T(8,128)(2,1)S(1)}, bf16[24,32]{1,0:T(8,128)(2,1)S(1)}, u32[]{:S(2)}, u32[]{:S(2)}) %collective-permute-start) | collective-permute-done | bytes 1568 | tf_op jit(solution)/shard_map/ppermute | solution.py:347
  22.6 0.3 collective-permute-start.1
  23.0 3.6 %collective-permute-done.1.r2_ref = bf16[24,32]{1,0:T(8,128)(2,1)S(1)} collective-permute-done((bf16[24,32]{1,0:T(8,128)(2,1)S(1)}, bf16[24,32]{1,0:T(8,128)(2,1)S(1)}, u32[]{:S(2)}, u32[]{:S(2)}) %collective-permute-start.1) | collective-permute-done | bytes 1568 | tf_op jit(solution)/shard_map/ppermute | solution.py:347
  26.6 0.6 shard_map.137
  27.2 19.0 %all_to_all.10.recv_ref = bf16[32,24,128]{2,1,0:T(8,128)(2,1)S(1)} all-to-all(bf16[32,24,128]{2,1,0:T(8,128)(2,1)S(1)} %shard_map.137), channel_id=1, replica_groups=mesh['pp'=4,'ym'=2,'yh'=2,'tz'=4,'tc'=2] {'pp','tz','tc'}, dimensions={0} | all-to-all | bytes 393216 | tf_op jit(solution)/shard_map/all_to_all | solution.py:426
  46.3 2.3 %shard_map.138 = (bf16[96,256]{1,0:T(8,128)(2,1)S(1)}, f32[96,256]{1,0:T(8,128)S(1)}, bf16[96,256]{1,0:T(8,128)(2,1)S(1)}) custom-call(s32[4]{0:T(128)S(1)} %pad_add_fusion.where_ref, bf16[32,24,128]{2,1,0:T(8,128)(2,1)S(1)} %all_to_all.10.recv_ref, bf16[168,1024]{1,0:T(8,128)(2,1)S(1)} %get-tuple-element.23.refs_0_, ...), custom_call_target="tpu_custom_call" | custom-call | tf_op jit(solution)/shard_map/pallas_call | solution.py:432
  48.6 0.4 collective-permute-start.6
  48.9 0.9 collective-permute-done.6
  49.9 1.0 collective-permute-start.9
  50.9 1.1 collective-permute-start.8
  52.0 1.2 collective-permute-start.7
  53.2 0.9 collective-permute-done.9
  54.1 1.3 %collective-permute-done.8 = bf16[96,256]{1,0:T(8,128)(2,1)S(1)} collective-permute-done((bf16[96,256]{1,0:T(8,128)(2,1)S(1)}, bf16[96,256]{1,0:T(8,128)(2,1)S(1)}, u32[]{:S(2)}, u32[]{:S(2)}) %collective-permute-start.8) | collective-permute-done | bytes 49184 | tf_op jit(solution)/shard_map/ppermute | solution.py:347
  55.4 0.1 collective-permute-start.12
  55.5 1.2 collective-permute-start.10
  56.7 2.7 %collective-permute-done.12.c_ref = bf16[96,256]{1,0:T(8,128)(2,1)S(1)} collective-permute-done((bf16[96,256]{1,0:T(8,128)(2,1)S(1)}, bf16[96,256]{1,0:T(8,128)(2,1)S(1)}, u32[]{:S(2)}, u32[]{:S(2)}) %collective-permute-start.12) | collective-permute-done | bytes 49184 | tf_op jit(solution)/shard_map/ppermute | solution.py:444
  59.4 2.8 %collective-permute-start.13 = (bf16[96,256]{1,0:T(8,128)(2,1)S(1)}, bf16[96,256]{1,0:T(8,128)(2,1)S(1)}, u32[]{:S(2)}, u32[]{:S(2)}) collective-permute-start(bf16[96,256]{1,0:T(8,128)(2,1)S(1)} %collective-permute-done.12.c_ref), channel_id=1, source_target_pairs={{0,1},{1,0},{2,3},{3,2},{4,5},{5,4},{6,7},{7,6},{8,9},{9,8},{10,11... | collective-permute-start | bytes 147464 | tf_op jit(solution)/shard_map/ppermute | solution.py:347
  62.2 0.9 collective-permute-done.13.d_ref
  63.1 0.4 collective-permute-done.11.b_ref
  63.4 2.2 %shard_map.139 = (f32[96,256]{1,0:T(8,128)S(1)}, bf16[96,256]{1,0:T(8,128)(2,1)S(1)}) custom-call(s32[4]{0:T(128)S(1)} %pad_add_fusion.where_ref, bf16[96,256]{1,0:T(8,128)(2,1)S(1)} %collective-permute-done.10.a_ref, bf16[96,256]{1,0:T(8,128)(2,1)S(1)} %collective-permute-done.11.b_ref, bf16[96,256]{1,0:T(8,128)(2,1)S(1)} %collective-permute-done.12.c_ref, ...), custom_call_target="tpu_custom_call" | custom-call | tf_op jit(solution)/shard_map/pallas_call | solution.py:448
  65.6 0.2 collective-permute-start.14
  65.9 1.1 collective-permute-done.14
  67.0 1.8 %collective-permute-start.17 = (bf16[96,256]{1,0:T(8,128)(2,1)S(1)}, bf16[96,256]{1,0:T(8,128)(2,1)S(1)}, u32[]{:S(2)}, u32[]{:S(2)}) collective-permute-start(bf16[96,256]{1,0:T(8,128)(2,1)S(1)} %add_convert_fusion.6), channel_id=1, source_target_pairs={{0,6},{2,4},{4,2},{6,0},{1,7},{3,5},{5,3},{7,1},{8,14},{10,12},{12... | collective-permute-start | bytes 147464 | tf_op jit(solution)/shard_map/ppermute | solution.py:347
  68.8 1.1 collective-permute-start.16
  69.9 0.4 collective-permute-start.15
  70.3 0.9 collective-permute-done.17
  71.2 2.0 %collective-permute-done.16 = bf16[96,256]{1,0:T(8,128)(2,1)S(1)} collective-permute-done((bf16[96,256]{1,0:T(8,128)(2,1)S(1)}, bf16[96,256]{1,0:T(8,128)(2,1)S(1)}, u32[]{:S(2)}, u32[]{:S(2)}) %collective-permute-start.16) | collective-permute-done | bytes 49184 | tf_op jit(solution)/shard_map/ppermute | solution.py:347
  73.3 1.8 %collective-permute-start.20 = (bf16[96,256]{1,0:T(8,128)(2,1)S(1)}, bf16[96,256]{1,0:T(8,128)(2,1)S(1)}, u32[]{:S(2)}, u32[]{:S(2)}) collective-permute-start(bf16[96,256]{1,0:T(8,128)(2,1)S(1)} %add_convert_fusion.4), channel_id=1, source_target_pairs={{0,1},{1,0},{8,9},{9,8},{32,72},{33,73},{40,64},{41,65},{64,40},{6... | collective-permute-start | bytes 147464 | tf_op jit(solution)/shard_map/ppermute | solution.py:444
  75.1 0.1 collective-permute-start.18
  75.2 0.8 collective-permute-done.20.c_ref
  76.0 0.3 collective-permute-start.21
  76.3 0.2 collective-permute-start.19
  76.5 0.7 collective-permute-done.21.d_ref
  77.2 0.4 collective-permute-done.19.b_ref
  77.6 2.2 %shard_map.140 = (f32[96,256]{1,0:T(8,128)S(1)}, bf16[96,256]{1,0:T(8,128)(2,1)S(1)}) custom-call(s32[4]{0:T(128)S(1)} %pad_add_fusion.where_ref, bf16[96,256]{1,0:T(8,128)(2,1)S(1)} %collective-permute-done.18.a_ref, bf16[96,256]{1,0:T(8,128)(2,1)S(1)} %collective-permute-done.19.b_ref, bf16[96,256]{1,0:T(8,128)(2,1)S(1)} %collective-permute-done.20.c_ref, ...), custom_call_target="tpu_custom_call" | custom-call | tf_op jit(solution)/shard_map/pallas_call | solution.py:448
  79.7 0.2 collective-permute-start.22
  80.0 1.1 collective-permute-done.22
  81.1 1.2 collective-permute-start.25
  82.3 0.8 collective-permute-start.24
  83.1 1.3 %collective-permute-start.23 = (bf16[96,256]{1,0:T(8,128)(2,1)S(1)}, bf16[96,256]{1,0:T(8,128)(2,1)S(1)}, u32[]{:S(2)}, u32[]{:S(2)}) collective-permute-start(bf16[96,256]{1,0:T(8,128)(2,1)S(1)} %add_convert_fusion.3), channel_id=1, source_target_pairs={{0,2},{2,0},{4,6},{6,4},{1,3},{3,1},{5,7},{7,5},{8,10},{10,8},{12,... | collective-permute-start | bytes 147464 | tf_op jit(solution)/shard_map/ppermute | solution.py:347
  84.4 0.9 collective-permute-done.25
  85.3 1.4 %collective-permute-done.24 = bf16[96,256]{1,0:T(8,128)(2,1)S(1)} collective-permute-done((bf16[96,256]{1,0:T(8,128)(2,1)S(1)}, bf16[96,256]{1,0:T(8,128)(2,1)S(1)}, u32[]{:S(2)}, u32[]{:S(2)}) %collective-permute-start.24) | collective-permute-done | bytes 49184 | tf_op jit(solution)/shard_map/ppermute | solution.py:347
  86.8 5.7 %collective-permute-start.28 = (bf16[96,256]{1,0:T(8,128)(2,1)S(1)}, bf16[96,256]{1,0:T(8,128)(2,1)S(1)}, u32[]{:S(2)}, u32[]{:S(2)}) collective-permute-start(bf16[96,256]{1,0:T(8,128)(2,1)S(1)} %add_convert_fusion.1), channel_id=1, source_target_pairs={{0,40},{1,41},{8,32},{9,33},{32,8},{33,9},{40,0},{41,1},{64,104},{... | collective-permute-start | bytes 147464 | tf_op jit(solution)/shard_map/ppermute | solution.py:444
  92.5 1.5 %collective-permute-done.28.c_ref = bf16[96,256]{1,0:T(8,128)(2,1)S(1)} collective-permute-done((bf16[96,256]{1,0:T(8,128)(2,1)S(1)}, bf16[96,256]{1,0:T(8,128)(2,1)S(1)}, u32[]{:S(2)}, u32[]{:S(2)}) %collective-permute-start.28) | collective-permute-done | bytes 49184 | tf_op jit(solution)/shard_map/ppermute | solution.py:444
  94.0 2.9 %collective-permute-start.29 = (bf16[96,256]{1,0:T(8,128)(2,1)S(1)}, bf16[96,256]{1,0:T(8,128)(2,1)S(1)}, u32[]{:S(2)}, u32[]{:S(2)}) collective-permute-start(bf16[96,256]{1,0:T(8,128)(2,1)S(1)} %collective-permute-done.28.c_ref), channel_id=1, source_target_pairs={{0,1},{1,0},{2,3},{3,2},{4,5},{5,4},{6,7},{7,6},{8,9},{9,8},{10,11... | collective-permute-start | bytes 147464 | tf_op jit(solution)/shard_map/ppermute | solution.py:347
  96.9 1.8 %collective-permute-start.27 = (bf16[96,256]{1,0:T(8,128)(2,1)S(1)}, bf16[96,256]{1,0:T(8,128)(2,1)S(1)}, u32[]{:S(2)}, u32[]{:S(2)}) collective-permute-start(bf16[96,256]{1,0:T(8,128)(2,1)S(1)} %collective-permute-done.26.a_ref.mine_ref), channel_id=1, source_target_pairs={{0,1},{1,0},{2,3},{3,2},{4,5},{5,4},{6,7},{7,6},{8,9},{9,8},{10,11... | collective-permute-start | bytes 147464 | tf_op jit(solution)/shard_map/ppermute | solution.py:347
  98.7 0.9 collective-permute-done.27.b_ref
  99.6 2.2 %shard_map.141 = (f32[96,256]{1,0:T(8,128)S(1)}, bf16[96,256]{1,0:T(8,128)(2,1)S(1)}) custom-call(s32[4]{0:T(128)S(1)} %pad_add_fusion.where_ref, bf16[96,256]{1,0:T(8,128)(2,1)S(1)} %collective-permute-done.26.a_ref.mine_ref, bf16[96,256]{1,0:T(8,128)(2,1)S(1)} %collective-permute-done.27.b_ref, bf16[96,256]{1,0:T(8,128)(2,1)S(1)} %collective-permute-done.28.c_ref, ...), custom_call_target="tpu_custom_call" | custom-call | tf_op jit(solution)/shard_map/pallas_call | solution.py:448
  101.8 0.4 collective-permute-start.30
  102.2 0.9 collective-permute-done.30
  103.1 1.3 %collective-permute-start.33 = (bf16[96,256]{1,0:T(8,128)(2,1)S(1)}, bf16[96,256]{1,0:T(8,128)(2,1)S(1)}, u32[]{:S(2)}, u32[]{:S(2)}) collective-permute-start(bf16[96,256]{1,0:T(8,128)(2,1)S(1)} %add_convert_fusion.m0_ref), channel_id=1, source_target_pairs={{0,6},{2,4},{4,2},{6,0},{1,7},{3,5},{5,3},{7,1},{8,14},{10,12},{12... | collective-permute-start | bytes 147464 | tf_op jit(solution)/shard_map/ppermute | solution.py:347
  104.3 1.0 collective-permute-start.32
  105.3 1.1 collective-permute-start.31
  106.4 0.9 collective-permute-done.33.m3_ref
  107.3 1.5 %collective-permute-done.32.m2_ref = bf16[96,256]{1,0:T(8,128)(2,1)S(1)} collective-permute-done((bf16[96,256]{1,0:T(8,128)(2,1)S(1)}, bf16[96,256]{1,0:T(8,128)(2,1)S(1)}, u32[]{:S(2)}, u32[]{:S(2)}) %collective-permute-start.32) | collective-permute-done | bytes 49184 | tf_op jit(solution)/shard_map/ppermute | solution.py:347
  108.8 0.7 shard_map.142
  109.5 12.9 %all_to_all.11.recv_ref = bf16[32,8,128]{2,1,0:T(8,128)(2,1)S(1)} all-to-all(bf16[32,8,128]{2,1,0:T(8,128)(2,1)S(1)} %shard_map.142), channel_id=1, replica_groups=mesh['pp'=4,'ym'=2,'yh'=2,'tz'=4,'tc'=2] {'pp','ym','yh','tc'}, dimensions={0} | all-to-all | bytes 131072 | tf_op jit(solution)/shard_map/all_to_all | solution.py:451
  122.5 1.4 %shard_map.143 = bf16[2,24,32]{2,1,0:T(8,128)(2,1)} custom-call(s32[4]{0:T(128)S(1)} %pad_add_fusion.where_ref, bf16[32,8,128]{2,1,0:T(8,128)(2,1)S(1)} %all_to_all.11.recv_ref), custom_call_target="tpu_custom_call" | custom-call | tf_op jit(solution)/shard_map/pallas_call | solution.py:452
  (26 shorter events, 0.2 us)
Async XLA Ops:
  2.8 43.4 %collective-permute-start.5 = (bf16[168,1024]{1,0:T(8,128)(2,1)S(1)}, bf16[168,1024]{1,0:T(8,128)(2,1)S(1)}, u32[]{:S(2)}, u32[]{:S(2)}) collective-permute-start(bf16[168,1024]{1,0:T(8,128)(2,1)S(1)} %get-tuple-element.24), channel_id=1, source_target_pairs={{0,24},{8,16},{16,8},{24,0},{1,25},{9,17},{17,9},{25,1},{2,26},{10... | collective-permute-start | bytes 1032200 | tf_op jit(solution)/shard_map/ppermute | solution.py:347
  6.4 39.8 %collective-permute-start.3 = (bf16[168,1024]{1,0:T(8,128)(2,1)S(1)}, bf16[168,1024]{1,0:T(8,128)(2,1)S(1)}, u32[]{:S(2)}, u32[]{:S(2)}) collective-permute-start(bf16[168,1024]{1,0:T(8,128)(2,1)S(1)} %get-tuple-element.24), channel_id=1, source_target_pairs={{0,8},{8,0},{16,24},{24,16},{1,9},{9,1},{17,25},{25,17},{2,10},{10... | collective-permute-start | bytes 1032200 | tf_op jit(solution)/shard_map/ppermute | solution.py:347
  6.4 39.8 %collective-permute-start.4 = (bf16[168,1024]{1,0:T(8,128)(2,1)S(1)}, bf16[168,1024]{1,0:T(8,128)(2,1)S(1)}, u32[]{:S(2)}, u32[]{:S(2)}) collective-permute-start(bf16[168,1024]{1,0:T(8,128)(2,1)S(1)} %get-tuple-element.23.refs_0_), channel_id=1, source_target_pairs={{0,16},{8,24},{16,0},{24,8},{1,17},{9,25},{17,1},{25,9},{2,18},{10... | collective-permute-start | bytes 1032200 | tf_op jit(solution)/shard_map/ppermute | solution.py:347
  7.7 14.9 %collective-permute-start = (bf16[24,32]{1,0:T(8,128)(2,1)S(1)}, bf16[24,32]{1,0:T(8,128)(2,1)S(1)}, u32[]{:S(2)}, u32[]{:S(2)}) collective-permute-start(bf16[24,32]{1,0:T(8,128)(2,1)S(1)} %get-tuple-element.21.r0_ref), channel_id=1, source_target_pairs={{0,8},{8,0},{16,24},{24,16},{1,9},{9,1},{17,25},{25,17},{2,10},{10... | collective-permute-start | bytes 4616 | tf_op jit(solution)/shard_map/ppermute | solution.py:347
  7.9 38.3 %copy-start = (bf16[1,1024,1,128]{3,1,2,0:T(8,128)(2,1)S(1)}, bf16[1,1024,1,128]{3,1,2,0:T(8,128)(2,1)}, u32[]{:S(2)}) copy-start(bf16[1,1024,1,128]{3,1,2,0:T(8,128)(2,1)} %param.18) | copy-start | bytes 786436
  7.9 38.3 %copy-start.1 = (bf16[1,1024,1,128]{3,1,2,0:T(8,128)(2,1)S(1)}, bf16[1,1024,1,128]{3,1,2,0:T(8,128)(2,1)}, u32[]{:S(2)}) copy-start(bf16[1,1024,1,128]{3,1,2,0:T(8,128)(2,1)} %param.19) | copy-start | bytes 786436
  7.9 15.1 %collective-permute-start.2 = (bf16[24,32]{1,0:T(8,128)(2,1)S(1)}, bf16[24,32]{1,0:T(8,128)(2,1)S(1)}, u32[]{:S(2)}, u32[]{:S(2)}) collective-permute-start(bf16[24,32]{1,0:T(8,128)(2,1)S(1)} %get-tuple-element.22), channel_id=1, source_target_pairs={{0,24},{8,16},{16,8},{24,0},{1,25},{9,17},{17,9},{25,1},{2,26},{10... | collective-permute-start | bytes 4616 | tf_op jit(solution)/shard_map/ppermute | solution.py:347
  22.6 4.0 %collective-permute-start.1 = (bf16[24,32]{1,0:T(8,128)(2,1)S(1)}, bf16[24,32]{1,0:T(8,128)(2,1)S(1)}, u32[]{:S(2)}, u32[]{:S(2)}) collective-permute-start(bf16[24,32]{1,0:T(8,128)(2,1)S(1)} %get-tuple-element.22), channel_id=1, source_target_pairs={{0,16},{8,24},{16,0},{24,8},{1,17},{9,25},{17,1},{25,9},{2,18},{10... | collective-permute-start | bytes 4616 | tf_op jit(solution)/shard_map/ppermute | solution.py:347
  48.6 1.3 %collective-permute-start.6 = (bf16[96,256]{1,0:T(8,128)(2,1)S(1)}, bf16[96,256]{1,0:T(8,128)(2,1)S(1)}, u32[]{:S(2)}, u32[]{:S(2)}) collective-permute-start(bf16[96,256]{1,0:T(8,128)(2,1)S(1)} %get-tuple-element.30), channel_id=1, source_target_pairs={{0,1},{1,0},{2,3},{3,2},{4,5},{5,4},{6,7},{7,6},{8,9},{9,8},{10,11... | collective-permute-start | bytes 147464 | tf_op jit(solution)/shard_map/ppermute | solution.py:347
  49.9 4.2 %collective-permute-start.9 = (bf16[96,256]{1,0:T(8,128)(2,1)S(1)}, bf16[96,256]{1,0:T(8,128)(2,1)S(1)}, u32[]{:S(2)}, u32[]{:S(2)}) collective-permute-start(bf16[96,256]{1,0:T(8,128)(2,1)S(1)} %add_convert_fusion.9), channel_id=1, source_target_pairs={{0,6},{2,4},{4,2},{6,0},{1,7},{3,5},{5,3},{7,1},{8,14},{10,12},{12... | collective-permute-start | bytes 147464 | tf_op jit(solution)/shard_map/ppermute | solution.py:347
  50.9 4.5 %collective-permute-start.8 = (bf16[96,256]{1,0:T(8,128)(2,1)S(1)}, bf16[96,256]{1,0:T(8,128)(2,1)S(1)}, u32[]{:S(2)}, u32[]{:S(2)}) collective-permute-start(bf16[96,256]{1,0:T(8,128)(2,1)S(1)} %add_convert_fusion.9), channel_id=1, source_target_pairs={{0,4},{2,6},{4,0},{6,2},{1,5},{3,7},{5,1},{7,3},{8,12},{10,14},{12... | collective-permute-start | bytes 147464 | tf_op jit(solution)/shard_map/ppermute | solution.py:347
  52.0 3.4 %collective-permute-start.7 = (bf16[96,256]{1,0:T(8,128)(2,1)S(1)}, bf16[96,256]{1,0:T(8,128)(2,1)S(1)}, u32[]{:S(2)}, u32[]{:S(2)}) collective-permute-start(bf16[96,256]{1,0:T(8,128)(2,1)S(1)} %add_convert_fusion.9), channel_id=1, source_target_pairs={{0,2},{2,0},{4,6},{6,4},{1,3},{3,1},{5,7},{7,5},{8,10},{10,8},{12,... | collective-permute-start | bytes 147464 | tf_op jit(solution)/shard_map/ppermute | solution.py:347
  55.4 3.9 %collective-permute-start.12 = (bf16[96,256]{1,0:T(8,128)(2,1)S(1)}, bf16[96,256]{1,0:T(8,128)(2,1)S(1)}, u32[]{:S(2)}, u32[]{:S(2)}) collective-permute-start(bf16[96,256]{1,0:T(8,128)(2,1)S(1)} %add_convert_fusion.7), channel_id=1, source_target_pairs={{0,40},{1,41},{8,32},{9,33},{32,8},{33,9},{40,0},{41,1},{64,104},{... | collective-permute-start | bytes 147464 | tf_op jit(solution)/shard_map/ppermute | solution.py:444
  55.5 6.7 %collective-permute-start.10 = (bf16[96,256]{1,0:T(8,128)(2,1)S(1)}, bf16[96,256]{1,0:T(8,128)(2,1)S(1)}, u32[]{:S(2)}, u32[]{:S(2)}) collective-permute-start(bf16[96,256]{1,0:T(8,128)(2,1)S(1)} %add_convert_fusion.7), channel_id=1, source_target_pairs={{0,32},{1,33},{8,40},{9,41},{32,0},{33,1},{40,8},{41,9},{64,96},{6... | collective-permute-start | bytes 147464 | tf_op jit(solution)/shard_map/ppermute | solution.py:444
  59.4 3.7 %collective-permute-start.13 = (bf16[96,256]{1,0:T(8,128)(2,1)S(1)}, bf16[96,256]{1,0:T(8,128)(2,1)S(1)}, u32[]{:S(2)}, u32[]{:S(2)}) collective-permute-start(bf16[96,256]{1,0:T(8,128)(2,1)S(1)} %collective-permute-done.12.c_ref), channel_id=1, source_target_pairs={{0,1},{1,0},{2,3},{3,2},{4,5},{5,4},{6,7},{7,6},{8,9},{9,8},{10,11... | collective-permute-start | bytes 147464 | tf_op jit(solution)/shard_map/ppermute | solution.py:347
  62.2 1.2 collective-permute-start.11
  65.6 1.3 %collective-permute-start.14 = (bf16[96,256]{1,0:T(8,128)(2,1)S(1)}, bf16[96,256]{1,0:T(8,128)(2,1)S(1)}, u32[]{:S(2)}, u32[]{:S(2)}) collective-permute-start(bf16[96,256]{1,0:T(8,128)(2,1)S(1)} %get-tuple-element.32), channel_id=1, source_target_pairs={{0,1},{1,0},{2,3},{3,2},{4,5},{5,4},{6,7},{7,6},{8,9},{9,8},{10,11... | collective-permute-start | bytes 147464 | tf_op jit(solution)/shard_map/ppermute | solution.py:347
  67.0 4.2 %collective-permute-start.17 = (bf16[96,256]{1,0:T(8,128)(2,1)S(1)}, bf16[96,256]{1,0:T(8,128)(2,1)S(1)}, u32[]{:S(2)}, u32[]{:S(2)}) collective-permute-start(bf16[96,256]{1,0:T(8,128)(2,1)S(1)} %add_convert_fusion.6), channel_id=1, source_target_pairs={{0,6},{2,4},{4,2},{6,0},{1,7},{3,5},{5,3},{7,1},{8,14},{10,12},{12... | collective-permute-start | bytes 147464 | tf_op jit(solution)/shard_map/ppermute | solution.py:347
  68.8 4.4 %collective-permute-start.16 = (bf16[96,256]{1,0:T(8,128)(2,1)S(1)}, bf16[96,256]{1,0:T(8,128)(2,1)S(1)}, u32[]{:S(2)}, u32[]{:S(2)}) collective-permute-start(bf16[96,256]{1,0:T(8,128)(2,1)S(1)} %add_convert_fusion.6), channel_id=1, source_target_pairs={{0,4},{2,6},{4,0},{6,2},{1,5},{3,7},{5,1},{7,3},{8,12},{10,14},{12... | collective-permute-start | bytes 147464 | tf_op jit(solution)/shard_map/ppermute | solution.py:347
  69.9 3.3 %collective-permute-start.15 = (bf16[96,256]{1,0:T(8,128)(2,1)S(1)}, bf16[96,256]{1,0:T(8,128)(2,1)S(1)}, u32[]{:S(2)}, u32[]{:S(2)}) collective-permute-start(bf16[96,256]{1,0:T(8,128)(2,1)S(1)} %add_convert_fusion.6), channel_id=1, source_target_pairs={{0,2},{2,0},{4,6},{6,4},{1,3},{3,1},{5,7},{7,5},{8,10},{10,8},{12,... | collective-permute-start | bytes 147464 | tf_op jit(solution)/shard_map/ppermute | solution.py:347
  73.3 2.7 %collective-permute-start.20 = (bf16[96,256]{1,0:T(8,128)(2,1)S(1)}, bf16[96,256]{1,0:T(8,128)(2,1)S(1)}, u32[]{:S(2)}, u32[]{:S(2)}) collective-permute-start(bf16[96,256]{1,0:T(8,128)(2,1)S(1)} %add_convert_fusion.4), channel_id=1, source_target_pairs={{0,1},{1,0},{8,9},{9,8},{32,72},{33,73},{40,64},{41,65},{64,40},{6... | collective-permute-start | bytes 147464 | tf_op jit(solution)/shard_map/ppermute | solution.py:444
  75.1 1.2 collective-permute-start.18
  76.0 1.2 collective-permute-start.21
  76.3 1.2 collective-permute-start.19
  79.7 1.3 %collective-permute-start.22 = (bf16[96,256]{1,0:T(8,128)(2,1)S(1)}, bf16[96,256]{1,0:T(8,128)(2,1)S(1)}, u32[]{:S(2)}, u32[]{:S(2)}) collective-permute-start(bf16[96,256]{1,0:T(8,128)(2,1)S(1)} %get-tuple-element.34), channel_id=1, source_target_pairs={{0,1},{1,0},{2,3},{3,2},{4,5},{5,4},{6,7},{7,6},{8,9},{9,8},{10,11... | collective-permute-start | bytes 147464 | tf_op jit(solution)/shard_map/ppermute | solution.py:347
  81.1 4.2 %collective-permute-start.25 = (bf16[96,256]{1,0:T(8,128)(2,1)S(1)}, bf16[96,256]{1,0:T(8,128)(2,1)S(1)}, u32[]{:S(2)}, u32[]{:S(2)}) collective-permute-start(bf16[96,256]{1,0:T(8,128)(2,1)S(1)} %add_convert_fusion.3), channel_id=1, source_target_pairs={{0,6},{2,4},{4,2},{6,0},{1,7},{3,5},{5,3},{7,1},{8,14},{10,12},{12... | collective-permute-start | bytes 147464 | tf_op jit(solution)/shard_map/ppermute | solution.py:347
  82.3 4.4 %collective-permute-start.24 = (bf16[96,256]{1,0:T(8,128)(2,1)S(1)}, bf16[96,256]{1,0:T(8,128)(2,1)S(1)}, u32[]{:S(2)}, u32[]{:S(2)}) collective-permute-start(bf16[96,256]{1,0:T(8,128)(2,1)S(1)} %add_convert_fusion.3), channel_id=1, source_target_pairs={{0,4},{2,6},{4,0},{6,2},{1,5},{3,7},{5,1},{7,3},{8,12},{10,14},{12... | collective-permute-start | bytes 147464 | tf_op jit(solution)/shard_map/ppermute | solution.py:347
  83.1 3.7 %collective-permute-start.23 = (bf16[96,256]{1,0:T(8,128)(2,1)S(1)}, bf16[96,256]{1,0:T(8,128)(2,1)S(1)}, u32[]{:S(2)}, u32[]{:S(2)}) collective-permute-start(bf16[96,256]{1,0:T(8,128)(2,1)S(1)} %add_convert_fusion.3), channel_id=1, source_target_pairs={{0,2},{2,0},{4,6},{6,4},{1,3},{3,1},{5,7},{7,5},{8,10},{10,8},{12,... | collective-permute-start | bytes 147464 | tf_op jit(solution)/shard_map/ppermute | solution.py:347
  86.8 7.2 %collective-permute-start.28 = (bf16[96,256]{1,0:T(8,128)(2,1)S(1)}, bf16[96,256]{1,0:T(8,128)(2,1)S(1)}, u32[]{:S(2)}, u32[]{:S(2)}) collective-permute-start(bf16[96,256]{1,0:T(8,128)(2,1)S(1)} %add_convert_fusion.1), channel_id=1, source_target_pairs={{0,40},{1,41},{8,32},{9,33},{32,8},{33,9},{40,0},{41,1},{64,104},{... | collective-permute-start | bytes 147464 | tf_op jit(solution)/shard_map/ppermute | solution.py:444
  92.5 4.3 %collective-permute-start.26 = (bf16[96,256]{1,0:T(8,128)(2,1)S(1)}, bf16[96,256]{1,0:T(8,128)(2,1)S(1)}, u32[]{:S(2)}, u32[]{:S(2)}) collective-permute-start(bf16[96,256]{1,0:T(8,128)(2,1)S(1)} %add_convert_fusion.1), channel_id=1, source_target_pairs={{0,32},{1,33},{8,40},{9,41},{32,0},{33,1},{40,8},{41,9},{64,96},{6... | collective-permute-start | bytes 147464 | tf_op jit(solution)/shard_map/ppermute | solution.py:444
  94.0 4.7 %collective-permute-start.29 = (bf16[96,256]{1,0:T(8,128)(2,1)S(1)}, bf16[96,256]{1,0:T(8,128)(2,1)S(1)}, u32[]{:S(2)}, u32[]{:S(2)}) collective-permute-start(bf16[96,256]{1,0:T(8,128)(2,1)S(1)} %collective-permute-done.28.c_ref), channel_id=1, source_target_pairs={{0,1},{1,0},{2,3},{3,2},{4,5},{5,4},{6,7},{7,6},{8,9},{9,8},{10,11... | collective-permute-start | bytes 147464 | tf_op jit(solution)/shard_map/ppermute | solution.py:347
  96.9 2.7 %collective-permute-start.27 = (bf16[96,256]{1,0:T(8,128)(2,1)S(1)}, bf16[96,256]{1,0:T(8,128)(2,1)S(1)}, u32[]{:S(2)}, u32[]{:S(2)}) collective-permute-start(bf16[96,256]{1,0:T(8,128)(2,1)S(1)} %collective-permute-done.26.a_ref.mine_ref), channel_id=1, source_target_pairs={{0,1},{1,0},{2,3},{3,2},{4,5},{5,4},{6,7},{7,6},{8,9},{9,8},{10,11... | collective-permute-start | bytes 147464 | tf_op jit(solution)/shard_map/ppermute | solution.py:347
  101.8 1.3 %collective-permute-start.30 = (bf16[96,256]{1,0:T(8,128)(2,1)S(1)}, bf16[96,256]{1,0:T(8,128)(2,1)S(1)}, u32[]{:S(2)}, u32[]{:S(2)}) collective-permute-start(bf16[96,256]{1,0:T(8,128)(2,1)S(1)} %get-tuple-element.36), channel_id=1, source_target_pairs={{0,1},{1,0},{2,3},{3,2},{4,5},{5,4},{6,7},{7,6},{8,9},{9,8},{10,11... | collective-permute-start | bytes 147464 | tf_op jit(solution)/shard_map/ppermute | solution.py:347
  103.1 4.2 %collective-permute-start.33 = (bf16[96,256]{1,0:T(8,128)(2,1)S(1)}, bf16[96,256]{1,0:T(8,128)(2,1)S(1)}, u32[]{:S(2)}, u32[]{:S(2)}) collective-permute-start(bf16[96,256]{1,0:T(8,128)(2,1)S(1)} %add_convert_fusion.m0_ref), channel_id=1, source_target_pairs={{0,6},{2,4},{4,2},{6,0},{1,7},{3,5},{5,3},{7,1},{8,14},{10,12},{12... | collective-permute-start | bytes 147464 | tf_op jit(solution)/shard_map/ppermute | solution.py:347
  104.3 4.4 %collective-permute-start.32 = (bf16[96,256]{1,0:T(8,128)(2,1)S(1)}, bf16[96,256]{1,0:T(8,128)(2,1)S(1)}, u32[]{:S(2)}, u32[]{:S(2)}) collective-permute-start(bf16[96,256]{1,0:T(8,128)(2,1)S(1)} %add_convert_fusion.m0_ref), channel_id=1, source_target_pairs={{0,4},{2,6},{4,0},{6,2},{1,5},{3,7},{5,1},{7,3},{8,12},{10,14},{12... | collective-permute-start | bytes 147464 | tf_op jit(solution)/shard_map/ppermute | solution.py:347
  105.3 3.5 %collective-permute-start.31 = (bf16[96,256]{1,0:T(8,128)(2,1)S(1)}, bf16[96,256]{1,0:T(8,128)(2,1)S(1)}, u32[]{:S(2)}, u32[]{:S(2)}) collective-permute-start(bf16[96,256]{1,0:T(8,128)(2,1)S(1)} %add_convert_fusion.m0_ref), channel_id=1, source_target_pairs={{0,2},{2,0},{4,6},{6,4},{1,3},{3,1},{5,7},{7,5},{8,10},{10,8},{12,... | collective-permute-start | bytes 147464 | tf_op jit(solution)/shard_map/ppermute | solution.py:347

commit v2 on v1

--- a/solution.py
+++ b/solution.py
@@ -27,6 +27,10 @@
     mid = (v - hi).astype(BF16).astype(F32)
     low = v - hi - mid
     return hi, mid, low
+
+
+def flag(where_ref, row, width=256):
+    return where_ref[row : row + 1, :width] == 0
 
 
 def permuted(v):
@@ -92,8 +96,8 @@
     for copy in copies:
         copy.wait()
     gate_ref, value_ref, out_ref, step_ref, taps_ref, bias_ref, decay_ref, skip_ref, gain_ref, micro_ref = buffers[:10]
-    core = where_ref[1] == 0
-    half = where_ref[0] == 0
+    core = flag(where_ref, 1, 128)
+    half = flag(where_ref, 0, 128)
     gate = jnp.concatenate(permuted(gate_ref[...].astype(F32)), axis=1).astype(BF16)
     value = jnp.concatenate(permuted(value_ref[...].astype(F32)), axis=1).astype(BF16)
     step = jnp.concatenate(permuted(step_ref[...].astype(F32)), axis=1)
@@ -111,20 +115,21 @@
         first, second = out[4 * h : 4 * h + 2], out[4 * h + 2 : 4 * h + 4]
         own = [jnp.where(core, a, b) for a, b in zip(first, second)]
         far = [jnp.where(core, b, a) for a, b in zip(first, second)]
-        halves.append(jnp.concatenate(own + far, axis=1))
-    for ref, pick in ((same_ref, half), (other_ref, jnp.logical_not(half))):
-        part = jnp.where(pick, halves[0], halves[1])
+        halves.append(own + far)
+    for ref, pair in ((same_ref, zip(*halves)), (other_ref, zip(*halves[::-1]))):
+        part = jnp.concatenate([jnp.where(half, a, b) for a, b in pair], axis=1)
         ref[0:64] = gate
         ref[64:128] = value
         ref[128:160] = jnp.concatenate([part[0:32], part[32:64]], axis=1).astype(BF16)
         ref[160:168] = misc
-    first = where_ref[3] == 0
-    near_ref[...] = jnp.where(first, micro_ref[0], micro_ref[1])
-    away_ref[...] = jnp.where(first, micro_ref[1], micro_ref[0])
+    first = flag(where_ref, 4, 32)
+    micro = [micro_ref[m].astype(F32) for m in range(2)]
+    near_ref[...] = jnp.where(first, micro[0], micro[1]).astype(BF16)
+    away_ref[...] = jnp.where(first, micro[1], micro[0]).astype(BF16)
 
 
 def block_kernel(where_ref, r0_ref, r1_ref, r2_ref, r3_ref, send_ref):
-    y = 2 * where_ref[3] + where_ref[0]
+    y = 2 * where_ref[4:5, :128] + where_ref[0:1, :128]
     group = lanes((24, 128)) // 32
     blank = jnp.zeros((24, 96), F32)
     block = jnp.zeros((24, 128), F32)
@@ -132,7 +137,7 @@
         wide = jnp.concatenate([ref[...].astype(F32), blank], axis=1)
         for k in range(4):
             moved = wide if k == 0 else pltpu.roll(wide, 32 * k, 1)
-            block = jnp.where((group == k) & ((y ^ bits) == k), moved, block)
+            block = jnp.where((group == k) & ((y ^ bits) == group), moved, block)
     block = block.astype(BF16)
     for peer in range(32):
         send_ref[peer] = block
@@ -256,15 +261,15 @@
     for q in range(4):
         quarter_ref[q] = jnp.concatenate(blocks[2 * q : 2 * q + 2], axis=1)
     quarters = [[quarter_ref[2 * h + c] for c in range(2)] for h in range(2)]
-    mine = quarter_ref[2 * where_ref[0] + where_ref[1]]
+    half, core = flag(where_ref, 0), flag(where_ref, 1)
+    mine = jnp.where(half, jnp.where(core, *quarters[0]), jnp.where(core, *quarters[1]))
     quarter_out[...] = mine.astype(BF16)
     section_body(quarters, rest[0:4], *rest[4:7], rest[7:9], own_ref, far_ref, pad_ref)
 
 
 def relay_section_kernel(where_ref, a_ref, b_ref, c_ref, d_ref, *refs):
     *rest, own_ref, far_ref, pad_ref = refs
-    half = where_ref[0] == 0
-    core = where_ref[1] == 0
+    half, core = flag(where_ref, 0), flag(where_ref, 1)
     a, b, c, d = [r[...].astype(F32) for r in (a_ref, b_ref, c_ref, d_ref)]
     own0, own1 = jnp.where(half, a, c), jnp.where(half, c, a)
     far0, far1 = jnp.where(half, b, d), jnp.where(half, d, b)
@@ -282,9 +287,8 @@
     squares = final * final
     squares = jnp.sum(squares[:, :128] + squares[:, 128:], axis=1, keepdims=True)
     squares = jnp.broadcast_to(squares, (T, 128))
-    zpos = where_ref[2]
-    own = jnp.where(zpos < 2, final[:, :128], final[:, 128:])
-    own = jnp.where(zpos % 2 == 0, own, pltpu.roll(own, 64, 1))
+    own = jnp.where(flag(where_ref, 2, 128), final[:, :128], final[:, 128:])
+    own = jnp.where(flag(where_ref, 3, 128), own, pltpu.roll(own, 64, 1))
     turned = {d: own if d == 0 else pltpu.roll(own, (32 * d) % 128, 1) for d in (-1, 0, 1, 2, 3)}
     lane = lanes((6, 128))
     group = lane // 32
@@ -306,6 +310,7 @@
 
 
 def exit_unpack_kernel(where_ref, recv_ref, out_ref):
+    half, core = flag(where_ref, 0, 128), flag(where_ref, 1, 128)
     lane = lanes((8, 128))
     spot = lane % 32 == lax.broadcasted_iota(jnp.int32, (8, 128), 0)
     same_group = (
@@ -321,13 +326,13 @@
     spread = nn_dot(jnp.concatenate(parts, axis=0).astype(BF16), same_group)
     for m in range(2):
         total = (spread[24 * m : 24 * m + 8] + spread[24 * m + 8 : 24 * m + 16]) + spread[24 * m + 16 : 24 * m + 24]
-        block = recv_ref[(6 + m) * 4 + 2 * where_ref[0] + where_ref[1]].astype(F32)
+        blocks = [recv_ref[(6 + m) * 4 + i].astype(F32) for i in range(4)]
+        block = jnp.where(half, jnp.where(core, *blocks[:2]), jnp.where(core, *blocks[2:]))
         block = block * lax.rsqrt(total * (1.0 / D) + EPS)
         rows = [block if k == 0 else pltpu.roll(block, 128 - 32 * k, 1) for k in range(4)]
         out_ref[m] = jnp.concatenate([r[:6, :32] for r in rows], axis=0).astype(BF16)
 
 
-SMEM_SPEC = pl.BlockSpec(memory_space=pltpu.SMEM)
 VMEM_SPEC = pl.BlockSpec(memory_space=pltpu.VMEM)
 
 
@@ -335,7 +340,7 @@
     return pl.pallas_call(
         kernel,
         out_shape=out_shape,
-        in_specs=[SMEM_SPEC] + [VMEM_SPEC] * count,
+        in_specs=[VMEM_SPEC] + [VMEM_SPEC] * count,
         out_specs=[VMEM_SPEC] * len(out_shape),
         scratch_shapes=scratch,
         compiler_params=pltpu.CompilerParams(vmem_limit_bytes=24 * 1024 * 1024),
@@ -379,9 +384,11 @@
 ):
     sections = lax.axis_size("pp")
     half = lax.axis_index("yh")
+    micro = lax.axis_index("ym")
     core = lax.axis_index("tc")
     zpos = lax.axis_index("tz")
-    where = jnp.stack([half, core, zpos, lax.axis_index("ym")]).astype(jnp.int32)
+    where = jnp.stack([half, core, zpos // 2, zpos % 2, micro]).astype(jnp.int32)
+    where = jnp.broadcast_to(where[:, None], (5, 256))
 
     shape = jax.ShapeDtypeStruct
     raw = (
@@ -410,7 +417,7 @@
             shape((5, 1, 128), F32),
             shape((5, 1, 128), F32),
         ],
-        in_specs=[SMEM_SPEC] + [pl.BlockSpec(memory_space=pltpu.HBM)] * len(raw),
+        in_specs=[VMEM_SPEC] + [pl.BlockSpec(memory_space=pltpu.HBM)] * len(raw),
         out_specs=[VMEM_SPEC] * 7,
         scratch_shapes=[pltpu.VMEM(raw[i].shape, raw[i].dtype) for i in order]
         + [pltpu.SemaphoreType.DMA((len(raw),))],

time: 124 us -> 120 us (0.968)
  Pallas kernels: 13.6 us -> 9.38 us
    pallas_call x3, Pallas kernels: 6.53 us -> 4.93 us  [per_device(): call_kernel(relay_section_kernel, outs, 13, [pad])]
  transfers between devices with their start and end apart: 34 -> 34, of which waited for: 22 -> 22; matrix products, arithmetic and copies ran while one was open for 0% -> 0% of each run, Pallas kernels for 1% -> 0%
where the time goes in v2:
time: 120 us
  starting transfers between devices  39.4 us (33%)
  waiting for transfers between devices  37.8 us (31%)
  blocking collectives  31.9 us (27%)
  Pallas kernels  9.38 us (8%)
    ppermute x28, waiting for transfers between devices, flip(): return lax.ppermute(v, axes, [(i, i ^ bits) for i in range(size)])  32.9 us
    ppermute x28, starting transfers between devices, flip(): return lax.ppermute(v, axes, [(i, i ^ bits) for i in range(size)])  30.5 us
    all_to_all x1, blocking collectives, per_device(): recv = lax.all_to_all(send, BLOCKS, 0, 0)  19 us
    all_to_all x1, blocking collectives, per_device(): recv = lax.all_to_all(send, ('pp', 'ym', 'yh', 'tc'), 0, 0)  12.9 us
    ppermute x6, starting transfers between devices, per_device(): lax.ppermute(produced, ('pp', 'yh', 'tc'), hop_pairs(s, sections, f))  8.93 us
    pallas_call x3, Pallas kernels, per_device(): call_kernel(relay_section_kernel, outs, 13, [pad])  4.93 us
    ppermute x6, waiting for transfers between devices, per_device(): lax.ppermute(produced, ('pp', 'yh', 'tc'), hop_pairs(s, sections, f))  4.92 us
  transfers between devices with their start and end apart: 34, of which 22 were waited for; matrix products, arithmetic and copies ran while one was open for 0% of the time, Pallas kernels for 0%

profile of v2, /device:TPU:1, one launch (start us, length us, event | category | flops | bytes accessed | tf_op | source)
XLA Modules:
  0.0 119.7 jit_solution(4035730074952327695)
XLA Ops:
  0.7 0.1 stack.23
  0.8 1.5 %shard_map.136 = (bf16[24,32]{1,0:T(8,128)(2,1)S(1)}, bf16[24,32]{1,0:T(8,128)(2,1)S(1)}, bf16[168,1024]{1,0:T(8,128)(2,1)S(1)}, bf16[168,1024]{1,0:T(8,128)(2,1...) custom-call(s32[5,256]{1,0:T(8,128)S(1)} %broadcast_in_dim.2.where_ref, ...), custom_call_target="tpu_custom_call" | custom-call | tf_op jit(solution)/shard_map/pallas_call | solution.py:409
  2.4 3.6 %collective-permute-start.5 = (bf16[168,1024]{1,0:T(8,128)(2,1)S(1)}, bf16[168,1024]{1,0:T(8,128)(2,1)S(1)}, u32[]{:S(2)}, u32[]{:S(2)}) collective-permute-start(bf16[168,1024]{1,0:T(8,128)(2,1)S(1)} %get-tuple-element.24), channel_id=1, source_target_pairs={{0,24},{8,16},{16,8},{24,0},{1,25},{9,17},{17,9},{25,1},{2,26},{10... | collective-permute-start | bytes 1032200 | tf_op jit(solution)/shard_map/ppermute | solution.py:352
  6.0 1.3 %collective-permute-start.4 = (bf16[168,1024]{1,0:T(8,128)(2,1)S(1)}, bf16[168,1024]{1,0:T(8,128)(2,1)S(1)}, u32[]{:S(2)}, u32[]{:S(2)}) collective-permute-start(bf16[168,1024]{1,0:T(8,128)(2,1)S(1)} %get-tuple-element.23.refs_0_), channel_id=1, source_target_pairs={{0,16},{8,24},{16,0},{24,8},{1,17},{9,25},{17,1},{25,9},{2,18},{10... | collective-permute-start | bytes 1032200 | tf_op jit(solution)/shard_map/ppermute | solution.py:352
  7.3 0.2 collective-permute-start
  7.5 2.4 %collective-permute-start.2 = (bf16[24,32]{1,0:T(8,128)(2,1)S(1)}, bf16[24,32]{1,0:T(8,128)(2,1)S(1)}, u32[]{:S(2)}, u32[]{:S(2)}) collective-permute-start(bf16[24,32]{1,0:T(8,128)(2,1)S(1)} %get-tuple-element.22), channel_id=1, source_target_pairs={{0,24},{8,16},{16,8},{24,0},{1,25},{9,17},{17,9},{25,1},{2,26},{10... | collective-permute-start | bytes 4616 | tf_op jit(solution)/shard_map/ppermute | solution.py:352
  9.9 12.3 %collective-permute-done.r1_ref = bf16[24,32]{1,0:T(8,128)(2,1)S(1)} collective-permute-done((bf16[24,32]{1,0:T(8,128)(2,1)S(1)}, bf16[24,32]{1,0:T(8,128)(2,1)S(1)}, u32[]{:S(2)}, u32[]{:S(2)}) %collective-permute-start) | collective-permute-done | bytes 1568 | tf_op jit(solution)/shard_map/ppermute | solution.py:352
  22.2 0.3 collective-permute-start.1
  22.5 3.6 %collective-permute-done.1.r2_ref = bf16[24,32]{1,0:T(8,128)(2,1)S(1)} collective-permute-done((bf16[24,32]{1,0:T(8,128)(2,1)S(1)}, bf16[24,32]{1,0:T(8,128)(2,1)S(1)}, u32[]{:S(2)}, u32[]{:S(2)}) %collective-permute-start.1) | collective-permute-done | bytes 1568 | tf_op jit(solution)/shard_map/ppermute | solution.py:352
  26.1 0.1 shard_map.137
  26.3 19.0 %all_to_all.10.recv_ref = bf16[32,24,128]{2,1,0:T(8,128)(2,1)S(1)} all-to-all(bf16[32,24,128]{2,1,0:T(8,128)(2,1)S(1)} %shard_map.137), channel_id=1, replica_groups=mesh['pp'=4,'ym'=2,'yh'=2,'tz'=4,'tc'=2] {'pp','tz','tc'}, dimensions={0} | all-to-all | bytes 393216 | tf_op jit(solution)/shard_map/all_to_all | solution.py:433
  45.3 1.8 %shard_map.138 = (bf16[96,256]{1,0:T(8,128)(2,1)S(1)}, f32[96,256]{1,0:T(8,128)S(1)}, bf16[96,256]{1,0:T(8,128)(2,1)S(1)}) custom-call(s32[5,256]{1,0:T(8,128)S(1)} %broadcast_in_dim.2.where_ref, bf16[32,24,128]{2,1,0:T(8,128)(2,1)S(1)} %all_to_all.10.recv_ref, bf16[168,1024]{1,0:T(8,128)(2,1)S(1)} %get-tuple-element.23.refs_0_, ...), custom_call_target="tpu_custom_call" | custom-call | tf_op jit(solution)/shard_map/pallas_call | solution.py:439
  47.1 0.4 collective-permute-start.6
  47.4 0.9 collective-permute-done.6
  48.4 1.0 collective-permute-start.9
  49.4 1.1 collective-permute-start.8
  50.5 1.2 %collective-permute-start.7 = (bf16[96,256]{1,0:T(8,128)(2,1)S(1)}, bf16[96,256]{1,0:T(8,128)(2,1)S(1)}, u32[]{:S(2)}, u32[]{:S(2)}) collective-permute-start(bf16[96,256]{1,0:T(8,128)(2,1)S(1)} %add_convert_fusion.9), channel_id=1, source_target_pairs={{0,2},{2,0},{4,6},{6,4},{1,3},{3,1},{5,7},{7,5},{8,10},{10,8},{12,... | collective-permute-start | bytes 147464 | tf_op jit(solution)/shard_map/ppermute | solution.py:352
  51.7 0.9 collective-permute-done.9
  52.6 1.3 %collective-permute-done.8 = bf16[96,256]{1,0:T(8,128)(2,1)S(1)} collective-permute-done((bf16[96,256]{1,0:T(8,128)(2,1)S(1)}, bf16[96,256]{1,0:T(8,128)(2,1)S(1)}, u32[]{:S(2)}, u32[]{:S(2)}) %collective-permute-start.8) | collective-permute-done | bytes 49184 | tf_op jit(solution)/shard_map/ppermute | solution.py:352
  54.0 0.1 collective-permute-start.12
  54.0 1.2 collective-permute-start.10
  55.2 2.7 %collective-permute-done.12.c_ref = bf16[96,256]{1,0:T(8,128)(2,1)S(1)} collective-permute-done((bf16[96,256]{1,0:T(8,128)(2,1)S(1)}, bf16[96,256]{1,0:T(8,128)(2,1)S(1)}, u32[]{:S(2)}, u32[]{:S(2)}) %collective-permute-start.12) | collective-permute-done | bytes 49184 | tf_op jit(solution)/shard_map/ppermute | solution.py:451
  57.9 2.8 %collective-permute-start.13 = (bf16[96,256]{1,0:T(8,128)(2,1)S(1)}, bf16[96,256]{1,0:T(8,128)(2,1)S(1)}, u32[]{:S(2)}, u32[]{:S(2)}) collective-permute-start(bf16[96,256]{1,0:T(8,128)(2,1)S(1)} %collective-permute-done.12.c_ref), channel_id=1, source_target_pairs={{0,1},{1,0},{2,3},{3,2},{4,5},{5,4},{6,7},{7,6},{8,9},{9,8},{10,11... | collective-permute-start | bytes 147464 | tf_op jit(solution)/shard_map/ppermute | solution.py:352
  60.7 0.9 collective-permute-done.13.d_ref
  61.6 0.4 collective-permute-done.11.b_ref
  62.0 1.6 %shard_map.139 = (f32[96,256]{1,0:T(8,128)S(1)}, bf16[96,256]{1,0:T(8,128)(2,1)S(1)}) custom-call(s32[5,256]{1,0:T(8,128)S(1)} %broadcast_in_dim.2.where_ref, bf16[96,256]{1,0:T(8,128)(2,1)S(1)} %collective-permute-done.10.a_ref, bf16[96,256]{1,0:T(8,128)(2,1)S(1)} %collective-permute-done.11.b_ref, bf16[96,256]{1,0:T(8,128)(2,1)S(1)} %collective-permute-done.12.c_ref, ...), custom_call_target="tpu_custom_call" | custom-call | tf_op jit(solution)/shard_map/pallas_call | solution.py:455
  63.6 0.2 collective-permute-start.14
  63.8 1.1 collective-permute-done.14
  64.9 1.8 %collective-permute-start.17 = (bf16[96,256]{1,0:T(8,128)(2,1)S(1)}, bf16[96,256]{1,0:T(8,128)(2,1)S(1)}, u32[]{:S(2)}, u32[]{:S(2)}) collective-permute-start(bf16[96,256]{1,0:T(8,128)(2,1)S(1)} %add_convert_fusion.6), channel_id=1, source_target_pairs={{0,6},{2,4},{4,2},{6,0},{1,7},{3,5},{5,3},{7,1},{8,14},{10,12},{12... | collective-permute-start | bytes 147464 | tf_op jit(solution)/shard_map/ppermute | solution.py:352
  66.7 1.1 collective-permute-start.16
  67.9 0.4 collective-permute-start.15
  68.3 0.9 collective-permute-done.17
  69.2 2.0 %collective-permute-done.16 = bf16[96,256]{1,0:T(8,128)(2,1)S(1)} collective-permute-done((bf16[96,256]{1,0:T(8,128)(2,1)S(1)}, bf16[96,256]{1,0:T(8,128)(2,1)S(1)}, u32[]{:S(2)}, u32[]{:S(2)}) %collective-permute-start.16) | collective-permute-done | bytes 49184 | tf_op jit(solution)/shard_map/ppermute | solution.py:352
  71.2 1.8 %collective-permute-start.20 = (bf16[96,256]{1,0:T(8,128)(2,1)S(1)}, bf16[96,256]{1,0:T(8,128)(2,1)S(1)}, u32[]{:S(2)}, u32[]{:S(2)}) collective-permute-start(bf16[96,256]{1,0:T(8,128)(2,1)S(1)} %add_convert_fusion.4), channel_id=1, source_target_pairs={{0,1},{1,0},{8,9},{9,8},{32,72},{33,73},{40,64},{41,65},{64,40},{6... | collective-permute-start | bytes 147464 | tf_op jit(solution)/shard_map/ppermute | solution.py:451
  73.1 0.1 collective-permute-start.18
  73.2 0.8 collective-permute-done.20.c_ref
  73.9 0.3 collective-permute-start.21
  74.3 0.2 collective-permute-start.19
  74.5 0.7 collective-permute-done.21.d_ref
  75.2 0.4 collective-permute-done.19.b_ref
  75.5 1.6 %shard_map.140 = (f32[96,256]{1,0:T(8,128)S(1)}, bf16[96,256]{1,0:T(8,128)(2,1)S(1)}) custom-call(s32[5,256]{1,0:T(8,128)S(1)} %broadcast_in_dim.2.where_ref, bf16[96,256]{1,0:T(8,128)(2,1)S(1)} %collective-permute-done.18.a_ref, bf16[96,256]{1,0:T(8,128)(2,1)S(1)} %collective-permute-done.19.b_ref, bf16[96,256]{1,0:T(8,128)(2,1)S(1)} %collective-permute-done.20.c_ref, ...), custom_call_target="tpu_custom_call" | custom-call | tf_op jit(solution)/shard_map/pallas_call | solution.py:455
  77.2 0.2 collective-permute-start.22
  77.4 1.1 collective-permute-done.22
  78.5 1.2 %collective-permute-start.25 = (bf16[96,256]{1,0:T(8,128)(2,1)S(1)}, bf16[96,256]{1,0:T(8,128)(2,1)S(1)}, u32[]{:S(2)}, u32[]{:S(2)}) collective-permute-start(bf16[96,256]{1,0:T(8,128)(2,1)S(1)} %add_convert_fusion.3), channel_id=1, source_target_pairs={{0,6},{2,4},{4,2},{6,0},{1,7},{3,5},{5,3},{7,1},{8,14},{10,12},{12... | collective-permute-start | bytes 147464 | tf_op jit(solution)/shard_map/ppermute | solution.py:352
  79.7 0.8 collective-permute-start.24
  80.5 1.3 %collective-permute-start.23 = (bf16[96,256]{1,0:T(8,128)(2,1)S(1)}, bf16[96,256]{1,0:T(8,128)(2,1)S(1)}, u32[]{:S(2)}, u32[]{:S(2)}) collective-permute-start(bf16[96,256]{1,0:T(8,128)(2,1)S(1)} %add_convert_fusion.3), channel_id=1, source_target_pairs={{0,2},{2,0},{4,6},{6,4},{1,3},{3,1},{5,7},{7,5},{8,10},{10,8},{12,... | collective-permute-start | bytes 147464 | tf_op jit(solution)/shard_map/ppermute | solution.py:352
  81.8 0.9 collective-permute-done.25
  82.7 1.4 %collective-permute-done.24 = bf16[96,256]{1,0:T(8,128)(2,1)S(1)} collective-permute-done((bf16[96,256]{1,0:T(8,128)(2,1)S(1)}, bf16[96,256]{1,0:T(8,128)(2,1)S(1)}, u32[]{:S(2)}, u32[]{:S(2)}) %collective-permute-start.24) | collective-permute-done | bytes 49184 | tf_op jit(solution)/shard_map/ppermute | solution.py:352
  84.2 5.7 %collective-permute-start.28 = (bf16[96,256]{1,0:T(8,128)(2,1)S(1)}, bf16[96,256]{1,0:T(8,128)(2,1)S(1)}, u32[]{:S(2)}, u32[]{:S(2)}) collective-permute-start(bf16[96,256]{1,0:T(8,128)(2,1)S(1)} %add_convert_fusion.1), channel_id=1, source_target_pairs={{0,40},{1,41},{8,32},{9,33},{32,8},{33,9},{40,0},{41,1},{64,104},{... | collective-permute-start | bytes 147464 | tf_op jit(solution)/shard_map/ppermute | solution.py:451
  90.0 1.5 %collective-permute-done.28.c_ref = bf16[96,256]{1,0:T(8,128)(2,1)S(1)} collective-permute-done((bf16[96,256]{1,0:T(8,128)(2,1)S(1)}, bf16[96,256]{1,0:T(8,128)(2,1)S(1)}, u32[]{:S(2)}, u32[]{:S(2)}) %collective-permute-start.28) | collective-permute-done | bytes 49184 | tf_op jit(solution)/shard_map/ppermute | solution.py:451
  91.5 2.9 %collective-permute-start.29 = (bf16[96,256]{1,0:T(8,128)(2,1)S(1)}, bf16[96,256]{1,0:T(8,128)(2,1)S(1)}, u32[]{:S(2)}, u32[]{:S(2)}) collective-permute-start(bf16[96,256]{1,0:T(8,128)(2,1)S(1)} %collective-permute-done.28.c_ref), channel_id=1, source_target_pairs={{0,1},{1,0},{2,3},{3,2},{4,5},{5,4},{6,7},{7,6},{8,9},{9,8},{10,11... | collective-permute-start | bytes 147464 | tf_op jit(solution)/shard_map/ppermute | solution.py:352
  94.3 1.8 %collective-permute-start.27 = (bf16[96,256]{1,0:T(8,128)(2,1)S(1)}, bf16[96,256]{1,0:T(8,128)(2,1)S(1)}, u32[]{:S(2)}, u32[]{:S(2)}) collective-permute-start(bf16[96,256]{1,0:T(8,128)(2,1)S(1)} %collective-permute-done.26.a_ref.mine_ref), channel_id=1, source_target_pairs={{0,1},{1,0},{2,3},{3,2},{4,5},{5,4},{6,7},{7,6},{8,9},{9,8},{10,11... | collective-permute-start | bytes 147464 | tf_op jit(solution)/shard_map/ppermute | solution.py:352
  96.1 0.9 collective-permute-done.27.b_ref
  97.0 1.6 %shard_map.141 = (f32[96,256]{1,0:T(8,128)S(1)}, bf16[96,256]{1,0:T(8,128)(2,1)S(1)}) custom-call(s32[5,256]{1,0:T(8,128)S(1)} %broadcast_in_dim.2.where_ref, bf16[96,256]{1,0:T(8,128)(2,1)S(1)} %collective-permute-done.26.a_ref.mine_ref, bf16[96,256]{1,0:T(8,128)(2,1)S(1)} %collective-permute-done.27.b_ref, ...), custom_call_target="tpu_custom_call" | custom-call | tf_op jit(solution)/shard_map/pallas_call | solution.py:455
  98.7 0.4 collective-permute-start.30
  99.1 0.9 collective-permute-done.30
  100.0 1.3 %collective-permute-start.33 = (bf16[96,256]{1,0:T(8,128)(2,1)S(1)}, bf16[96,256]{1,0:T(8,128)(2,1)S(1)}, u32[]{:S(2)}, u32[]{:S(2)}) collective-permute-start(bf16[96,256]{1,0:T(8,128)(2,1)S(1)} %add_convert_fusion.m0_ref), channel_id=1, source_target_pairs={{0,6},{2,4},{4,2},{6,0},{1,7},{3,5},{5,3},{7,1},{8,14},{10,12},{12... | collective-permute-start | bytes 147464 | tf_op jit(solution)/shard_map/ppermute | solution.py:352
  101.3 1.0 collective-permute-start.32
  102.2 1.1 collective-permute-start.31
  103.3 0.9 collective-permute-done.33.m3_ref
  104.2 1.5 %collective-permute-done.32.m2_ref = bf16[96,256]{1,0:T(8,128)(2,1)S(1)} collective-permute-done((bf16[96,256]{1,0:T(8,128)(2,1)S(1)}, bf16[96,256]{1,0:T(8,128)(2,1)S(1)}, u32[]{:S(2)}, u32[]{:S(2)}) %collective-permute-start.32) | collective-permute-done | bytes 49184 | tf_op jit(solution)/shard_map/ppermute | solution.py:352
  105.7 0.2 shard_map.142
  105.9 12.9 %all_to_all.11.recv_ref = bf16[32,8,128]{2,1,0:T(8,128)(2,1)S(1)} all-to-all(bf16[32,8,128]{2,1,0:T(8,128)(2,1)S(1)} %shard_map.142), channel_id=1, replica_groups=mesh['pp'=4,'ym'=2,'yh'=2,'tz'=4,'tc'=2] {'pp','ym','yh','tc'}, dimensions={0} | all-to-all | bytes 131072 | tf_op jit(solution)/shard_map/all_to_all | solution.py:458
  118.8 0.8 shard_map.143
  (27 shorter events, 0.3 us)
Async XLA Ops:
  2.4 42.9 %collective-permute-start.5 = (bf16[168,1024]{1,0:T(8,128)(2,1)S(1)}, bf16[168,1024]{1,0:T(8,128)(2,1)S(1)}, u32[]{:S(2)}, u32[]{:S(2)}) collective-permute-start(bf16[168,1024]{1,0:T(8,128)(2,1)S(1)} %get-tuple-element.24), channel_id=1, source_target_pairs={{0,24},{8,16},{16,8},{24,0},{1,25},{9,17},{17,9},{25,1},{2,26},{10... | collective-permute-start | bytes 1032200 | tf_op jit(solution)/shard_map/ppermute | solution.py:352
  6.0 39.3 %collective-permute-start.3 = (bf16[168,1024]{1,0:T(8,128)(2,1)S(1)}, bf16[168,1024]{1,0:T(8,128)(2,1)S(1)}, u32[]{:S(2)}, u32[]{:S(2)}) collective-permute-start(bf16[168,1024]{1,0:T(8,128)(2,1)S(1)} %get-tuple-element.24), channel_id=1, source_target_pairs={{0,8},{8,0},{16,24},{24,16},{1,9},{9,1},{17,25},{25,17},{2,10},{10... | collective-permute-start | bytes 1032200 | tf_op jit(solution)/shard_map/ppermute | solution.py:352
  6.0 39.3 %collective-permute-start.4 = (bf16[168,1024]{1,0:T(8,128)(2,1)S(1)}, bf16[168,1024]{1,0:T(8,128)(2,1)S(1)}, u32[]{:S(2)}, u32[]{:S(2)}) collective-permute-start(bf16[168,1024]{1,0:T(8,128)(2,1)S(1)} %get-tuple-element.23.refs_0_), channel_id=1, source_target_pairs={{0,16},{8,24},{16,0},{24,8},{1,17},{9,25},{17,1},{25,9},{2,18},{10... | collective-permute-start | bytes 1032200 | tf_op jit(solution)/shard_map/ppermute | solution.py:352
  7.3 14.9 %collective-permute-start = (bf16[24,32]{1,0:T(8,128)(2,1)S(1)}, bf16[24,32]{1,0:T(8,128)(2,1)S(1)}, u32[]{:S(2)}, u32[]{:S(2)}) collective-permute-start(bf16[24,32]{1,0:T(8,128)(2,1)S(1)} %get-tuple-element.21.r0_ref), channel_id=1, source_target_pairs={{0,8},{8,0},{16,24},{24,16},{1,9},{9,1},{17,25},{25,17},{2,10},{10... | collective-permute-start | bytes 4616 | tf_op jit(solution)/shard_map/ppermute | solution.py:352
  7.5 37.8 %copy-start = (bf16[1,1024,1,128]{3,1,2,0:T(8,128)(2,1)S(1)}, bf16[1,1024,1,128]{3,1,2,0:T(8,128)(2,1)}, u32[]{:S(2)}) copy-start(bf16[1,1024,1,128]{3,1,2,0:T(8,128)(2,1)} %param.18) | copy-start | bytes 786436
  7.5 37.8 %copy-start.1 = (bf16[1,1024,1,128]{3,1,2,0:T(8,128)(2,1)S(1)}, bf16[1,1024,1,128]{3,1,2,0:T(8,128)(2,1)}, u32[]{:S(2)}) copy-start(bf16[1,1024,1,128]{3,1,2,0:T(8,128)(2,1)} %param.19) | copy-start | bytes 786436
  7.5 15.1 %collective-permute-start.2 = (bf16[24,32]{1,0:T(8,128)(2,1)S(1)}, bf16[24,32]{1,0:T(8,128)(2,1)S(1)}, u32[]{:S(2)}, u32[]{:S(2)}) collective-permute-start(bf16[24,32]{1,0:T(8,128)(2,1)S(1)} %get-tuple-element.22), channel_id=1, source_target_pairs={{0,24},{8,16},{16,8},{24,0},{1,25},{9,17},{17,9},{25,1},{2,26},{10... | collective-permute-start | bytes 4616 | tf_op jit(solution)/shard_map/ppermute | solution.py:352
  22.2 4.0 %collective-permute-start.1 = (bf16[24,32]{1,0:T(8,128)(2,1)S(1)}, bf16[24,32]{1,0:T(8,128)(2,1)S(1)}, u32[]{:S(2)}, u32[]{:S(2)}) collective-permute-start(bf16[24,32]{1,0:T(8,128)(2,1)S(1)} %get-tuple-element.22), channel_id=1, source_target_pairs={{0,16},{8,24},{16,0},{24,8},{1,17},{9,25},{17,1},{25,9},{2,18},{10... | collective-permute-start | bytes 4616 | tf_op jit(solution)/shard_map/ppermute | solution.py:352
  47.1 1.3 %collective-permute-start.6 = (bf16[96,256]{1,0:T(8,128)(2,1)S(1)}, bf16[96,256]{1,0:T(8,128)(2,1)S(1)}, u32[]{:S(2)}, u32[]{:S(2)}) collective-permute-start(bf16[96,256]{1,0:T(8,128)(2,1)S(1)} %get-tuple-element.30), channel_id=1, source_target_pairs={{0,1},{1,0},{2,3},{3,2},{4,5},{5,4},{6,7},{7,6},{8,9},{9,8},{10,11... | collective-permute-start | bytes 147464 | tf_op jit(solution)/shard_map/ppermute | solution.py:352
  48.4 4.2 %collective-permute-start.9 = (bf16[96,256]{1,0:T(8,128)(2,1)S(1)}, bf16[96,256]{1,0:T(8,128)(2,1)S(1)}, u32[]{:S(2)}, u32[]{:S(2)}) collective-permute-start(bf16[96,256]{1,0:T(8,128)(2,1)S(1)} %add_convert_fusion.9), channel_id=1, source_target_pairs={{0,6},{2,4},{4,2},{6,0},{1,7},{3,5},{5,3},{7,1},{8,14},{10,12},{12... | collective-permute-start | bytes 147464 | tf_op jit(solution)/shard_map/ppermute | solution.py:352
  49.4 4.5 %collective-permute-start.8 = (bf16[96,256]{1,0:T(8,128)(2,1)S(1)}, bf16[96,256]{1,0:T(8,128)(2,1)S(1)}, u32[]{:S(2)}, u32[]{:S(2)}) collective-permute-start(bf16[96,256]{1,0:T(8,128)(2,1)S(1)} %add_convert_fusion.9), channel_id=1, source_target_pairs={{0,4},{2,6},{4,0},{6,2},{1,5},{3,7},{5,1},{7,3},{8,12},{10,14},{12... | collective-permute-start | bytes 147464 | tf_op jit(solution)/shard_map/ppermute | solution.py:352
  50.5 3.4 %collective-permute-start.7 = (bf16[96,256]{1,0:T(8,128)(2,1)S(1)}, bf16[96,256]{1,0:T(8,128)(2,1)S(1)}, u32[]{:S(2)}, u32[]{:S(2)}) collective-permute-start(bf16[96,256]{1,0:T(8,128)(2,1)S(1)} %add_convert_fusion.9), channel_id=1, source_target_pairs={{0,2},{2,0},{4,6},{6,4},{1,3},{3,1},{5,7},{7,5},{8,10},{10,8},{12,... | collective-permute-start | bytes 147464 | tf_op jit(solution)/shard_map/ppermute | solution.py:352
  54.0 3.9 %collective-permute-start.12 = (bf16[96,256]{1,0:T(8,128)(2,1)S(1)}, bf16[96,256]{1,0:T(8,128)(2,1)S(1)}, u32[]{:S(2)}, u32[]{:S(2)}) collective-permute-start(bf16[96,256]{1,0:T(8,128)(2,1)S(1)} %add_convert_fusion.7), channel_id=1, source_target_pairs={{0,40},{1,41},{8,32},{9,33},{32,8},{33,9},{40,0},{41,1},{64,104},{... | collective-permute-start | bytes 147464 | tf_op jit(solution)/shard_map/ppermute | solution.py:451
  54.0 6.7 %collective-permute-start.10 = (bf16[96,256]{1,0:T(8,128)(2,1)S(1)}, bf16[96,256]{1,0:T(8,128)(2,1)S(1)}, u32[]{:S(2)}, u32[]{:S(2)}) collective-permute-start(bf16[96,256]{1,0:T(8,128)(2,1)S(1)} %add_convert_fusion.7), channel_id=1, source_target_pairs={{0,32},{1,33},{8,40},{9,41},{32,0},{33,1},{40,8},{41,9},{64,96},{6... | collective-permute-start | bytes 147464 | tf_op jit(solution)/shard_map/ppermute | solution.py:451
  57.9 3.7 %collective-permute-start.13 = (bf16[96,256]{1,0:T(8,128)(2,1)S(1)}, bf16[96,256]{1,0:T(8,128)(2,1)S(1)}, u32[]{:S(2)}, u32[]{:S(2)}) collective-permute-start(bf16[96,256]{1,0:T(8,128)(2,1)S(1)} %collective-permute-done.12.c_ref), channel_id=1, source_target_pairs={{0,1},{1,0},{2,3},{3,2},{4,5},{5,4},{6,7},{7,6},{8,9},{9,8},{10,11... | collective-permute-start | bytes 147464 | tf_op jit(solution)/shard_map/ppermute | solution.py:352
  60.7 1.2 %collective-permute-start.11 = (bf16[96,256]{1,0:T(8,128)(2,1)S(1)}, bf16[96,256]{1,0:T(8,128)(2,1)S(1)}, u32[]{:S(2)}, u32[]{:S(2)}) collective-permute-start(bf16[96,256]{1,0:T(8,128)(2,1)S(1)} %collective-permute-done.10.a_ref), channel_id=1, source_target_pairs={{0,1},{1,0},{2,3},{3,2},{4,5},{5,4},{6,7},{7,6},{8,9},{9,8},{10,11... | collective-permute-start | bytes 147464 | tf_op jit(solution)/shard_map/ppermute | solution.py:352
  63.6 1.3 %collective-permute-start.14 = (bf16[96,256]{1,0:T(8,128)(2,1)S(1)}, bf16[96,256]{1,0:T(8,128)(2,1)S(1)}, u32[]{:S(2)}, u32[]{:S(2)}) collective-permute-start(bf16[96,256]{1,0:T(8,128)(2,1)S(1)} %get-tuple-element.32), channel_id=1, source_target_pairs={{0,1},{1,0},{2,3},{3,2},{4,5},{5,4},{6,7},{7,6},{8,9},{9,8},{10,11... | collective-permute-start | bytes 147464 | tf_op jit(solution)/shard_map/ppermute | solution.py:352
  64.9 4.2 %collective-permute-start.17 = (bf16[96,256]{1,0:T(8,128)(2,1)S(1)}, bf16[96,256]{1,0:T(8,128)(2,1)S(1)}, u32[]{:S(2)}, u32[]{:S(2)}) collective-permute-start(bf16[96,256]{1,0:T(8,128)(2,1)S(1)} %add_convert_fusion.6), channel_id=1, source_target_pairs={{0,6},{2,4},{4,2},{6,0},{1,7},{3,5},{5,3},{7,1},{8,14},{10,12},{12... | collective-permute-start | bytes 147464 | tf_op jit(solution)/shard_map/ppermute | solution.py:352
  66.7 4.4 %collective-permute-start.16 = (bf16[96,256]{1,0:T(8,128)(2,1)S(1)}, bf16[96,256]{1,0:T(8,128)(2,1)S(1)}, u32[]{:S(2)}, u32[]{:S(2)}) collective-permute-start(bf16[96,256]{1,0:T(8,128)(2,1)S(1)} %add_convert_fusion.6), channel_id=1, source_target_pairs={{0,4},{2,6},{4,0},{6,2},{1,5},{3,7},{5,1},{7,3},{8,12},{10,14},{12... | collective-permute-start | bytes 147464 | tf_op jit(solution)/shard_map/ppermute | solution.py:352
  67.9 3.3 %collective-permute-start.15 = (bf16[96,256]{1,0:T(8,128)(2,1)S(1)}, bf16[96,256]{1,0:T(8,128)(2,1)S(1)}, u32[]{:S(2)}, u32[]{:S(2)}) collective-permute-start(bf16[96,256]{1,0:T(8,128)(2,1)S(1)} %add_convert_fusion.6), channel_id=1, source_target_pairs={{0,2},{2,0},{4,6},{6,4},{1,3},{3,1},{5,7},{7,5},{8,10},{10,8},{12,... | collective-permute-start | bytes 147464 | tf_op jit(solution)/shard_map/ppermute | solution.py:352
  71.2 2.7 %collective-permute-start.20 = (bf16[96,256]{1,0:T(8,128)(2,1)S(1)}, bf16[96,256]{1,0:T(8,128)(2,1)S(1)}, u32[]{:S(2)}, u32[]{:S(2)}) collective-permute-start(bf16[96,256]{1,0:T(8,128)(2,1)S(1)} %add_convert_fusion.4), channel_id=1, source_target_pairs={{0,1},{1,0},{8,9},{9,8},{32,72},{33,73},{40,64},{41,65},{64,40},{6... | collective-permute-start | bytes 147464 | tf_op jit(solution)/shard_map/ppermute | solution.py:451
  73.1 1.2 %collective-permute-start.18 = (bf16[96,256]{1,0:T(8,128)(2,1)S(1)}, bf16[96,256]{1,0:T(8,128)(2,1)S(1)}, u32[]{:S(2)}, u32[]{:S(2)}) collective-permute-start(bf16[96,256]{1,0:T(8,128)(2,1)S(1)} %add_convert_fusion.4), channel_id=1, source_target_pairs={{0,1},{1,0},{8,9},{9,8},{32,64},{33,65},{40,72},{41,73},{64,32},{6... | collective-permute-start | bytes 147464 | tf_op jit(solution)/shard_map/ppermute | solution.py:451
  73.9 1.2 %collective-permute-start.21 = (bf16[96,256]{1,0:T(8,128)(2,1)S(1)}, bf16[96,256]{1,0:T(8,128)(2,1)S(1)}, u32[]{:S(2)}, u32[]{:S(2)}) collective-permute-start(bf16[96,256]{1,0:T(8,128)(2,1)S(1)} %collective-permute-done.20.c_ref), channel_id=1, source_target_pairs={{0,1},{1,0},{2,3},{3,2},{4,5},{5,4},{6,7},{7,6},{8,9},{9,8},{10,11... | collective-permute-start | bytes 147464 | tf_op jit(solution)/shard_map/ppermute | solution.py:352
  74.3 1.2 %collective-permute-start.19 = (bf16[96,256]{1,0:T(8,128)(2,1)S(1)}, bf16[96,256]{1,0:T(8,128)(2,1)S(1)}, u32[]{:S(2)}, u32[]{:S(2)}) collective-permute-start(bf16[96,256]{1,0:T(8,128)(2,1)S(1)} %collective-permute-done.18.a_ref), channel_id=1, source_target_pairs={{0,1},{1,0},{2,3},{3,2},{4,5},{5,4},{6,7},{7,6},{8,9},{9,8},{10,11... | collective-permute-start | bytes 147464 | tf_op jit(solution)/shard_map/ppermute | solution.py:352
  77.2 1.3 %collective-permute-start.22 = (bf16[96,256]{1,0:T(8,128)(2,1)S(1)}, bf16[96,256]{1,0:T(8,128)(2,1)S(1)}, u32[]{:S(2)}, u32[]{:S(2)}) collective-permute-start(bf16[96,256]{1,0:T(8,128)(2,1)S(1)} %get-tuple-element.34), channel_id=1, source_target_pairs={{0,1},{1,0},{2,3},{3,2},{4,5},{5,4},{6,7},{7,6},{8,9},{9,8},{10,11... | collective-permute-start | bytes 147464 | tf_op jit(solution)/shard_map/ppermute | solution.py:352
  78.5 4.2 %collective-permute-start.25 = (bf16[96,256]{1,0:T(8,128)(2,1)S(1)}, bf16[96,256]{1,0:T(8,128)(2,1)S(1)}, u32[]{:S(2)}, u32[]{:S(2)}) collective-permute-start(bf16[96,256]{1,0:T(8,128)(2,1)S(1)} %add_convert_fusion.3), channel_id=1, source_target_pairs={{0,6},{2,4},{4,2},{6,0},{1,7},{3,5},{5,3},{7,1},{8,14},{10,12},{12... | collective-permute-start | bytes 147464 | tf_op jit(solution)/shard_map/ppermute | solution.py:352
  79.7 4.4 %collective-permute-start.24 = (bf16[96,256]{1,0:T(8,128)(2,1)S(1)}, bf16[96,256]{1,0:T(8,128)(2,1)S(1)}, u32[]{:S(2)}, u32[]{:S(2)}) collective-permute-start(bf16[96,256]{1,0:T(8,128)(2,1)S(1)} %add_convert_fusion.3), channel_id=1, source_target_pairs={{0,4},{2,6},{4,0},{6,2},{1,5},{3,7},{5,1},{7,3},{8,12},{10,14},{12... | collective-permute-start | bytes 147464 | tf_op jit(solution)/shard_map/ppermute | solution.py:352
  80.5 3.7 %collective-permute-start.23 = (bf16[96,256]{1,0:T(8,128)(2,1)S(1)}, bf16[96,256]{1,0:T(8,128)(2,1)S(1)}, u32[]{:S(2)}, u32[]{:S(2)}) collective-permute-start(bf16[96,256]{1,0:T(8,128)(2,1)S(1)} %add_convert_fusion.3), channel_id=1, source_target_pairs={{0,2},{2,0},{4,6},{6,4},{1,3},{3,1},{5,7},{7,5},{8,10},{10,8},{12,... | collective-permute-start | bytes 147464 | tf_op jit(solution)/shard_map/ppermute | solution.py:352
  84.2 7.2 %collective-permute-start.28 = (bf16[96,256]{1,0:T(8,128)(2,1)S(1)}, bf16[96,256]{1,0:T(8,128)(2,1)S(1)}, u32[]{:S(2)}, u32[]{:S(2)}) collective-permute-start(bf16[96,256]{1,0:T(8,128)(2,1)S(1)} %add_convert_fusion.1), channel_id=1, source_target_pairs={{0,40},{1,41},{8,32},{9,33},{32,8},{33,9},{40,0},{41,1},{64,104},{... | collective-permute-start | bytes 147464 | tf_op jit(solution)/shard_map/ppermute | solution.py:451
  90.0 4.3 %collective-permute-start.26 = (bf16[96,256]{1,0:T(8,128)(2,1)S(1)}, bf16[96,256]{1,0:T(8,128)(2,1)S(1)}, u32[]{:S(2)}, u32[]{:S(2)}) collective-permute-start(bf16[96,256]{1,0:T(8,128)(2,1)S(1)} %add_convert_fusion.1), channel_id=1, source_target_pairs={{0,32},{1,33},{8,40},{9,41},{32,0},{33,1},{40,8},{41,9},{64,96},{6... | collective-permute-start | bytes 147464 | tf_op jit(solution)/shard_map/ppermute | solution.py:451
  91.5 4.7 %collective-permute-start.29 = (bf16[96,256]{1,0:T(8,128)(2,1)S(1)}, bf16[96,256]{1,0:T(8,128)(2,1)S(1)}, u32[]{:S(2)}, u32[]{:S(2)}) collective-permute-start(bf16[96,256]{1,0:T(8,128)(2,1)S(1)} %collective-permute-done.28.c_ref), channel_id=1, source_target_pairs={{0,1},{1,0},{2,3},{3,2},{4,5},{5,4},{6,7},{7,6},{8,9},{9,8},{10,11... | collective-permute-start | bytes 147464 | tf_op jit(solution)/shard_map/ppermute | solution.py:352
  94.3 2.7 %collective-permute-start.27 = (bf16[96,256]{1,0:T(8,128)(2,1)S(1)}, bf16[96,256]{1,0:T(8,128)(2,1)S(1)}, u32[]{:S(2)}, u32[]{:S(2)}) collective-permute-start(bf16[96,256]{1,0:T(8,128)(2,1)S(1)} %collective-permute-done.26.a_ref.mine_ref), channel_id=1, source_target_pairs={{0,1},{1,0},{2,3},{3,2},{4,5},{5,4},{6,7},{7,6},{8,9},{9,8},{10,11... | collective-permute-start | bytes 147464 | tf_op jit(solution)/shard_map/ppermute | solution.py:352
  98.7 1.3 %collective-permute-start.30 = (bf16[96,256]{1,0:T(8,128)(2,1)S(1)}, bf16[96,256]{1,0:T(8,128)(2,1)S(1)}, u32[]{:S(2)}, u32[]{:S(2)}) collective-permute-start(bf16[96,256]{1,0:T(8,128)(2,1)S(1)} %get-tuple-element.36), channel_id=1, source_target_pairs={{0,1},{1,0},{2,3},{3,2},{4,5},{5,4},{6,7},{7,6},{8,9},{9,8},{10,11... | collective-permute-start | bytes 147464 | tf_op jit(solution)/shard_map/ppermute | solution.py:352
  100.0 4.2 %collective-permute-start.33 = (bf16[96,256]{1,0:T(8,128)(2,1)S(1)}, bf16[96,256]{1,0:T(8,128)(2,1)S(1)}, u32[]{:S(2)}, u32[]{:S(2)}) collective-permute-start(bf16[96,256]{1,0:T(8,128)(2,1)S(1)} %add_convert_fusion.m0_ref), channel_id=1, source_target_pairs={{0,6},{2,4},{4,2},{6,0},{1,7},{3,5},{5,3},{7,1},{8,14},{10,12},{12... | collective-permute-start | bytes 147464 | tf_op jit(solution)/shard_map/ppermute | solution.py:352
  101.3 4.4 %collective-permute-start.32 = (bf16[96,256]{1,0:T(8,128)(2,1)S(1)}, bf16[96,256]{1,0:T(8,128)(2,1)S(1)}, u32[]{:S(2)}, u32[]{:S(2)}) collective-permute-start(bf16[96,256]{1,0:T(8,128)(2,1)S(1)} %add_convert_fusion.m0_ref), channel_id=1, source_target_pairs={{0,4},{2,6},{4,0},{6,2},{1,5},{3,7},{5,1},{7,3},{8,12},{10,14},{12... | collective-permute-start | bytes 147464 | tf_op jit(solution)/shard_map/ppermute | solution.py:352
  102.2 3.5 %collective-permute-start.31 = (bf16[96,256]{1,0:T(8,128)(2,1)S(1)}, bf16[96,256]{1,0:T(8,128)(2,1)S(1)}, u32[]{:S(2)}, u32[]{:S(2)}) collective-permute-start(bf16[96,256]{1,0:T(8,128)(2,1)S(1)} %add_convert_fusion.m0_ref), channel_id=1, source_target_pairs={{0,2},{2,0},{4,6},{6,4},{1,3},{3,1},{5,7},{7,5},{8,10},{10,8},{12,... | collective-permute-start | bytes 147464 | tf_op jit(solution)/shard_map/ppermute | solution.py:352

commit v3 on v2

--- a/solution.py
+++ b/solution.py
@@ -442,13 +442,16 @@
     for s in range(sections):
         got = flip(far, "tc", 1)
         mixed = (own + got.astype(F32)).astype(BF16)
-        others = [flip(mixed, "tz", d) for d in (1, 2, 3)]
+        others = []
+        for d in (1, 2, 3):
+            others.append(flip(mixed, "tz", d))
         if s + 1 == sections:
             break
         r1, r2, r3 = [v.astype(F32) for v in others]
         branch = ((mixed.astype(F32) + r1) + (r2 + r3)).astype(BF16).astype(F32)
         produced = (mine.astype(F32) + 0.5 * branch).astype(BF16)
-        a, c = [lax.ppermute(produced, ("pp", "yh", "tc"), hop_pairs(s, sections, f)) for f in (False, True)]
+        a = lax.ppermute(produced, ("pp", "yh", "tc"), hop_pairs(s, sections, False))
+        c = lax.ppermute(produced, ("pp", "yh", "tc"), hop_pairs(s, sections, True))
         b = flip(a, "tc", 1)
         d = flip(c, "tc", 1)
         mine = a

time: 120 us -> 120 us (level)
  no operation moved by 1% of the time
where the time goes in v3:
time: 120 us
  starting transfers between devices  39.4 us (33%)
  waiting for transfers between devices  37.8 us (31%)
  blocking collectives  31.9 us (27%)
  Pallas kernels  9.38 us (8%)
    ppermute x28, waiting for transfers between devices, flip(): return lax.ppermute(v, axes, [(i, i ^ bits) for i in range(size)])  32.9 us
    ppermute x28, starting transfers between devices, flip(): return lax.ppermute(v, axes, [(i, i ^ bits) for i in range(size)])  30.5 us
    all_to_all x1, blocking collectives, per_device(): recv = lax.all_to_all(send, BLOCKS, 0, 0)  19 us
    all_to_all x1, blocking collectives, per_device(): recv = lax.all_to_all(send, ('pp', 'ym', 'yh', 'tc'), 0, 0)  12.9 us
    ppermute x3, starting transfers between devices, per_device(): c = lax.ppermute(produced, ('pp', 'yh', 'tc'), hop_pairs(s, sections, True))  7.66 us
    pallas_call x3, Pallas kernels, per_device(): call_kernel(relay_section_kernel, outs, 13, [pad])  4.93 us
    ppermute x3, waiting for transfers between devices, per_device(): c = lax.ppermute(produced, ('pp', 'yh', 'tc'), hop_pairs(s, sections, True))  4.92 us
  transfers between devices with their start and end apart: 34, of which 22 were waited for; matrix products, arithmetic and copies ran while one was open for 0% of the time, Pallas kernels for 0%

profile of v3, /device:TPU:1, one launch (start us, length us, event | category | flops | bytes accessed | tf_op | source)
XLA Modules:
  0.0 119.7 jit_solution(4035730074952327695)
XLA Ops:
  0.7 0.1 stack.23
  0.8 1.5 %shard_map.136 = (bf16[24,32]{1,0:T(8,128)(2,1)S(1)}, bf16[24,32]{1,0:T(8,128)(2,1)S(1)}, bf16[168,1024]{1,0:T(8,128)(2,1)S(1)}, bf16[168,1024]{1,0:T(8,128)(2,1...) custom-call(s32[5,256]{1,0:T(8,128)S(1)} %broadcast_in_dim.2.where_ref, ...), custom_call_target="tpu_custom_call" | custom-call | tf_op jit(solution)/shard_map/pallas_call | solution.py:409
  2.4 3.6 %collective-permute-start.5 = (bf16[168,1024]{1,0:T(8,128)(2,1)S(1)}, bf16[168,1024]{1,0:T(8,128)(2,1)S(1)}, u32[]{:S(2)}, u32[]{:S(2)}) collective-permute-start(bf16[168,1024]{1,0:T(8,128)(2,1)S(1)} %get-tuple-element.24), channel_id=1, source_target_pairs={{0,24},{8,16},{16,8},{24,0},{1,25},{9,17},{17,9},{25,1},{2,26},{10... | collective-permute-start | bytes 1032200 | tf_op jit(solution)/shard_map/ppermute | solution.py:352
  6.0 1.3 %collective-permute-start.4 = (bf16[168,1024]{1,0:T(8,128)(2,1)S(1)}, bf16[168,1024]{1,0:T(8,128)(2,1)S(1)}, u32[]{:S(2)}, u32[]{:S(2)}) collective-permute-start(bf16[168,1024]{1,0:T(8,128)(2,1)S(1)} %get-tuple-element.23.refs_0_), channel_id=1, source_target_pairs={{0,16},{8,24},{16,0},{24,8},{1,17},{9,25},{17,1},{25,9},{2,18},{10... | collective-permute-start | bytes 1032200 | tf_op jit(solution)/shard_map/ppermute | solution.py:352
  7.3 0.2 collective-permute-start
  7.5 2.4 %collective-permute-start.2 = (bf16[24,32]{1,0:T(8,128)(2,1)S(1)}, bf16[24,32]{1,0:T(8,128)(2,1)S(1)}, u32[]{:S(2)}, u32[]{:S(2)}) collective-permute-start(bf16[24,32]{1,0:T(8,128)(2,1)S(1)} %get-tuple-element.22), channel_id=1, source_target_pairs={{0,24},{8,16},{16,8},{24,0},{1,25},{9,17},{17,9},{25,1},{2,26},{10... | collective-permute-start | bytes 4616 | tf_op jit(solution)/shard_map/ppermute | solution.py:352
  9.9 12.3 %collective-permute-done.r1_ref = bf16[24,32]{1,0:T(8,128)(2,1)S(1)} collective-permute-done((bf16[24,32]{1,0:T(8,128)(2,1)S(1)}, bf16[24,32]{1,0:T(8,128)(2,1)S(1)}, u32[]{:S(2)}, u32[]{:S(2)}) %collective-permute-start) | collective-permute-done | bytes 1568 | tf_op jit(solution)/shard_map/ppermute | solution.py:352
  22.2 0.3 collective-permute-start.1
  22.5 3.6 %collective-permute-done.1.r2_ref = bf16[24,32]{1,0:T(8,128)(2,1)S(1)} collective-permute-done((bf16[24,32]{1,0:T(8,128)(2,1)S(1)}, bf16[24,32]{1,0:T(8,128)(2,1)S(1)}, u32[]{:S(2)}, u32[]{:S(2)}) %collective-permute-start.1) | collective-permute-done | bytes 1568 | tf_op jit(solution)/shard_map/ppermute | solution.py:352
  26.1 0.1 shard_map.137
  26.3 19.0 %all_to_all.10.recv_ref = bf16[32,24,128]{2,1,0:T(8,128)(2,1)S(1)} all-to-all(bf16[32,24,128]{2,1,0:T(8,128)(2,1)S(1)} %shard_map.137), channel_id=1, replica_groups=mesh['pp'=4,'ym'=2,'yh'=2,'tz'=4,'tc'=2] {'pp','tz','tc'}, dimensions={0} | all-to-all | bytes 393216 | tf_op jit(solution)/shard_map/all_to_all | solution.py:433
  45.3 1.8 %shard_map.138 = (bf16[96,256]{1,0:T(8,128)(2,1)S(1)}, f32[96,256]{1,0:T(8,128)S(1)}, bf16[96,256]{1,0:T(8,128)(2,1)S(1)}) custom-call(s32[5,256]{1,0:T(8,128)S(1)} %broadcast_in_dim.2.where_ref, bf16[32,24,128]{2,1,0:T(8,128)(2,1)S(1)} %all_to_all.10.recv_ref, bf16[168,1024]{1,0:T(8,128)(2,1)S(1)} %get-tuple-element.23.refs_0_, ...), custom_call_target="tpu_custom_call" | custom-call | tf_op jit(solution)/shard_map/pallas_call | solution.py:439
  47.1 0.4 collective-permute-start.6
  47.4 0.9 collective-permute-done.6
  48.4 1.0 collective-permute-start.9
  49.4 1.1 collective-permute-start.8
  50.5 1.2 %collective-permute-start.7 = (bf16[96,256]{1,0:T(8,128)(2,1)S(1)}, bf16[96,256]{1,0:T(8,128)(2,1)S(1)}, u32[]{:S(2)}, u32[]{:S(2)}) collective-permute-start(bf16[96,256]{1,0:T(8,128)(2,1)S(1)} %add_convert_fusion.9), channel_id=1, source_target_pairs={{0,2},{2,0},{4,6},{6,4},{1,3},{3,1},{5,7},{7,5},{8,10},{10,8},{12,... | collective-permute-start | bytes 147464 | tf_op jit(solution)/shard_map/ppermute | solution.py:352
  51.7 0.9 collective-permute-done.9
  52.6 1.3 %collective-permute-done.8 = bf16[96,256]{1,0:T(8,128)(2,1)S(1)} collective-permute-done((bf16[96,256]{1,0:T(8,128)(2,1)S(1)}, bf16[96,256]{1,0:T(8,128)(2,1)S(1)}, u32[]{:S(2)}, u32[]{:S(2)}) %collective-permute-start.8) | collective-permute-done | bytes 49184 | tf_op jit(solution)/shard_map/ppermute | solution.py:352
  54.0 0.1 collective-permute-start.12
  54.0 1.2 collective-permute-start.10
  55.2 2.7 %collective-permute-done.12.c_ref = bf16[96,256]{1,0:T(8,128)(2,1)S(1)} collective-permute-done((bf16[96,256]{1,0:T(8,128)(2,1)S(1)}, bf16[96,256]{1,0:T(8,128)(2,1)S(1)}, u32[]{:S(2)}, u32[]{:S(2)}) %collective-permute-start.12) | collective-permute-done | bytes 49184 | tf_op jit(solution)/shard_map/ppermute | solution.py:454
  57.9 2.8 %collective-permute-start.13 = (bf16[96,256]{1,0:T(8,128)(2,1)S(1)}, bf16[96,256]{1,0:T(8,128)(2,1)S(1)}, u32[]{:S(2)}, u32[]{:S(2)}) collective-permute-start(bf16[96,256]{1,0:T(8,128)(2,1)S(1)} %collective-permute-done.12.c_ref), channel_id=1, source_target_pairs={{0,1},{1,0},{2,3},{3,2},{4,5},{5,4},{6,7},{7,6},{8,9},{9,8},{10,11... | collective-permute-start | bytes 147464 | tf_op jit(solution)/shard_map/ppermute | solution.py:352
  60.7 0.9 collective-permute-done.13.d_ref
  61.6 0.4 collective-permute-done.11.b_ref
  62.0 1.6 %shard_map.139 = (f32[96,256]{1,0:T(8,128)S(1)}, bf16[96,256]{1,0:T(8,128)(2,1)S(1)}) custom-call(s32[5,256]{1,0:T(8,128)S(1)} %broadcast_in_dim.2.where_ref, bf16[96,256]{1,0:T(8,128)(2,1)S(1)} %collective-permute-done.10.a_ref, bf16[96,256]{1,0:T(8,128)(2,1)S(1)} %collective-permute-done.11.b_ref, bf16[96,256]{1,0:T(8,128)(2,1)S(1)} %collective-permute-done.12.c_ref, ...), custom_call_target="tpu_custom_call" | custom-call | tf_op jit(solution)/shard_map/pallas_call | solution.py:458
  63.6 0.2 collective-permute-start.14
  63.8 1.1 collective-permute-done.14
  64.9 1.8 %collective-permute-start.17 = (bf16[96,256]{1,0:T(8,128)(2,1)S(1)}, bf16[96,256]{1,0:T(8,128)(2,1)S(1)}, u32[]{:S(2)}, u32[]{:S(2)}) collective-permute-start(bf16[96,256]{1,0:T(8,128)(2,1)S(1)} %add_convert_fusion.6), channel_id=1, source_target_pairs={{0,6},{2,4},{4,2},{6,0},{1,7},{3,5},{5,3},{7,1},{8,14},{10,12},{12... | collective-permute-start | bytes 147464 | tf_op jit(solution)/shard_map/ppermute | solution.py:352
  66.7 1.1 collective-permute-start.16
  67.9 0.4 collective-permute-start.15
  68.3 0.9 collective-permute-done.17
  69.2 2.0 %collective-permute-done.16 = bf16[96,256]{1,0:T(8,128)(2,1)S(1)} collective-permute-done((bf16[96,256]{1,0:T(8,128)(2,1)S(1)}, bf16[96,256]{1,0:T(8,128)(2,1)S(1)}, u32[]{:S(2)}, u32[]{:S(2)}) %collective-permute-start.16) | collective-permute-done | bytes 49184 | tf_op jit(solution)/shard_map/ppermute | solution.py:352
  71.2 1.8 %collective-permute-start.20 = (bf16[96,256]{1,0:T(8,128)(2,1)S(1)}, bf16[96,256]{1,0:T(8,128)(2,1)S(1)}, u32[]{:S(2)}, u32[]{:S(2)}) collective-permute-start(bf16[96,256]{1,0:T(8,128)(2,1)S(1)} %add_convert_fusion.4), channel_id=1, source_target_pairs={{0,1},{1,0},{8,9},{9,8},{32,72},{33,73},{40,64},{41,65},{64,40},{6... | collective-permute-start | bytes 147464 | tf_op jit(solution)/shard_map/ppermute | solution.py:454
  73.1 0.1 collective-permute-start.18
  73.2 0.8 collective-permute-done.20.c_ref
  73.9 0.3 collective-permute-start.21
  74.3 0.2 collective-permute-start.19
  74.5 0.7 collective-permute-done.21.d_ref
  75.2 0.4 collective-permute-done.19.b_ref
  75.5 1.6 %shard_map.140 = (f32[96,256]{1,0:T(8,128)S(1)}, bf16[96,256]{1,0:T(8,128)(2,1)S(1)}) custom-call(s32[5,256]{1,0:T(8,128)S(1)} %broadcast_in_dim.2.where_ref, bf16[96,256]{1,0:T(8,128)(2,1)S(1)} %collective-permute-done.18.a_ref, bf16[96,256]{1,0:T(8,128)(2,1)S(1)} %collective-permute-done.19.b_ref, bf16[96,256]{1,0:T(8,128)(2,1)S(1)} %collective-permute-done.20.c_ref, ...), custom_call_target="tpu_custom_call" | custom-call | tf_op jit(solution)/shard_map/pallas_call | solution.py:458
  77.2 0.2 collective-permute-start.22
  77.4 1.1 collective-permute-done.22
  78.5 1.2 %collective-permute-start.25 = (bf16[96,256]{1,0:T(8,128)(2,1)S(1)}, bf16[96,256]{1,0:T(8,128)(2,1)S(1)}, u32[]{:S(2)}, u32[]{:S(2)}) collective-permute-start(bf16[96,256]{1,0:T(8,128)(2,1)S(1)} %add_convert_fusion.3), channel_id=1, source_target_pairs={{0,6},{2,4},{4,2},{6,0},{1,7},{3,5},{5,3},{7,1},{8,14},{10,12},{12... | collective-permute-start | bytes 147464 | tf_op jit(solution)/shard_map/ppermute | solution.py:352
  79.7 0.8 collective-permute-start.24
  80.5 1.3 %collective-permute-start.23 = (bf16[96,256]{1,0:T(8,128)(2,1)S(1)}, bf16[96,256]{1,0:T(8,128)(2,1)S(1)}, u32[]{:S(2)}, u32[]{:S(2)}) collective-permute-start(bf16[96,256]{1,0:T(8,128)(2,1)S(1)} %add_convert_fusion.3), channel_id=1, source_target_pairs={{0,2},{2,0},{4,6},{6,4},{1,3},{3,1},{5,7},{7,5},{8,10},{10,8},{12,... | collective-permute-start | bytes 147464 | tf_op jit(solution)/shard_map/ppermute | solution.py:352
  81.8 0.9 collective-permute-done.25
  82.7 1.4 %collective-permute-done.24 = bf16[96,256]{1,0:T(8,128)(2,1)S(1)} collective-permute-done((bf16[96,256]{1,0:T(8,128)(2,1)S(1)}, bf16[96,256]{1,0:T(8,128)(2,1)S(1)}, u32[]{:S(2)}, u32[]{:S(2)}) %collective-permute-start.24) | collective-permute-done | bytes 49184 | tf_op jit(solution)/shard_map/ppermute | solution.py:352
  84.2 5.7 %collective-permute-start.28 = (bf16[96,256]{1,0:T(8,128)(2,1)S(1)}, bf16[96,256]{1,0:T(8,128)(2,1)S(1)}, u32[]{:S(2)}, u32[]{:S(2)}) collective-permute-start(bf16[96,256]{1,0:T(8,128)(2,1)S(1)} %add_convert_fusion.1), channel_id=1, source_target_pairs={{0,40},{1,41},{8,32},{9,33},{32,8},{33,9},{40,0},{41,1},{64,104},{... | collective-permute-start | bytes 147464 | tf_op jit(solution)/shard_map/ppermute | solution.py:454
  90.0 1.5 %collective-permute-done.28.c_ref = bf16[96,256]{1,0:T(8,128)(2,1)S(1)} collective-permute-done((bf16[96,256]{1,0:T(8,128)(2,1)S(1)}, bf16[96,256]{1,0:T(8,128)(2,1)S(1)}, u32[]{:S(2)}, u32[]{:S(2)}) %collective-permute-start.28) | collective-permute-done | bytes 49184 | tf_op jit(solution)/shard_map/ppermute | solution.py:454
  91.5 2.9 %collective-permute-start.29 = (bf16[96,256]{1,0:T(8,128)(2,1)S(1)}, bf16[96,256]{1,0:T(8,128)(2,1)S(1)}, u32[]{:S(2)}, u32[]{:S(2)}) collective-permute-start(bf16[96,256]{1,0:T(8,128)(2,1)S(1)} %collective-permute-done.28.c_ref), channel_id=1, source_target_pairs={{0,1},{1,0},{2,3},{3,2},{4,5},{5,4},{6,7},{7,6},{8,9},{9,8},{10,11... | collective-permute-start | bytes 147464 | tf_op jit(solution)/shard_map/ppermute | solution.py:352
  94.3 1.8 %collective-permute-start.27 = (bf16[96,256]{1,0:T(8,128)(2,1)S(1)}, bf16[96,256]{1,0:T(8,128)(2,1)S(1)}, u32[]{:S(2)}, u32[]{:S(2)}) collective-permute-start(bf16[96,256]{1,0:T(8,128)(2,1)S(1)} %collective-permute-done.26.a_ref.mine_ref), channel_id=1, source_target_pairs={{0,1},{1,0},{2,3},{3,2},{4,5},{5,4},{6,7},{7,6},{8,9},{9,8},{10,11... | collective-permute-start | bytes 147464 | tf_op jit(solution)/shard_map/ppermute | solution.py:352
  96.1 0.9 collective-permute-done.27.b_ref
  97.0 1.6 %shard_map.141 = (f32[96,256]{1,0:T(8,128)S(1)}, bf16[96,256]{1,0:T(8,128)(2,1)S(1)}) custom-call(s32[5,256]{1,0:T(8,128)S(1)} %broadcast_in_dim.2.where_ref, bf16[96,256]{1,0:T(8,128)(2,1)S(1)} %collective-permute-done.26.a_ref.mine_ref, bf16[96,256]{1,0:T(8,128)(2,1)S(1)} %collective-permute-done.27.b_ref, ...), custom_call_target="tpu_custom_call" | custom-call | tf_op jit(solution)/shard_map/pallas_call | solution.py:458
  98.7 0.4 collective-permute-start.30
  99.1 0.9 collective-permute-done.30
  100.0 1.3 %collective-permute-start.33 = (bf16[96,256]{1,0:T(8,128)(2,1)S(1)}, bf16[96,256]{1,0:T(8,128)(2,1)S(1)}, u32[]{:S(2)}, u32[]{:S(2)}) collective-permute-start(bf16[96,256]{1,0:T(8,128)(2,1)S(1)} %add_convert_fusion.m0_ref), channel_id=1, source_target_pairs={{0,6},{2,4},{4,2},{6,0},{1,7},{3,5},{5,3},{7,1},{8,14},{10,12},{12... | collective-permute-start | bytes 147464 | tf_op jit(solution)/shard_map/ppermute | solution.py:352
  101.3 1.0 collective-permute-start.32
  102.2 1.1 collective-permute-start.31
  103.3 0.9 collective-permute-done.33.m3_ref
  104.2 1.5 %collective-permute-done.32.m2_ref = bf16[96,256]{1,0:T(8,128)(2,1)S(1)} collective-permute-done((bf16[96,256]{1,0:T(8,128)(2,1)S(1)}, bf16[96,256]{1,0:T(8,128)(2,1)S(1)}, u32[]{:S(2)}, u32[]{:S(2)}) %collective-permute-start.32) | collective-permute-done | bytes 49184 | tf_op jit(solution)/shard_map/ppermute | solution.py:352
  105.7 0.2 shard_map.142
  105.9 12.9 %all_to_all.11.recv_ref = bf16[32,8,128]{2,1,0:T(8,128)(2,1)S(1)} all-to-all(bf16[32,8,128]{2,1,0:T(8,128)(2,1)S(1)} %shard_map.142), channel_id=1, replica_groups=mesh['pp'=4,'ym'=2,'yh'=2,'tz'=4,'tc'=2] {'pp','ym','yh','tc'}, dimensions={0} | all-to-all | bytes 131072 | tf_op jit(solution)/shard_map/all_to_all | solution.py:461
  118.8 0.8 shard_map.143
  (27 shorter events, 0.3 us)
Async XLA Ops:
  2.4 42.9 %collective-permute-start.5 = (bf16[168,1024]{1,0:T(8,128)(2,1)S(1)}, bf16[168,1024]{1,0:T(8,128)(2,1)S(1)}, u32[]{:S(2)}, u32[]{:S(2)}) collective-permute-start(bf16[168,1024]{1,0:T(8,128)(2,1)S(1)} %get-tuple-element.24), channel_id=1, source_target_pairs={{0,24},{8,16},{16,8},{24,0},{1,25},{9,17},{17,9},{25,1},{2,26},{10... | collective-permute-start | bytes 1032200 | tf_op jit(solution)/shard_map/ppermute | solution.py:352
  6.0 39.3 %collective-permute-start.3 = (bf16[168,1024]{1,0:T(8,128)(2,1)S(1)}, bf16[168,1024]{1,0:T(8,128)(2,1)S(1)}, u32[]{:S(2)}, u32[]{:S(2)}) collective-permute-start(bf16[168,1024]{1,0:T(8,128)(2,1)S(1)} %get-tuple-element.24), channel_id=1, source_target_pairs={{0,8},{8,0},{16,24},{24,16},{1,9},{9,1},{17,25},{25,17},{2,10},{10... | collective-permute-start | bytes 1032200 | tf_op jit(solution)/shard_map/ppermute | solution.py:352
  6.0 39.3 %collective-permute-start.4 = (bf16[168,1024]{1,0:T(8,128)(2,1)S(1)}, bf16[168,1024]{1,0:T(8,128)(2,1)S(1)}, u32[]{:S(2)}, u32[]{:S(2)}) collective-permute-start(bf16[168,1024]{1,0:T(8,128)(2,1)S(1)} %get-tuple-element.23.refs_0_), channel_id=1, source_target_pairs={{0,16},{8,24},{16,0},{24,8},{1,17},{9,25},{17,1},{25,9},{2,18},{10... | collective-permute-start | bytes 1032200 | tf_op jit(solution)/shard_map/ppermute | solution.py:352
  7.3 14.9 %collective-permute-start = (bf16[24,32]{1,0:T(8,128)(2,1)S(1)}, bf16[24,32]{1,0:T(8,128)(2,1)S(1)}, u32[]{:S(2)}, u32[]{:S(2)}) collective-permute-start(bf16[24,32]{1,0:T(8,128)(2,1)S(1)} %get-tuple-element.21.r0_ref), channel_id=1, source_target_pairs={{0,8},{8,0},{16,24},{24,16},{1,9},{9,1},{17,25},{25,17},{2,10},{10... | collective-permute-start | bytes 4616 | tf_op jit(solution)/shard_map/ppermute | solution.py:352
  7.5 37.8 %copy-start = (bf16[1,1024,1,128]{3,1,2,0:T(8,128)(2,1)S(1)}, bf16[1,1024,1,128]{3,1,2,0:T(8,128)(2,1)}, u32[]{:S(2)}) copy-start(bf16[1,1024,1,128]{3,1,2,0:T(8,128)(2,1)} %param.18) | copy-start | bytes 786436
  7.5 37.8 %copy-start.1 = (bf16[1,1024,1,128]{3,1,2,0:T(8,128)(2,1)S(1)}, bf16[1,1024,1,128]{3,1,2,0:T(8,128)(2,1)}, u32[]{:S(2)}) copy-start(bf16[1,1024,1,128]{3,1,2,0:T(8,128)(2,1)} %param.19) | copy-start | bytes 786436
  7.5 15.1 %collective-permute-start.2 = (bf16[24,32]{1,0:T(8,128)(2,1)S(1)}, bf16[24,32]{1,0:T(8,128)(2,1)S(1)}, u32[]{:S(2)}, u32[]{:S(2)}) collective-permute-start(bf16[24,32]{1,0:T(8,128)(2,1)S(1)} %get-tuple-element.22), channel_id=1, source_target_pairs={{0,24},{8,16},{16,8},{24,0},{1,25},{9,17},{17,9},{25,1},{2,26},{10... | collective-permute-start | bytes 4616 | tf_op jit(solution)/shard_map/ppermute | solution.py:352
  22.2 4.0 %collective-permute-start.1 = (bf16[24,32]{1,0:T(8,128)(2,1)S(1)}, bf16[24,32]{1,0:T(8,128)(2,1)S(1)}, u32[]{:S(2)}, u32[]{:S(2)}) collective-permute-start(bf16[24,32]{1,0:T(8,128)(2,1)S(1)} %get-tuple-element.22), channel_id=1, source_target_pairs={{0,16},{8,24},{16,0},{24,8},{1,17},{9,25},{17,1},{25,9},{2,18},{10... | collective-permute-start | bytes 4616 | tf_op jit(solution)/shard_map/ppermute | solution.py:352
  47.1 1.3 %collective-permute-start.6 = (bf16[96,256]{1,0:T(8,128)(2,1)S(1)}, bf16[96,256]{1,0:T(8,128)(2,1)S(1)}, u32[]{:S(2)}, u32[]{:S(2)}) collective-permute-start(bf16[96,256]{1,0:T(8,128)(2,1)S(1)} %get-tuple-element.30), channel_id=1, source_target_pairs={{0,1},{1,0},{2,3},{3,2},{4,5},{5,4},{6,7},{7,6},{8,9},{9,8},{10,11... | collective-permute-start | bytes 147464 | tf_op jit(solution)/shard_map/ppermute | solution.py:352
  48.4 4.2 %collective-permute-start.9 = (bf16[96,256]{1,0:T(8,128)(2,1)S(1)}, bf16[96,256]{1,0:T(8,128)(2,1)S(1)}, u32[]{:S(2)}, u32[]{:S(2)}) collective-permute-start(bf16[96,256]{1,0:T(8,128)(2,1)S(1)} %add_convert_fusion.9), channel_id=1, source_target_pairs={{0,6},{2,4},{4,2},{6,0},{1,7},{3,5},{5,3},{7,1},{8,14},{10,12},{12... | collective-permute-start | bytes 147464 | tf_op jit(solution)/shard_map/ppermute | solution.py:352
  49.4 4.5 %collective-permute-start.8 = (bf16[96,256]{1,0:T(8,128)(2,1)S(1)}, bf16[96,256]{1,0:T(8,128)(2,1)S(1)}, u32[]{:S(2)}, u32[]{:S(2)}) collective-permute-start(bf16[96,256]{1,0:T(8,128)(2,1)S(1)} %add_convert_fusion.9), channel_id=1, source_target_pairs={{0,4},{2,6},{4,0},{6,2},{1,5},{3,7},{5,1},{7,3},{8,12},{10,14},{12... | collective-permute-start | bytes 147464 | tf_op jit(solution)/shard_map/ppermute | solution.py:352
  50.5 3.4 %collective-permute-start.7 = (bf16[96,256]{1,0:T(8,128)(2,1)S(1)}, bf16[96,256]{1,0:T(8,128)(2,1)S(1)}, u32[]{:S(2)}, u32[]{:S(2)}) collective-permute-start(bf16[96,256]{1,0:T(8,128)(2,1)S(1)} %add_convert_fusion.9), channel_id=1, source_target_pairs={{0,2},{2,0},{4,6},{6,4},{1,3},{3,1},{5,7},{7,5},{8,10},{10,8},{12,... | collective-permute-start | bytes 147464 | tf_op jit(solution)/shard_map/ppermute | solution.py:352
  54.0 3.9 %collective-permute-start.12 = (bf16[96,256]{1,0:T(8,128)(2,1)S(1)}, bf16[96,256]{1,0:T(8,128)(2,1)S(1)}, u32[]{:S(2)}, u32[]{:S(2)}) collective-permute-start(bf16[96,256]{1,0:T(8,128)(2,1)S(1)} %add_convert_fusion.7), channel_id=1, source_target_pairs={{0,40},{1,41},{8,32},{9,33},{32,8},{33,9},{40,0},{41,1},{64,104},{... | collective-permute-start | bytes 147464 | tf_op jit(solution)/shard_map/ppermute | solution.py:454
  54.0 6.7 %collective-permute-start.10 = (bf16[96,256]{1,0:T(8,128)(2,1)S(1)}, bf16[96,256]{1,0:T(8,128)(2,1)S(1)}, u32[]{:S(2)}, u32[]{:S(2)}) collective-permute-start(bf16[96,256]{1,0:T(8,128)(2,1)S(1)} %add_convert_fusion.7), channel_id=1, source_target_pairs={{0,32},{1,33},{8,40},{9,41},{32,0},{33,1},{40,8},{41,9},{64,96},{6... | collective-permute-start | bytes 147464 | tf_op jit(solution)/shard_map/ppermute | solution.py:453
  57.9 3.7 %collective-permute-start.13 = (bf16[96,256]{1,0:T(8,128)(2,1)S(1)}, bf16[96,256]{1,0:T(8,128)(2,1)S(1)}, u32[]{:S(2)}, u32[]{:S(2)}) collective-permute-start(bf16[96,256]{1,0:T(8,128)(2,1)S(1)} %collective-permute-done.12.c_ref), channel_id=1, source_target_pairs={{0,1},{1,0},{2,3},{3,2},{4,5},{5,4},{6,7},{7,6},{8,9},{9,8},{10,11... | collective-permute-start | bytes 147464 | tf_op jit(solution)/shard_map/ppermute | solution.py:352
  60.7 1.2 %collective-permute-start.11 = (bf16[96,256]{1,0:T(8,128)(2,1)S(1)}, bf16[96,256]{1,0:T(8,128)(2,1)S(1)}, u32[]{:S(2)}, u32[]{:S(2)}) collective-permute-start(bf16[96,256]{1,0:T(8,128)(2,1)S(1)} %collective-permute-done.10.a_ref), channel_id=1, source_target_pairs={{0,1},{1,0},{2,3},{3,2},{4,5},{5,4},{6,7},{7,6},{8,9},{9,8},{10,11... | collective-permute-start | bytes 147464 | tf_op jit(solution)/shard_map/ppermute | solution.py:352
  63.6 1.3 %collective-permute-start.14 = (bf16[96,256]{1,0:T(8,128)(2,1)S(1)}, bf16[96,256]{1,0:T(8,128)(2,1)S(1)}, u32[]{:S(2)}, u32[]{:S(2)}) collective-permute-start(bf16[96,256]{1,0:T(8,128)(2,1)S(1)} %get-tuple-element.32), channel_id=1, source_target_pairs={{0,1},{1,0},{2,3},{3,2},{4,5},{5,4},{6,7},{7,6},{8,9},{9,8},{10,11... | collective-permute-start | bytes 147464 | tf_op jit(solution)/shard_map/ppermute | solution.py:352
  64.9 4.2 %collective-permute-start.17 = (bf16[96,256]{1,0:T(8,128)(2,1)S(1)}, bf16[96,256]{1,0:T(8,128)(2,1)S(1)}, u32[]{:S(2)}, u32[]{:S(2)}) collective-permute-start(bf16[96,256]{1,0:T(8,128)(2,1)S(1)} %add_convert_fusion.6), channel_id=1, source_target_pairs={{0,6},{2,4},{4,2},{6,0},{1,7},{3,5},{5,3},{7,1},{8,14},{10,12},{12... | collective-permute-start | bytes 147464 | tf_op jit(solution)/shard_map/ppermute | solution.py:352
  66.7 4.4 %collective-permute-start.16 = (bf16[96,256]{1,0:T(8,128)(2,1)S(1)}, bf16[96,256]{1,0:T(8,128)(2,1)S(1)}, u32[]{:S(2)}, u32[]{:S(2)}) collective-permute-start(bf16[96,256]{1,0:T(8,128)(2,1)S(1)} %add_convert_fusion.6), channel_id=1, source_target_pairs={{0,4},{2,6},{4,0},{6,2},{1,5},{3,7},{5,1},{7,3},{8,12},{10,14},{12... | collective-permute-start | bytes 147464 | tf_op jit(solution)/shard_map/ppermute | solution.py:352
  67.9 3.3 %collective-permute-start.15 = (bf16[96,256]{1,0:T(8,128)(2,1)S(1)}, bf16[96,256]{1,0:T(8,128)(2,1)S(1)}, u32[]{:S(2)}, u32[]{:S(2)}) collective-permute-start(bf16[96,256]{1,0:T(8,128)(2,1)S(1)} %add_convert_fusion.6), channel_id=1, source_target_pairs={{0,2},{2,0},{4,6},{6,4},{1,3},{3,1},{5,7},{7,5},{8,10},{10,8},{12,... | collective-permute-start | bytes 147464 | tf_op jit(solution)/shard_map/ppermute | solution.py:352
  71.2 2.7 %collective-permute-start.20 = (bf16[96,256]{1,0:T(8,128)(2,1)S(1)}, bf16[96,256]{1,0:T(8,128)(2,1)S(1)}, u32[]{:S(2)}, u32[]{:S(2)}) collective-permute-start(bf16[96,256]{1,0:T(8,128)(2,1)S(1)} %add_convert_fusion.4), channel_id=1, source_target_pairs={{0,1},{1,0},{8,9},{9,8},{32,72},{33,73},{40,64},{41,65},{64,40},{6... | collective-permute-start | bytes 147464 | tf_op jit(solution)/shard_map/ppermute | solution.py:454
  73.1 1.2 %collective-permute-start.18 = (bf16[96,256]{1,0:T(8,128)(2,1)S(1)}, bf16[96,256]{1,0:T(8,128)(2,1)S(1)}, u32[]{:S(2)}, u32[]{:S(2)}) collective-permute-start(bf16[96,256]{1,0:T(8,128)(2,1)S(1)} %add_convert_fusion.4), channel_id=1, source_target_pairs={{0,1},{1,0},{8,9},{9,8},{32,64},{33,65},{40,72},{41,73},{64,32},{6... | collective-permute-start | bytes 147464 | tf_op jit(solution)/shard_map/ppermute | solution.py:453
  73.9 1.2 %collective-permute-start.21 = (bf16[96,256]{1,0:T(8,128)(2,1)S(1)}, bf16[96,256]{1,0:T(8,128)(2,1)S(1)}, u32[]{:S(2)}, u32[]{:S(2)}) collective-permute-start(bf16[96,256]{1,0:T(8,128)(2,1)S(1)} %collective-permute-done.20.c_ref), channel_id=1, source_target_pairs={{0,1},{1,0},{2,3},{3,2},{4,5},{5,4},{6,7},{7,6},{8,9},{9,8},{10,11... | collective-permute-start | bytes 147464 | tf_op jit(solution)/shard_map/ppermute | solution.py:352
  74.3 1.2 %collective-permute-start.19 = (bf16[96,256]{1,0:T(8,128)(2,1)S(1)}, bf16[96,256]{1,0:T(8,128)(2,1)S(1)}, u32[]{:S(2)}, u32[]{:S(2)}) collective-permute-start(bf16[96,256]{1,0:T(8,128)(2,1)S(1)} %collective-permute-done.18.a_ref), channel_id=1, source_target_pairs={{0,1},{1,0},{2,3},{3,2},{4,5},{5,4},{6,7},{7,6},{8,9},{9,8},{10,11... | collective-permute-start | bytes 147464 | tf_op jit(solution)/shard_map/ppermute | solution.py:352
  77.2 1.3 %collective-permute-start.22 = (bf16[96,256]{1,0:T(8,128)(2,1)S(1)}, bf16[96,256]{1,0:T(8,128)(2,1)S(1)}, u32[]{:S(2)}, u32[]{:S(2)}) collective-permute-start(bf16[96,256]{1,0:T(8,128)(2,1)S(1)} %get-tuple-element.34), channel_id=1, source_target_pairs={{0,1},{1,0},{2,3},{3,2},{4,5},{5,4},{6,7},{7,6},{8,9},{9,8},{10,11... | collective-permute-start | bytes 147464 | tf_op jit(solution)/shard_map/ppermute | solution.py:352
  78.5 4.2 %collective-permute-start.25 = (bf16[96,256]{1,0:T(8,128)(2,1)S(1)}, bf16[96,256]{1,0:T(8,128)(2,1)S(1)}, u32[]{:S(2)}, u32[]{:S(2)}) collective-permute-start(bf16[96,256]{1,0:T(8,128)(2,1)S(1)} %add_convert_fusion.3), channel_id=1, source_target_pairs={{0,6},{2,4},{4,2},{6,0},{1,7},{3,5},{5,3},{7,1},{8,14},{10,12},{12... | collective-permute-start | bytes 147464 | tf_op jit(solution)/shard_map/ppermute | solution.py:352
  79.7 4.4 %collective-permute-start.24 = (bf16[96,256]{1,0:T(8,128)(2,1)S(1)}, bf16[96,256]{1,0:T(8,128)(2,1)S(1)}, u32[]{:S(2)}, u32[]{:S(2)}) collective-permute-start(bf16[96,256]{1,0:T(8,128)(2,1)S(1)} %add_convert_fusion.3), channel_id=1, source_target_pairs={{0,4},{2,6},{4,0},{6,2},{1,5},{3,7},{5,1},{7,3},{8,12},{10,14},{12... | collective-permute-start | bytes 147464 | tf_op jit(solution)/shard_map/ppermute | solution.py:352
  80.5 3.7 %collective-permute-start.23 = (bf16[96,256]{1,0:T(8,128)(2,1)S(1)}, bf16[96,256]{1,0:T(8,128)(2,1)S(1)}, u32[]{:S(2)}, u32[]{:S(2)}) collective-permute-start(bf16[96,256]{1,0:T(8,128)(2,1)S(1)} %add_convert_fusion.3), channel_id=1, source_target_pairs={{0,2},{2,0},{4,6},{6,4},{1,3},{3,1},{5,7},{7,5},{8,10},{10,8},{12,... | collective-permute-start | bytes 147464 | tf_op jit(solution)/shard_map/ppermute | solution.py:352
  84.2 7.2 %collective-permute-start.28 = (bf16[96,256]{1,0:T(8,128)(2,1)S(1)}, bf16[96,256]{1,0:T(8,128)(2,1)S(1)}, u32[]{:S(2)}, u32[]{:S(2)}) collective-permute-start(bf16[96,256]{1,0:T(8,128)(2,1)S(1)} %add_convert_fusion.1), channel_id=1, source_target_pairs={{0,40},{1,41},{8,32},{9,33},{32,8},{33,9},{40,0},{41,1},{64,104},{... | collective-permute-start | bytes 147464 | tf_op jit(solution)/shard_map/ppermute | solution.py:454
  90.0 4.3 %collective-permute-start.26 = (bf16[96,256]{1,0:T(8,128)(2,1)S(1)}, bf16[96,256]{1,0:T(8,128)(2,1)S(1)}, u32[]{:S(2)}, u32[]{:S(2)}) collective-permute-start(bf16[96,256]{1,0:T(8,128)(2,1)S(1)} %add_convert_fusion.1), channel_id=1, source_target_pairs={{0,32},{1,33},{8,40},{9,41},{32,0},{33,1},{40,8},{41,9},{64,96},{6... | collective-permute-start | bytes 147464 | tf_op jit(solution)/shard_map/ppermute | solution.py:453
  91.5 4.7 %collective-permute-start.29 = (bf16[96,256]{1,0:T(8,128)(2,1)S(1)}, bf16[96,256]{1,0:T(8,128)(2,1)S(1)}, u32[]{:S(2)}, u32[]{:S(2)}) collective-permute-start(bf16[96,256]{1,0:T(8,128)(2,1)S(1)} %collective-permute-done.28.c_ref), channel_id=1, source_target_pairs={{0,1},{1,0},{2,3},{3,2},{4,5},{5,4},{6,7},{7,6},{8,9},{9,8},{10,11... | collective-permute-start | bytes 147464 | tf_op jit(solution)/shard_map/ppermute | solution.py:352
  94.3 2.7 %collective-permute-start.27 = (bf16[96,256]{1,0:T(8,128)(2,1)S(1)}, bf16[96,256]{1,0:T(8,128)(2,1)S(1)}, u32[]{:S(2)}, u32[]{:S(2)}) collective-permute-start(bf16[96,256]{1,0:T(8,128)(2,1)S(1)} %collective-permute-done.26.a_ref.mine_ref), channel_id=1, source_target_pairs={{0,1},{1,0},{2,3},{3,2},{4,5},{5,4},{6,7},{7,6},{8,9},{9,8},{10,11... | collective-permute-start | bytes 147464 | tf_op jit(solution)/shard_map/ppermute | solution.py:352
  98.7 1.3 %collective-permute-start.30 = (bf16[96,256]{1,0:T(8,128)(2,1)S(1)}, bf16[96,256]{1,0:T(8,128)(2,1)S(1)}, u32[]{:S(2)}, u32[]{:S(2)}) collective-permute-start(bf16[96,256]{1,0:T(8,128)(2,1)S(1)} %get-tuple-element.36), channel_id=1, source_target_pairs={{0,1},{1,0},{2,3},{3,2},{4,5},{5,4},{6,7},{7,6},{8,9},{9,8},{10,11... | collective-permute-start | bytes 147464 | tf_op jit(solution)/shard_map/ppermute | solution.py:352
  100.0 4.2 %collective-permute-start.33 = (bf16[96,256]{1,0:T(8,128)(2,1)S(1)}, bf16[96,256]{1,0:T(8,128)(2,1)S(1)}, u32[]{:S(2)}, u32[]{:S(2)}) collective-permute-start(bf16[96,256]{1,0:T(8,128)(2,1)S(1)} %add_convert_fusion.m0_ref), channel_id=1, source_target_pairs={{0,6},{2,4},{4,2},{6,0},{1,7},{3,5},{5,3},{7,1},{8,14},{10,12},{12... | collective-permute-start | bytes 147464 | tf_op jit(solution)/shard_map/ppermute | solution.py:352
  101.3 4.4 %collective-permute-start.32 = (bf16[96,256]{1,0:T(8,128)(2,1)S(1)}, bf16[96,256]{1,0:T(8,128)(2,1)S(1)}, u32[]{:S(2)}, u32[]{:S(2)}) collective-permute-start(bf16[96,256]{1,0:T(8,128)(2,1)S(1)} %add_convert_fusion.m0_ref), channel_id=1, source_target_pairs={{0,4},{2,6},{4,0},{6,2},{1,5},{3,7},{5,1},{7,3},{8,12},{10,14},{12... | collective-permute-start | bytes 147464 | tf_op jit(solution)/shard_map/ppermute | solution.py:352
  102.2 3.5 %collective-permute-start.31 = (bf16[96,256]{1,0:T(8,128)(2,1)S(1)}, bf16[96,256]{1,0:T(8,128)(2,1)S(1)}, u32[]{:S(2)}, u32[]{:S(2)}) collective-permute-start(bf16[96,256]{1,0:T(8,128)(2,1)S(1)} %add_convert_fusion.m0_ref), channel_id=1, source_target_pairs={{0,2},{2,0},{4,6},{6,4},{1,3},{3,1},{5,7},{7,5},{8,10},{10,8},{12,... | collective-permute-start | bytes 147464 | tf_op jit(solution)/shard_map/ppermute | solution.py:352

commit v4 on v3

--- a/solution.py
+++ b/solution.py
@@ -352,17 +352,13 @@
     return lax.ppermute(v, axes, [(i, i ^ bits) for i in range(size)])
 
 
-def hop_pairs(first, size, flip_half):
+def sum_pairs(active, sections, bits):
     pairs = []
-    for i in range(size):
-        j = i + 1 if (i - first) % 2 == 0 else i - 1
-        for h in range(2):
+    for i in range(sections):
+        for z in range(4):
             for c in range(2):
-                if 0 <= j < size:
-                    target = (j, 1 - h if flip_half else h, c)
-                else:
-                    target = (i, h, 1 - c)
-                pairs.append((4 * i + 2 * h + c, 4 * target[0] + 2 * target[1] + target[2]))
+                target = 2 * (z ^ bits) + c if i == active else 2 * z + 1 - c
+                pairs.append((8 * i + 2 * z + c, 8 * i + target))
     return pairs
 
 
@@ -439,19 +435,21 @@
     mine, own, far = call_kernel(
         entry_section_kernel, [quarter, *outs], 10, [pad, pltpu.VMEM((4, T, 256), F32)]
     )(where, recv, *params)
+    hop = [(i, (i + 1) % sections) for i in range(sections)]
+    hop_flip = [(2 * i + h, 2 * j + 1 - h) for i, j in hop for h in range(2)]
     for s in range(sections):
         got = flip(far, "tc", 1)
         mixed = (own + got.astype(F32)).astype(BF16)
         others = []
         for d in (1, 2, 3):
-            others.append(flip(mixed, "tz", d))
+            others.append(lax.ppermute(mixed, ("pp", "tz", "tc"), sum_pairs(s, sections, d)))
         if s + 1 == sections:
             break
         r1, r2, r3 = [v.astype(F32) for v in others]
         branch = ((mixed.astype(F32) + r1) + (r2 + r3)).astype(BF16).astype(F32)
         produced = (mine.astype(F32) + 0.5 * branch).astype(BF16)
-        a = lax.ppermute(produced, ("pp", "yh", "tc"), hop_pairs(s, sections, False))
-        c = lax.ppermute(produced, ("pp", "yh", "tc"), hop_pairs(s, sections, True))
+        a = lax.ppermute(produced, "pp", hop)
+        c = lax.ppermute(produced, ("pp", "yh"), hop_flip)
         b = flip(a, "tc", 1)
         d = flip(c, "tc", 1)
         mine = a

time: 120 us -> 114 us (0.950)
  starting transfers between devices: 39.4 us -> 30.6 us
  blocking collectives: 31.9 us -> 35 us
    ppermute x28 -> x16, starting transfers between devices: 30.5 us -> 18.7 us  [flip(): return lax.ppermute(v, axes, [(i, i ^ bits) for i in range(size)])]
    ppermute x6 -> x18, waiting for transfers between devices: 4.92 us -> 14.9 us  [the longest x3 9.25 us: per_device(): c = lax.ppermute(produced, ('pp', 'yh'), hop_flip)]
    ppermute x28 -> x16, waiting for transfers between devices: 32.9 us -> 23.1 us  [flip(): return lax.ppermute(v, axes, [(i, i ^ bits) for i in range(size)])]
    all_to_all x1, blocking collectives: 12.9 us -> 16 us  [per_device(): recv = lax.all_to_all(send, ('pp', 'ym', 'yh', 'tc'), 0, 0)]
    ppermute x6 -> x18, starting transfers between devices: 8.93 us -> 11.9 us  [the longest x12 5.77 us: per_device(): lax.ppermute(mixed, ('pp', 'tz', 'tc'), sum_pairs(s, sections, d))]
  transfers between devices with their start and end apart: 34 -> 34, of which waited for: 22 -> 26; matrix products, arithmetic and copies ran while one was open for 0% -> 0% of each run, Pallas kernels for 0% -> 0%
where the time goes in v4:
time: 114 us
  waiting for transfers between devices  38 us (33%)
  blocking collectives  35 us (31%)
  starting transfers between devices  30.6 us (27%)
  Pallas kernels  9.37 us (8%)
    ppermute x16, waiting for transfers between devices, flip(): return lax.ppermute(v, axes, [(i, i ^ bits) for i in range(size)])  23.1 us
    all_to_all x1, blocking collectives, per_device(): recv = lax.all_to_all(send, BLOCKS, 0, 0)  19 us
    ppermute x16, starting transfers between devices, flip(): return lax.ppermute(v, axes, [(i, i ^ bits) for i in range(size)])  18.7 us
    all_to_all x1, blocking collectives, per_device(): recv = lax.all_to_all(send, ('pp', 'ym', 'yh', 'tc'), 0, 0)  16 us
    ppermute x3, waiting for transfers between devices, per_device(): c = lax.ppermute(produced, ('pp', 'yh'), hop_flip)  9.25 us
    ppermute x12, starting transfers between devices, per_device(): lax.ppermute(mixed, ('pp', 'tz', 'tc'), sum_pairs(s, sections, d))  5.77 us
    ppermute x12, waiting for transfers between devices, per_device(): lax.ppermute(mixed, ('pp', 'tz', 'tc'), sum_pairs(s, sections, d))  5.31 us
    pallas_call x3, Pallas kernels, per_device(): call_kernel(relay_section_kernel, outs, 13, [pad])  4.93 us
  transfers between devices with their start and end apart: 34, of which 26 were waited for; matrix products, arithmetic and copies ran while one was open for 0% of the time, Pallas kernels for 0%

profile of v4, /device:TPU:1, one launch (start us, length us, event | category | flops | bytes accessed | tf_op | source)
XLA Modules:
  0.0 114.1 jit_solution(7796700606527428638)
XLA Ops:
  0.8 1.5 %shard_map.136 = (bf16[24,32]{1,0:T(8,128)(2,1)S(1)}, bf16[24,32]{1,0:T(8,128)(2,1)S(1)}, bf16[168,1024]{1,0:T(8,128)(2,1)S(1)}, bf16[168,1024]{1,0:T(8,128)(2,1...) custom-call(s32[5,256]{1,0:T(8,128)S(1)} %broadcast_in_dim.2.where_ref, ...), custom_call_target="tpu_custom_call" | custom-call | tf_op jit(solution)/shard_map/pallas_call | solution.py:405
  2.4 3.6 %collective-permute-start.5 = (bf16[168,1024]{1,0:T(8,128)(2,1)S(1)}, bf16[168,1024]{1,0:T(8,128)(2,1)S(1)}, u32[]{:S(2)}, u32[]{:S(2)}) collective-permute-start(bf16[168,1024]{1,0:T(8,128)(2,1)S(1)} %get-tuple-element.24), channel_id=1, source_target_pairs={{0,24},{8,16},{16,8},{24,0},{1,25},{9,17},{17,9},{25,1},{2,26},{10... | collective-permute-start | bytes 1032200 | tf_op jit(solution)/shard_map/ppermute | solution.py:352
  6.0 1.3 %collective-permute-start.4 = (bf16[168,1024]{1,0:T(8,128)(2,1)S(1)}, bf16[168,1024]{1,0:T(8,128)(2,1)S(1)}, u32[]{:S(2)}, u32[]{:S(2)}) collective-permute-start(bf16[168,1024]{1,0:T(8,128)(2,1)S(1)} %get-tuple-element.23.refs_0_), channel_id=1, source_target_pairs={{0,16},{8,24},{16,0},{24,8},{1,17},{9,25},{17,1},{25,9},{2,18},{10... | collective-permute-start | bytes 1032200 | tf_op jit(solution)/shard_map/ppermute | solution.py:352
  7.3 0.2 collective-permute-start
  7.5 2.4 %collective-permute-start.2 = (bf16[24,32]{1,0:T(8,128)(2,1)S(1)}, bf16[24,32]{1,0:T(8,128)(2,1)S(1)}, u32[]{:S(2)}, u32[]{:S(2)}) collective-permute-start(bf16[24,32]{1,0:T(8,128)(2,1)S(1)} %get-tuple-element.22), channel_id=1, source_target_pairs={{0,24},{8,16},{16,8},{24,0},{1,25},{9,17},{17,9},{25,1},{2,26},{10... | collective-permute-start | bytes 4616 | tf_op jit(solution)/shard_map/ppermute | solution.py:352
  9.9 12.3 %collective-permute-done.r1_ref = bf16[24,32]{1,0:T(8,128)(2,1)S(1)} collective-permute-done((bf16[24,32]{1,0:T(8,128)(2,1)S(1)}, bf16[24,32]{1,0:T(8,128)(2,1)S(1)}, u32[]{:S(2)}, u32[]{:S(2)}) %collective-permute-start) | collective-permute-done | bytes 1568 | tf_op jit(solution)/shard_map/ppermute | solution.py:352
  22.2 0.3 collective-permute-start.1
  22.5 3.6 %collective-permute-done.1.r2_ref = bf16[24,32]{1,0:T(8,128)(2,1)S(1)} collective-permute-done((bf16[24,32]{1,0:T(8,128)(2,1)S(1)}, bf16[24,32]{1,0:T(8,128)(2,1)S(1)}, u32[]{:S(2)}, u32[]{:S(2)}) %collective-permute-start.1) | collective-permute-done | bytes 1568 | tf_op jit(solution)/shard_map/ppermute | solution.py:352
  26.1 0.1 shard_map.137
  26.3 19.0 %all_to_all.10.recv_ref = bf16[32,24,128]{2,1,0:T(8,128)(2,1)S(1)} all-to-all(bf16[32,24,128]{2,1,0:T(8,128)(2,1)S(1)} %shard_map.137), channel_id=1, replica_groups=mesh['pp'=4,'ym'=2,'yh'=2,'tz'=4,'tc'=2] {'pp','tz','tc'}, dimensions={0} | all-to-all | bytes 393216 | tf_op jit(solution)/shard_map/all_to_all | solution.py:429
  45.3 1.8 %shard_map.138 = (bf16[96,256]{1,0:T(8,128)(2,1)S(1)}, f32[96,256]{1,0:T(8,128)S(1)}, bf16[96,256]{1,0:T(8,128)(2,1)S(1)}) custom-call(s32[5,256]{1,0:T(8,128)S(1)} %broadcast_in_dim.2.where_ref, bf16[32,24,128]{2,1,0:T(8,128)(2,1)S(1)} %all_to_all.10.recv_ref, bf16[168,1024]{1,0:T(8,128)(2,1)S(1)} %get-tuple-element.23.refs_0_, ...), custom_call_target="tpu_custom_call" | custom-call | tf_op jit(solution)/shard_map/pallas_call | solution.py:435
  47.1 0.4 collective-permute-start.6
  47.4 0.9 collective-permute-done.6
  48.4 1.0 collective-permute-start.9
  49.4 1.1 collective-permute-start.8
  50.5 1.2 %collective-permute-start.7 = (bf16[96,256]{1,0:T(8,128)(2,1)S(1)}, bf16[96,256]{1,0:T(8,128)(2,1)S(1)}, u32[]{:S(2)}, u32[]{:S(2)}) collective-permute-start(bf16[96,256]{1,0:T(8,128)(2,1)S(1)} %add_convert_fusion.9), channel_id=1, source_target_pairs={{0,2},{1,3},{2,0},{3,1},{4,6},{5,7},{6,4},{7,5},{32,33},{33,32},{3... | collective-permute-start | bytes 147464 | tf_op jit(solution)/shard_map/ppermute | solution.py:445
  51.7 0.9 collective-permute-done.9
  52.6 1.3 %collective-permute-done.8 = bf16[96,256]{1,0:T(8,128)(2,1)S(1)} collective-permute-done((bf16[96,256]{1,0:T(8,128)(2,1)S(1)}, bf16[96,256]{1,0:T(8,128)(2,1)S(1)}, u32[]{:S(2)}, u32[]{:S(2)}) %collective-permute-start.8) | collective-permute-done | bytes 49184 | tf_op jit(solution)/shard_map/ppermute | solution.py:445
  54.1 5.0 %collective-permute-done.12.c_ref = bf16[96,256]{1,0:T(8,128)(2,1)S(1)} collective-permute-done((bf16[96,256]{1,0:T(8,128)(2,1)S(1)}, bf16[96,256]{1,0:T(8,128)(2,1)S(1)}, u32[]{:S(2)}, u32[]{:S(2)}) %collective-permute-start.12) | collective-permute-done | bytes 49184 | tf_op jit(solution)/shard_map/ppermute | solution.py:452
  59.1 2.8 %collective-permute-start.13 = (bf16[96,256]{1,0:T(8,128)(2,1)S(1)}, bf16[96,256]{1,0:T(8,128)(2,1)S(1)}, u32[]{:S(2)}, u32[]{:S(2)}) collective-permute-start(bf16[96,256]{1,0:T(8,128)(2,1)S(1)} %collective-permute-done.12.c_ref), channel_id=1, source_target_pairs={{0,1},{1,0},{2,3},{3,2},{4,5},{5,4},{6,7},{7,6},{8,9},{9,8},{10,11... | collective-permute-start | bytes 147464 | tf_op jit(solution)/shard_map/ppermute | solution.py:352
  61.9 0.9 collective-permute-done.13.d_ref
  62.8 0.4 collective-permute-done.11.b_ref
  63.2 1.6 %shard_map.139 = (f32[96,256]{1,0:T(8,128)S(1)}, bf16[96,256]{1,0:T(8,128)(2,1)S(1)}) custom-call(s32[5,256]{1,0:T(8,128)S(1)} %broadcast_in_dim.2.where_ref, bf16[96,256]{1,0:T(8,128)(2,1)S(1)} %collective-permute-done.10.a_ref, bf16[96,256]{1,0:T(8,128)(2,1)S(1)} %collective-permute-done.11.b_ref, bf16[96,256]{1,0:T(8,128)(2,1)S(1)} %collective-permute-done.12.c_ref, ...), custom_call_target="tpu_custom_call" | custom-call | tf_op jit(solution)/shard_map/pallas_call | solution.py:456
  64.8 0.2 collective-permute-start.14
  65.0 1.1 collective-permute-done.14
  66.1 0.2 collective-permute-start.17
  66.4 0.3 collective-permute-start.16
  66.7 0.2 collective-permute-start.15
  66.9 0.6 collective-permute-done.17
  67.4 0.2 collective-permute-done.16
  67.6 0.3 collective-permute-done.15
  68.0 3.0 %collective-permute-start.20 = (bf16[96,256]{1,0:T(8,128)(2,1)S(1)}, bf16[96,256]{1,0:T(8,128)(2,1)S(1)}, u32[]{:S(2)}, u32[]{:S(2)}) collective-permute-start(bf16[96,256]{1,0:T(8,128)(2,1)S(1)} %add_convert_fusion.4), channel_id=1, source_target_pairs={{0,40},{8,32},{32,72},{40,64},{64,104},{72,96},{96,8},{104,0},{1,4... | collective-permute-start | bytes 147464 | tf_op jit(solution)/shard_map/ppermute | solution.py:452
  71.0 2.1 %collective-permute-done.20.c_ref = bf16[96,256]{1,0:T(8,128)(2,1)S(1)} collective-permute-done((bf16[96,256]{1,0:T(8,128)(2,1)S(1)}, bf16[96,256]{1,0:T(8,128)(2,1)S(1)}, u32[]{:S(2)}, u32[]{:S(2)}) %collective-permute-start.20) | collective-permute-done | bytes 49184 | tf_op jit(solution)/shard_map/ppermute | solution.py:452
  73.1 1.7 %collective-permute-start.21 = (bf16[96,256]{1,0:T(8,128)(2,1)S(1)}, bf16[96,256]{1,0:T(8,128)(2,1)S(1)}, u32[]{:S(2)}, u32[]{:S(2)}) collective-permute-start(bf16[96,256]{1,0:T(8,128)(2,1)S(1)} %collective-permute-done.20.c_ref), channel_id=1, source_target_pairs={{0,1},{1,0},{2,3},{3,2},{4,5},{5,4},{6,7},{7,6},{8,9},{9,8},{10,11... | collective-permute-start | bytes 147464 | tf_op jit(solution)/shard_map/ppermute | solution.py:352
  74.8 0.4 collective-permute-done.18.a_ref
  75.2 3.2 %collective-permute-start.19 = (bf16[96,256]{1,0:T(8,128)(2,1)S(1)}, bf16[96,256]{1,0:T(8,128)(2,1)S(1)}, u32[]{:S(2)}, u32[]{:S(2)}) collective-permute-start(bf16[96,256]{1,0:T(8,128)(2,1)S(1)} %collective-permute-done.18.a_ref), channel_id=1, source_target_pairs={{0,1},{1,0},{2,3},{3,2},{4,5},{5,4},{6,7},{7,6},{8,9},{9,8},{10,11... | collective-permute-start | bytes 147464 | tf_op jit(solution)/shard_map/ppermute | solution.py:352
  78.3 0.9 collective-permute-done.19.b_ref
  79.2 1.6 %shard_map.140 = (f32[96,256]{1,0:T(8,128)S(1)}, bf16[96,256]{1,0:T(8,128)(2,1)S(1)}) custom-call(s32[5,256]{1,0:T(8,128)S(1)} %broadcast_in_dim.2.where_ref, bf16[96,256]{1,0:T(8,128)(2,1)S(1)} %collective-permute-done.18.a_ref, bf16[96,256]{1,0:T(8,128)(2,1)S(1)} %collective-permute-done.19.b_ref, bf16[96,256]{1,0:T(8,128)(2,1)S(1)} %collective-permute-done.20.c_ref, ...), custom_call_target="tpu_custom_call" | custom-call | tf_op jit(solution)/shard_map/pallas_call | solution.py:456
  80.9 0.4 collective-permute-start.22
  81.3 0.9 collective-permute-done.22
  82.2 0.4 collective-permute-start.25
  82.6 0.3 collective-permute-start.24
  82.9 0.2 collective-permute-start.23
  83.1 0.4 collective-permute-done.25
  83.5 0.3 collective-permute-done.24
  83.9 0.3 collective-permute-done.23
  84.3 2.8 %collective-permute-start.26 = (bf16[96,256]{1,0:T(8,128)(2,1)S(1)}, bf16[96,256]{1,0:T(8,128)(2,1)S(1)}, u32[]{:S(2)}, u32[]{:S(2)}) collective-permute-start(bf16[96,256]{1,0:T(8,128)(2,1)S(1)} %add_convert_fusion.1), channel_id=1, source_target_pairs={{0,32},{32,64},{64,96},{96,0},{1,33},{33,65},{65,97},{97,1},{2,34}... | collective-permute-start | bytes 147464 | tf_op jit(solution)/shard_map/ppermute | solution.py:451
  87.1 2.2 %collective-permute-done.28.c_ref = bf16[96,256]{1,0:T(8,128)(2,1)S(1)} collective-permute-done((bf16[96,256]{1,0:T(8,128)(2,1)S(1)}, bf16[96,256]{1,0:T(8,128)(2,1)S(1)}, u32[]{:S(2)}, u32[]{:S(2)}) %collective-permute-start.28) | collective-permute-done | bytes 49184 | tf_op jit(solution)/shard_map/ppermute | solution.py:452
  89.3 1.7 %collective-permute-start.29 = (bf16[96,256]{1,0:T(8,128)(2,1)S(1)}, bf16[96,256]{1,0:T(8,128)(2,1)S(1)}, u32[]{:S(2)}, u32[]{:S(2)}) collective-permute-start(bf16[96,256]{1,0:T(8,128)(2,1)S(1)} %collective-permute-done.28.c_ref), channel_id=1, source_target_pairs={{0,1},{1,0},{2,3},{3,2},{4,5},{5,4},{6,7},{7,6},{8,9},{9,8},{10,11... | collective-permute-start | bytes 147464 | tf_op jit(solution)/shard_map/ppermute | solution.py:352
  91.0 0.2 collective-permute-start.27
  91.2 0.7 collective-permute-done.29.d_ref
  91.9 0.4 collective-permute-done.27.b_ref
  92.3 1.6 %shard_map.141 = (f32[96,256]{1,0:T(8,128)S(1)}, bf16[96,256]{1,0:T(8,128)(2,1)S(1)}) custom-call(s32[5,256]{1,0:T(8,128)S(1)} %broadcast_in_dim.2.where_ref, bf16[96,256]{1,0:T(8,128)(2,1)S(1)} %collective-permute-done.26.a_ref.mine_ref, bf16[96,256]{1,0:T(8,128)(2,1)S(1)} %collective-permute-done.27.b_ref, ...), custom_call_target="tpu_custom_call" | custom-call | tf_op jit(solution)/shard_map/pallas_call | solution.py:456
  93.9 0.2 collective-permute-start.30
  94.2 1.1 collective-permute-done.30
  95.3 0.2 collective-permute-start.33
  95.5 0.3 collective-permute-start.32
  95.8 0.2 collective-permute-start.31
  96.0 0.6 collective-permute-done.33.m3_ref
  96.6 0.2 collective-permute-done.32.m2_ref
  96.7 0.3 collective-permute-done.31.m1_ref
  97.1 0.2 shard_map.142
  97.3 16.0 %all_to_all.11.recv_ref = bf16[32,8,128]{2,1,0:T(8,128)(2,1)S(1)} all-to-all(bf16[32,8,128]{2,1,0:T(8,128)(2,1)S(1)} %shard_map.142), channel_id=1, replica_groups=mesh['pp'=4,'ym'=2,'yh'=2,'tz'=4,'tc'=2] {'pp','ym','yh','tc'}, dimensions={0} | all-to-all | bytes 131072 | tf_op jit(solution)/shard_map/all_to_all | solution.py:459
  113.3 0.8 shard_map.143
  (27 shorter events, 0.6 us)
Async XLA Ops:
  2.4 42.9 %collective-permute-start.5 = (bf16[168,1024]{1,0:T(8,128)(2,1)S(1)}, bf16[168,1024]{1,0:T(8,128)(2,1)S(1)}, u32[]{:S(2)}, u32[]{:S(2)}) collective-permute-start(bf16[168,1024]{1,0:T(8,128)(2,1)S(1)} %get-tuple-element.24), channel_id=1, source_target_pairs={{0,24},{8,16},{16,8},{24,0},{1,25},{9,17},{17,9},{25,1},{2,26},{10... | collective-permute-start | bytes 1032200 | tf_op jit(solution)/shard_map/ppermute | solution.py:352
  6.0 39.3 %collective-permute-start.3 = (bf16[168,1024]{1,0:T(8,128)(2,1)S(1)}, bf16[168,1024]{1,0:T(8,128)(2,1)S(1)}, u32[]{:S(2)}, u32[]{:S(2)}) collective-permute-start(bf16[168,1024]{1,0:T(8,128)(2,1)S(1)} %get-tuple-element.24), channel_id=1, source_target_pairs={{0,8},{8,0},{16,24},{24,16},{1,9},{9,1},{17,25},{25,17},{2,10},{10... | collective-permute-start | bytes 1032200 | tf_op jit(solution)/shard_map/ppermute | solution.py:352
  6.0 39.3 %collective-permute-start.4 = (bf16[168,1024]{1,0:T(8,128)(2,1)S(1)}, bf16[168,1024]{1,0:T(8,128)(2,1)S(1)}, u32[]{:S(2)}, u32[]{:S(2)}) collective-permute-start(bf16[168,1024]{1,0:T(8,128)(2,1)S(1)} %get-tuple-element.23.refs_0_), channel_id=1, source_target_pairs={{0,16},{8,24},{16,0},{24,8},{1,17},{9,25},{17,1},{25,9},{2,18},{10... | collective-permute-start | bytes 1032200 | tf_op jit(solution)/shard_map/ppermute | solution.py:352
  7.3 14.9 %collective-permute-start = (bf16[24,32]{1,0:T(8,128)(2,1)S(1)}, bf16[24,32]{1,0:T(8,128)(2,1)S(1)}, u32[]{:S(2)}, u32[]{:S(2)}) collective-permute-start(bf16[24,32]{1,0:T(8,128)(2,1)S(1)} %get-tuple-element.21.r0_ref), channel_id=1, source_target_pairs={{0,8},{8,0},{16,24},{24,16},{1,9},{9,1},{17,25},{25,17},{2,10},{10... | collective-permute-start | bytes 4616 | tf_op jit(solution)/shard_map/ppermute | solution.py:352
  7.5 37.8 %copy-start = (bf16[1,1024,1,128]{3,1,2,0:T(8,128)(2,1)S(1)}, bf16[1,1024,1,128]{3,1,2,0:T(8,128)(2,1)}, u32[]{:S(2)}) copy-start(bf16[1,1024,1,128]{3,1,2,0:T(8,128)(2,1)} %param.18) | copy-start | bytes 786436
  7.5 37.8 %copy-start.1 = (bf16[1,1024,1,128]{3,1,2,0:T(8,128)(2,1)S(1)}, bf16[1,1024,1,128]{3,1,2,0:T(8,128)(2,1)}, u32[]{:S(2)}) copy-start(bf16[1,1024,1,128]{3,1,2,0:T(8,128)(2,1)} %param.19) | copy-start | bytes 786436
  7.5 15.1 %collective-permute-start.2 = (bf16[24,32]{1,0:T(8,128)(2,1)S(1)}, bf16[24,32]{1,0:T(8,128)(2,1)S(1)}, u32[]{:S(2)}, u32[]{:S(2)}) collective-permute-start(bf16[24,32]{1,0:T(8,128)(2,1)S(1)} %get-tuple-element.22), channel_id=1, source_target_pairs={{0,24},{8,16},{16,8},{24,0},{1,25},{9,17},{17,9},{25,1},{2,26},{10... | collective-permute-start | bytes 4616 | tf_op jit(solution)/shard_map/ppermute | solution.py:352
  22.2 4.0 %collective-permute-start.1 = (bf16[24,32]{1,0:T(8,128)(2,1)S(1)}, bf16[24,32]{1,0:T(8,128)(2,1)S(1)}, u32[]{:S(2)}, u32[]{:S(2)}) collective-permute-start(bf16[24,32]{1,0:T(8,128)(2,1)S(1)} %get-tuple-element.22), channel_id=1, source_target_pairs={{0,16},{8,24},{16,0},{24,8},{1,17},{9,25},{17,1},{25,9},{2,18},{10... | collective-permute-start | bytes 4616 | tf_op jit(solution)/shard_map/ppermute | solution.py:352
  47.1 1.3 %collective-permute-start.6 = (bf16[96,256]{1,0:T(8,128)(2,1)S(1)}, bf16[96,256]{1,0:T(8,128)(2,1)S(1)}, u32[]{:S(2)}, u32[]{:S(2)}) collective-permute-start(bf16[96,256]{1,0:T(8,128)(2,1)S(1)} %get-tuple-element.30), channel_id=1, source_target_pairs={{0,1},{1,0},{2,3},{3,2},{4,5},{5,4},{6,7},{7,6},{8,9},{9,8},{10,11... | collective-permute-start | bytes 147464 | tf_op jit(solution)/shard_map/ppermute | solution.py:352
  48.4 4.2 %collective-permute-start.9 = (bf16[96,256]{1,0:T(8,128)(2,1)S(1)}, bf16[96,256]{1,0:T(8,128)(2,1)S(1)}, u32[]{:S(2)}, u32[]{:S(2)}) collective-permute-start(bf16[96,256]{1,0:T(8,128)(2,1)S(1)} %add_convert_fusion.9), channel_id=1, source_target_pairs={{0,6},{1,7},{2,4},{3,5},{4,2},{5,3},{6,0},{7,1},{32,33},{33,32},{3... | collective-permute-start | bytes 147464 | tf_op jit(solution)/shard_map/ppermute | solution.py:445
  49.4 4.5 %collective-permute-start.8 = (bf16[96,256]{1,0:T(8,128)(2,1)S(1)}, bf16[96,256]{1,0:T(8,128)(2,1)S(1)}, u32[]{:S(2)}, u32[]{:S(2)}) collective-permute-start(bf16[96,256]{1,0:T(8,128)(2,1)S(1)} %add_convert_fusion.9), channel_id=1, source_target_pairs={{0,4},{1,5},{2,6},{3,7},{4,0},{5,1},{6,2},{7,3},{32,33},{33,32},{3... | collective-permute-start | bytes 147464 | tf_op jit(solution)/shard_map/ppermute | solution.py:445
  50.5 3.4 %collective-permute-start.7 = (bf16[96,256]{1,0:T(8,128)(2,1)S(1)}, bf16[96,256]{1,0:T(8,128)(2,1)S(1)}, u32[]{:S(2)}, u32[]{:S(2)}) collective-permute-start(bf16[96,256]{1,0:T(8,128)(2,1)S(1)} %add_convert_fusion.9), channel_id=1, source_target_pairs={{0,2},{1,3},{2,0},{3,1},{4,6},{5,7},{6,4},{7,5},{32,33},{33,32},{3... | collective-permute-start | bytes 147464 | tf_op jit(solution)/shard_map/ppermute | solution.py:445
  54.0 5.1 %collective-permute-start.12 = (bf16[96,256]{1,0:T(8,128)(2,1)S(1)}, bf16[96,256]{1,0:T(8,128)(2,1)S(1)}, u32[]{:S(2)}, u32[]{:S(2)}) collective-permute-start(bf16[96,256]{1,0:T(8,128)(2,1)S(1)} %add_convert_fusion.7), channel_id=1, source_target_pairs={{0,40},{8,32},{32,72},{40,64},{64,104},{72,96},{96,8},{104,0},{1,4... | collective-permute-start | bytes 147464 | tf_op jit(solution)/shard_map/ppermute | solution.py:452
  54.0 7.9 %collective-permute-start.10 = (bf16[96,256]{1,0:T(8,128)(2,1)S(1)}, bf16[96,256]{1,0:T(8,128)(2,1)S(1)}, u32[]{:S(2)}, u32[]{:S(2)}) collective-permute-start(bf16[96,256]{1,0:T(8,128)(2,1)S(1)} %add_convert_fusion.7), channel_id=1, source_target_pairs={{0,32},{32,64},{64,96},{96,0},{1,33},{33,65},{65,97},{97,1},{2,34}... | collective-permute-start | bytes 147464 | tf_op jit(solution)/shard_map/ppermute | solution.py:451
  59.1 3.7 %collective-permute-start.13 = (bf16[96,256]{1,0:T(8,128)(2,1)S(1)}, bf16[96,256]{1,0:T(8,128)(2,1)S(1)}, u32[]{:S(2)}, u32[]{:S(2)}) collective-permute-start(bf16[96,256]{1,0:T(8,128)(2,1)S(1)} %collective-permute-done.12.c_ref), channel_id=1, source_target_pairs={{0,1},{1,0},{2,3},{3,2},{4,5},{5,4},{6,7},{7,6},{8,9},{9,8},{10,11... | collective-permute-start | bytes 147464 | tf_op jit(solution)/shard_map/ppermute | solution.py:352
  61.9 1.2 %collective-permute-start.11 = (bf16[96,256]{1,0:T(8,128)(2,1)S(1)}, bf16[96,256]{1,0:T(8,128)(2,1)S(1)}, u32[]{:S(2)}, u32[]{:S(2)}) collective-permute-start(bf16[96,256]{1,0:T(8,128)(2,1)S(1)} %collective-permute-done.10.a_ref), channel_id=1, source_target_pairs={{0,1},{1,0},{2,3},{3,2},{4,5},{5,4},{6,7},{7,6},{8,9},{9,8},{10,11... | collective-permute-start | bytes 147464 | tf_op jit(solution)/shard_map/ppermute | solution.py:352
  64.8 1.3 %collective-permute-start.14 = (bf16[96,256]{1,0:T(8,128)(2,1)S(1)}, bf16[96,256]{1,0:T(8,128)(2,1)S(1)}, u32[]{:S(2)}, u32[]{:S(2)}) collective-permute-start(bf16[96,256]{1,0:T(8,128)(2,1)S(1)} %get-tuple-element.32), channel_id=1, source_target_pairs={{0,1},{1,0},{2,3},{3,2},{4,5},{5,4},{6,7},{7,6},{8,9},{9,8},{10,11... | collective-permute-start | bytes 147464 | tf_op jit(solution)/shard_map/ppermute | solution.py:352
  66.1 1.3 %collective-permute-start.17 = (bf16[96,256]{1,0:T(8,128)(2,1)S(1)}, bf16[96,256]{1,0:T(8,128)(2,1)S(1)}, u32[]{:S(2)}, u32[]{:S(2)}) collective-permute-start(bf16[96,256]{1,0:T(8,128)(2,1)S(1)} %add_convert_fusion.6), channel_id=1, source_target_pairs={{0,1},{1,0},{2,3},{3,2},{4,5},{5,4},{6,7},{7,6},{32,38},{33,39},{3... | collective-permute-start | bytes 147464 | tf_op jit(solution)/shard_map/ppermute | solution.py:445
  66.4 1.2 %collective-permute-start.16 = (bf16[96,256]{1,0:T(8,128)(2,1)S(1)}, bf16[96,256]{1,0:T(8,128)(2,1)S(1)}, u32[]{:S(2)}, u32[]{:S(2)}) collective-permute-start(bf16[96,256]{1,0:T(8,128)(2,1)S(1)} %add_convert_fusion.6), channel_id=1, source_target_pairs={{0,1},{1,0},{2,3},{3,2},{4,5},{5,4},{6,7},{7,6},{32,36},{33,37},{3... | collective-permute-start | bytes 147464 | tf_op jit(solution)/shard_map/ppermute | solution.py:445
  66.7 1.2 %collective-permute-start.15 = (bf16[96,256]{1,0:T(8,128)(2,1)S(1)}, bf16[96,256]{1,0:T(8,128)(2,1)S(1)}, u32[]{:S(2)}, u32[]{:S(2)}) collective-permute-start(bf16[96,256]{1,0:T(8,128)(2,1)S(1)} %add_convert_fusion.6), channel_id=1, source_target_pairs={{0,1},{1,0},{2,3},{3,2},{4,5},{5,4},{6,7},{7,6},{32,34},{33,35},{3... | collective-permute-start | bytes 147464 | tf_op jit(solution)/shard_map/ppermute | solution.py:445
  68.0 5.1 %collective-permute-start.20 = (bf16[96,256]{1,0:T(8,128)(2,1)S(1)}, bf16[96,256]{1,0:T(8,128)(2,1)S(1)}, u32[]{:S(2)}, u32[]{:S(2)}) collective-permute-start(bf16[96,256]{1,0:T(8,128)(2,1)S(1)} %add_convert_fusion.4), channel_id=1, source_target_pairs={{0,40},{8,32},{32,72},{40,64},{64,104},{72,96},{96,8},{104,0},{1,4... | collective-permute-start | bytes 147464 | tf_op jit(solution)/shard_map/ppermute | solution.py:452
  71.0 4.2 %collective-permute-start.18 = (bf16[96,256]{1,0:T(8,128)(2,1)S(1)}, bf16[96,256]{1,0:T(8,128)(2,1)S(1)}, u32[]{:S(2)}, u32[]{:S(2)}) collective-permute-start(bf16[96,256]{1,0:T(8,128)(2,1)S(1)} %add_convert_fusion.4), channel_id=1, source_target_pairs={{0,32},{32,64},{64,96},{96,0},{1,33},{33,65},{65,97},{97,1},{2,34}... | collective-permute-start | bytes 147464 | tf_op jit(solution)/shard_map/ppermute | solution.py:451
  73.1 5.2 %collective-permute-start.21 = (bf16[96,256]{1,0:T(8,128)(2,1)S(1)}, bf16[96,256]{1,0:T(8,128)(2,1)S(1)}, u32[]{:S(2)}, u32[]{:S(2)}) collective-permute-start(bf16[96,256]{1,0:T(8,128)(2,1)S(1)} %collective-permute-done.20.c_ref), channel_id=1, source_target_pairs={{0,1},{1,0},{2,3},{3,2},{4,5},{5,4},{6,7},{7,6},{8,9},{9,8},{10,11... | collective-permute-start | bytes 147464 | tf_op jit(solution)/shard_map/ppermute | solution.py:352
  75.2 4.1 %collective-permute-start.19 = (bf16[96,256]{1,0:T(8,128)(2,1)S(1)}, bf16[96,256]{1,0:T(8,128)(2,1)S(1)}, u32[]{:S(2)}, u32[]{:S(2)}) collective-permute-start(bf16[96,256]{1,0:T(8,128)(2,1)S(1)} %collective-permute-done.18.a_ref), channel_id=1, source_target_pairs={{0,1},{1,0},{2,3},{3,2},{4,5},{5,4},{6,7},{7,6},{8,9},{9,8},{10,11... | collective-permute-start | bytes 147464 | tf_op jit(solution)/shard_map/ppermute | solution.py:352
  80.9 1.3 %collective-permute-start.22 = (bf16[96,256]{1,0:T(8,128)(2,1)S(1)}, bf16[96,256]{1,0:T(8,128)(2,1)S(1)}, u32[]{:S(2)}, u32[]{:S(2)}) collective-permute-start(bf16[96,256]{1,0:T(8,128)(2,1)S(1)} %get-tuple-element.34), channel_id=1, source_target_pairs={{0,1},{1,0},{2,3},{3,2},{4,5},{5,4},{6,7},{7,6},{8,9},{9,8},{10,11... | collective-permute-start | bytes 147464 | tf_op jit(solution)/shard_map/ppermute | solution.py:352
  82.2 1.3 %collective-permute-start.25 = (bf16[96,256]{1,0:T(8,128)(2,1)S(1)}, bf16[96,256]{1,0:T(8,128)(2,1)S(1)}, u32[]{:S(2)}, u32[]{:S(2)}) collective-permute-start(bf16[96,256]{1,0:T(8,128)(2,1)S(1)} %add_convert_fusion.3), channel_id=1, source_target_pairs={{0,1},{1,0},{2,3},{3,2},{4,5},{5,4},{6,7},{7,6},{32,33},{33,32},{3... | collective-permute-start | bytes 147464 | tf_op jit(solution)/shard_map/ppermute | solution.py:445
  82.6 1.2 %collective-permute-start.24 = (bf16[96,256]{1,0:T(8,128)(2,1)S(1)}, bf16[96,256]{1,0:T(8,128)(2,1)S(1)}, u32[]{:S(2)}, u32[]{:S(2)}) collective-permute-start(bf16[96,256]{1,0:T(8,128)(2,1)S(1)} %add_convert_fusion.3), channel_id=1, source_target_pairs={{0,1},{1,0},{2,3},{3,2},{4,5},{5,4},{6,7},{7,6},{32,33},{33,32},{3... | collective-permute-start | bytes 147464 | tf_op jit(solution)/shard_map/ppermute | solution.py:445
  82.9 1.2 %collective-permute-start.23 = (bf16[96,256]{1,0:T(8,128)(2,1)S(1)}, bf16[96,256]{1,0:T(8,128)(2,1)S(1)}, u32[]{:S(2)}, u32[]{:S(2)}) collective-permute-start(bf16[96,256]{1,0:T(8,128)(2,1)S(1)} %add_convert_fusion.3), channel_id=1, source_target_pairs={{0,1},{1,0},{2,3},{3,2},{4,5},{5,4},{6,7},{7,6},{32,33},{33,32},{3... | collective-permute-start | bytes 147464 | tf_op jit(solution)/shard_map/ppermute | solution.py:445
  84.2 5.1 %collective-permute-start.28 = (bf16[96,256]{1,0:T(8,128)(2,1)S(1)}, bf16[96,256]{1,0:T(8,128)(2,1)S(1)}, u32[]{:S(2)}, u32[]{:S(2)}) collective-permute-start(bf16[96,256]{1,0:T(8,128)(2,1)S(1)} %add_convert_fusion.1), channel_id=1, source_target_pairs={{0,40},{8,32},{32,72},{40,64},{64,104},{72,96},{96,8},{104,0},{1,4... | collective-permute-start | bytes 147464 | tf_op jit(solution)/shard_map/ppermute | solution.py:452
  84.3 6.8 %collective-permute-start.26 = (bf16[96,256]{1,0:T(8,128)(2,1)S(1)}, bf16[96,256]{1,0:T(8,128)(2,1)S(1)}, u32[]{:S(2)}, u32[]{:S(2)}) collective-permute-start(bf16[96,256]{1,0:T(8,128)(2,1)S(1)} %add_convert_fusion.1), channel_id=1, source_target_pairs={{0,32},{32,64},{64,96},{96,0},{1,33},{33,65},{65,97},{97,1},{2,34}... | collective-permute-start | bytes 147464 | tf_op jit(solution)/shard_map/ppermute | solution.py:451
  89.3 2.6 %collective-permute-start.29 = (bf16[96,256]{1,0:T(8,128)(2,1)S(1)}, bf16[96,256]{1,0:T(8,128)(2,1)S(1)}, u32[]{:S(2)}, u32[]{:S(2)}) collective-permute-start(bf16[96,256]{1,0:T(8,128)(2,1)S(1)} %collective-permute-done.28.c_ref), channel_id=1, source_target_pairs={{0,1},{1,0},{2,3},{3,2},{4,5},{5,4},{6,7},{7,6},{8,9},{9,8},{10,11... | collective-permute-start | bytes 147464 | tf_op jit(solution)/shard_map/ppermute | solution.py:352
  91.0 1.2 %collective-permute-start.27 = (bf16[96,256]{1,0:T(8,128)(2,1)S(1)}, bf16[96,256]{1,0:T(8,128)(2,1)S(1)}, u32[]{:S(2)}, u32[]{:S(2)}) collective-permute-start(bf16[96,256]{1,0:T(8,128)(2,1)S(1)} %collective-permute-done.26.a_ref.mine_ref), channel_id=1, source_target_pairs={{0,1},{1,0},{2,3},{3,2},{4,5},{5,4},{6,7},{7,6},{8,9},{9,8},{10,11... | collective-permute-start | bytes 147464 | tf_op jit(solution)/shard_map/ppermute | solution.py:352
  93.9 1.3 %collective-permute-start.30 = (bf16[96,256]{1,0:T(8,128)(2,1)S(1)}, bf16[96,256]{1,0:T(8,128)(2,1)S(1)}, u32[]{:S(2)}, u32[]{:S(2)}) collective-permute-start(bf16[96,256]{1,0:T(8,128)(2,1)S(1)} %get-tuple-element.36), channel_id=1, source_target_pairs={{0,1},{1,0},{2,3},{3,2},{4,5},{5,4},{6,7},{7,6},{8,9},{9,8},{10,11... | collective-permute-start | bytes 147464 | tf_op jit(solution)/shard_map/ppermute | solution.py:352
  95.3 1.3 %collective-permute-start.33 = (bf16[96,256]{1,0:T(8,128)(2,1)S(1)}, bf16[96,256]{1,0:T(8,128)(2,1)S(1)}, u32[]{:S(2)}, u32[]{:S(2)}) collective-permute-start(bf16[96,256]{1,0:T(8,128)(2,1)S(1)} %add_convert_fusion.m0_ref), channel_id=1, source_target_pairs={{0,1},{1,0},{2,3},{3,2},{4,5},{5,4},{6,7},{7,6},{32,33},{33,32},{3... | collective-permute-start | bytes 147464 | tf_op jit(solution)/shard_map/ppermute | solution.py:445
  95.5 1.2 %collective-permute-start.32 = (bf16[96,256]{1,0:T(8,128)(2,1)S(1)}, bf16[96,256]{1,0:T(8,128)(2,1)S(1)}, u32[]{:S(2)}, u32[]{:S(2)}) collective-permute-start(bf16[96,256]{1,0:T(8,128)(2,1)S(1)} %add_convert_fusion.m0_ref), channel_id=1, source_target_pairs={{0,1},{1,0},{2,3},{3,2},{4,5},{5,4},{6,7},{7,6},{32,33},{33,32},{3... | collective-permute-start | bytes 147464 | tf_op jit(solution)/shard_map/ppermute | solution.py:445
  95.8 1.2 %collective-permute-start.31 = (bf16[96,256]{1,0:T(8,128)(2,1)S(1)}, bf16[96,256]{1,0:T(8,128)(2,1)S(1)}, u32[]{:S(2)}, u32[]{:S(2)}) collective-permute-start(bf16[96,256]{1,0:T(8,128)(2,1)S(1)} %add_convert_fusion.m0_ref), channel_id=1, source_target_pairs={{0,1},{1,0},{2,3},{3,2},{4,5},{5,4},{6,7},{7,6},{32,33},{33,32},{3... | collective-permute-start | bytes 147464 | tf_op jit(solution)/shard_map/ppermute | solution.py:445
